TPU v7x, 512 devices: a whole 4x4x16 slice. The times are simulated.
512 devices in a mesh: ep: 32 (over z, core), tp: 16 (over y, x).
Axes of the slice: x: 4, y: 4, z: 16, core: 2. Of those that a mesh axis runs over, the one named last changes fastest.
Arguments:
- tokens: bfloat16 [4096, 2048], P('ep'), may hold values from -6 to 6
- selected: int32 [32, 1024], P(None, 'ep'), may hold values from -1 to 127, as said below
- affinity: float32 [32, 1024], P(None, 'ep'), may hold values from 0.05 to 1
- w_gate: bfloat16 [32, 2048, 2048], P('ep', None, 'tp'), may hold values from -0.125 to 0.125
- w_up: bfloat16 [32, 2048, 2048], P('ep', None, 'tp'), may hold values from -0.125 to 0.125
- w_down: bfloat16 [32, 2048, 2048], P('ep', 'tp'), may hold values from -0.125 to 0.125
Outputs:
- combined: bfloat16 [4096, 2048], P('ep', 'tp')
Inputs may be any that keep to these rules, and one draw needn't show every extreme that they name: `selected`: row e holds 32 aligned groups of 32 entries; the live entries of group j are distinct positions within the j-th block of 128 tokens, stand at the front of the group and are followed by -1; each row has 512 live entries in all, the number in a group varies, and some group of every row is full.
All inputs are finite; a program needn't handle non-finite values.
Results may differ from a plain program's by a relative error of at most 0.015.
Values may be sent and summed in bfloat16 or wider, within the bound.
No kernel may reach another device: no remote copies, remote signals or barrier semaphores. Data moves between devices by JAX's collectives and lax.ppermute only.
A program may use at most 64 MiB of HBM per device.

v0:
```python
import jax
import jax.numpy as jnp
from jax import lax
from jax.sharding import Mesh
from jax.sharding import PartitionSpec as P

EP = ("ep_0", "ep_1")


def in_blocks(array, dim, peers):
    dims = array.shape
    parts = array.reshape(*dims[:dim], peers, dims[dim] // peers, *dims[dim + 1 :])
    return jnp.moveaxis(parts, dim, 0)


def joined_along(parts, dim):
    dims = list(parts.shape[1:])
    dims[dim] *= parts.shape[0]
    return jnp.moveaxis(parts, 0, dim).reshape(dims)


def moved_by_axis(parts, axes, order):
    dims = [lax.axis_size(a) for a in axes]
    parts = parts.reshape(*dims, *parts.shape[1:])
    for k in order:
        parts = lax.all_to_all(parts, axes[k], split_axis=k, concat_axis=k, tiled=True)
    return parts.reshape(-1, *parts.shape[len(axes) :])


def two_step_exchange(array, groups, order, split_dim, concat_dim):
    peers = lax.axis_size(groups[0]) * lax.axis_size(groups[1])
    parts = in_blocks(array, split_dim, peers)
    return joined_along(moved_by_axis(parts, groups, order), concat_dim)


def sent_to_all(array, axis):
    peers = lax.axis_size(axis)
    return lax.all_to_all(
        jnp.broadcast_to(array[None], (peers, *array.shape)), axis, 0, 0, tiled=True
    )


def gather_directly(array, axis, dim):
    parts = sent_to_all(array, axis)
    return joined_along(parts, dim)


def summed_on_arrival(array, axis, dim):
    peers = lax.axis_size(axis)
    parts = lax.all_to_all(in_blocks(array, dim, peers), axis, 0, 0, tiled=True)
    return jnp.sum(parts.astype(jnp.float32), axis=0)


def per_device(tokens, selected, affinity, w_gate, w_up, w_down):
    ep_count = lax.axis_size(EP)
    tp_count = lax.axis_size("tp")
    local_tokens = tokens.shape[0]
    width = tokens.shape[1]
    experts_here = w_gate.shape[0]
    slot_count = selected.shape[1]
    clamped = jnp.maximum(selected, 0)
    gathered = jnp.take(tokens, clamped, axis=0)
    column_span = width // tp_count
    slab = lax.dynamic_slice_in_dim(gathered, lax.axis_index("tp") * column_span, column_span, 2)
    arrived = two_step_exchange(slab, ("ep_0", "ep_1"), (1, 0), 0, 1)
    segment = gather_directly(arrived, "tp", 2)
    gate_more = jnp.einsum("ecd,edf->ecf", segment, w_gate, preferred_element_type=jnp.float32)
    up_more = jnp.einsum("ecd,edf->ecf", segment, w_up, preferred_element_type=jnp.float32)
    hidden = (jax.nn.silu(gate_more) * up_more).astype(jnp.bfloat16)
    summed = summed_on_arrival(
        jnp.einsum("efd,ecf->dec", w_down, hidden, preferred_element_type=jnp.float32).astype(
            jnp.bfloat16
        ),
        "tp",
        0,
    ).astype(jnp.bfloat16)
    summed = summed.reshape(summed.shape[0], experts_here, ep_count, slot_count)
    returned = lax.all_to_all(summed, EP, split_axis=2, concat_axis=1, tiled=True)
    feature_cols = returned.shape[0]
    returned = returned.reshape(feature_cols, experts_here * ep_count * slot_count)
    weights = jnp.where(selected >= 0, affinity, jnp.zeros_like(affinity)).reshape(-1)
    scaled_rows = returned.astype(jnp.float32).T * weights[:, None]
    combined = (
        jnp.zeros((local_tokens, feature_cols), jnp.float32)
        .at[clamped.reshape(-1)]
        .add(scaled_rows)
    )
    return combined.astype(jnp.bfloat16)


def solution(mesh):
    torus = Mesh(mesh.devices.reshape(16, 2, mesh.shape["tp"]), ("ep_0", "ep_1", "tp"))
    in_specs = (
        P(EP, None),
        P(None, EP),
        P(None, EP),
        P(EP, None, "tp"),
        P(EP, None, "tp"),
        P(EP, "tp", None),
    )
    out_specs = P(EP, "tp")
    return jax.shard_map(
        per_device, mesh=torus, in_specs=in_specs, out_specs=out_specs, check_vma=False
    )
```

profile of v0, /device:TPU:1, one launch (start us, length us, event | category | flops | bytes accessed | tf_op | source)
XLA Modules:
  0.0 214.4 jit_solution(5828575752059299651)
XLA Ops:
  0.0 0.0 copy-start
  0.0 0.8 broadcast_maximum_fusion
  0.8 0.7 broadcast_compare_fusion
  1.5 0.1 reshape.94
  1.6 0.0 copy-done
  1.6 6.0 %gather_fusion = bf16[1024,2048]{1,0:T(8,128)(2,1)} fusion(bf16[128,2048]{1,0:T(8,128)(2,1)S(1)} %copy-done, s32[1024]{0:T(1024)S(1)} %broadcast_clamp_fusion), kind=kCustom, calls=%fused_computation | custom fusion | bytes 8392704 | tf_op jit(solution)/shard_map/jit(_take)/gather | solution.py:62
  7.6 1.1 dynamic-slice_select_fusion
  8.8 10.4 %all_to_all.29 = bf16[16,2,1,32,128]{4,3,0,2,1:T(8,128)(2,1)S(1)} all-to-all(bf16[16,2,1,32,128]{4,3,0,2,1:T(8,128)(2,1)S(1)} %copy.8), channel_id=1, replica_groups=mesh['ep_0'=16,'ep_1'=2,'tp'=16] {'ep_1'}, dimensions={1} | all-to-all | bytes 524288 | tf_op jit(solution)/shard_map/all_to_all | solution.py:26
  19.2 23.4 %all_to_all.30 = bf16[16,2,1,32,128]{4,3,1,2,0:T(8,128)(2,1)S(1)} all-to-all(bf16[16,2,1,32,128]{4,3,1,2,0:T(8,128)(2,1)S(1)} %copy.9), channel_id=1, replica_groups=mesh['ep_0'=16,'ep_1'=2,'tp'=16] {'ep_0'}, dimensions={0} | all-to-all | bytes 524288 | tf_op jit(solution)/shard_map/all_to_all | solution.py:26
  42.6 0.1 copy.10
  42.7 0.5 broadcast_in_dim.31
  43.3 0.0 copy-start.2
  43.3 53.3 %all_to_all.31 = bf16[16,1,1024,128]{2,3,1,0:T(8,128)(2,1)S(1)} all-to-all(bf16[16,1,1024,128]{2,3,1,0:T(8,128)(2,1)S(1)} %broadcast_in_dim.31), channel_id=1, replica_groups=mesh['ep_0'=16,'ep_1'=2,'tp'=16] {'tp'}, dimensions={0} | all-to-all | bytes 8388608 | tf_op jit(solution)/shard_map/all_to_all | solution.py:38
  96.6 0.0 copy-start.1
  96.6 0.0 copy-start.3
  96.6 0.0 copy-start.4
  96.6 1.9 copy-done.1
  98.6 0.0 copy-done.2
  98.6 1.3 fusion.7
  99.8 0.0 copy-done.3
  99.8 0.0 copy-done.4
  99.9 8.5 %convert_bitcast_fusion = bf16[1,128,16,8,128]{4,3,2,1,0:T(8,128)(2,1)} fusion(bf16[1024,2048]{0,1:T(8,128)(2,1)} %bitcast.36, bf16[1,128,2048]{2,1,0:T(8,128)(2,1)S(1)} %copy-done.3, bf16[1,2048,128]{2,1,0:T(8,128)(2,1)S(1)} %copy-done.4, f32[1024,128]{1,0:T(8,128)S(1)} %fusion.7), kind=kOutput, calls=%fused_computation.3 | convolution fusion | flops 1076625408 | bytes 9961472 | tf_op jit(solution)/shard_map/efd,ecf->dec/dot_general | solution.py:71
  108.4 3.3 %copy.15 = bf16[1,128,16,8,128]{4,3,1,0,2:T(8,128)(2,1)S(1)} copy(bf16[1,128,16,8,128]{4,3,2,1,0:T(8,128)(2,1)} %convert_bitcast_fusion) | data formatting | bytes 8388608 | tf_op jit(solution)/shard_map/reshape | solution.py:12
  111.6 47.9 %all_to_all.32 = bf16[16,128,1,1024]{1,3,2,0:T(8,128)(2,1)} all-to-all(bf16[16,128,1,1024]{1,3,2,0:T(8,128)(2,1)S(1)} %bitcast.37), channel_id=1, replica_groups=mesh['ep_0'=16,'ep_1'=2,'tp'=16] {'tp'}, dimensions={0} | all-to-all | bytes 8388608 | tf_op jit(solution)/shard_map/all_to_all | solution.py:50
  159.6 0.0 copy-start.5
  159.6 0.0 copy-start.6
  159.6 3.5 %reduce_sum.12 = bf16[128,1024]{0,1:T(8,128)(2,1)} reduce(bf16[16,128,1,1024]{1,3,2,0:T(8,128)(2,1)} %all_to_all.32, bf16[]{:T(256)} %constant.37.clone.1), dimensions={0,2}, to_apply=%region_0.1 | reduce | flops 1966080 | bytes 4456450 | tf_op jit(solution)/shard_map/reduce_sum | solution.py:51
  163.1 21.3 %all-to-all-start.4 = ((bf16[128,1,32,32]{0,3,1,2:T(8,128)(2,1)}), bf16[128,1,32,32]{0,3,1,2:T(8,128)(2,1)S(1)}, u32[]{:S(2)}, u32[]{:S(2)}) async-start(bf16[128,1,32,32]{0,3,1,2:T(8,128)(2,1)} %bitcast.14), calls=%async_computation.4 | async-start | bytes 524288 | tf_op jit(solution)/shard_map/all_to_all | solution.py:78
  184.5 0.1 reshape.84
  184.5 0.0 copy-done.5
  184.5 0.0 copy-done.6
  184.6 0.1 mul.28
  184.6 22.1 %all-to-all-done.4 = bf16[128,1,32,32]{0,3,1,2:T(8,128)(2,1)S(1)} async-done(((bf16[128,1,32,32]{0,3,1,2:T(8,128)(2,1)}), bf16[128,1,32,32]{0,3,1,2:T(8,128)(2,1)S(1)}, u32[]{:S(2)}, u32[]{:S(2)}) %all-to-all-start.4) | async-done | bytes 262176 | tf_op jit(solution)/shard_map/all_to_all | solution.py:78
  206.7 7.0 %scatter_custom_fusion = f32[128,128]{1,0:T(8,128)S(1)} fusion(s32[1024]{0:T(1024)S(1)} %bitcast.42, bf16[128,1024]{0,1:T(8,128)(2,1)S(1)} %bitcast.40, f32[1024]{0:T(1024)S(1)} %mul.28, f32[]{:T(128)} %constant.11.clone.1), kind=kCustom, calls=%fused_computation.8 | custom fusion | flops 393216 | bytes 331780 | tf_op jit(solution)/shard_map/scatter-add | solution.py:86
  213.8 0.6 convert_element_type.30
  (5 shorter events, 0.1 us)
Async XLA Ops:
  0.0 1.6 copy-start
  43.3 55.3 %copy-start.2 = (bf16[1,2048,128]{2,1,0:T(8,128)(2,1)S(1)}, bf16[1,2048,128]{2,1,0:T(8,128)(2,1)}, u32[]{:S(2)}) copy-start(bf16[1,2048,128]{2,1,0:T(8,128)(2,1)} %param.9) | copy-start | bytes 1572868
  96.6 1.9 copy-start.1
  96.6 3.2 %copy-start.3 = (bf16[1,128,2048]{2,1,0:T(8,128)(2,1)S(1)}, bf16[1,128,2048]{2,1,0:T(8,128)(2,1)}, u32[]{:S(2)}) copy-start(bf16[1,128,2048]{2,1,0:T(8,128)(2,1)} %param.11) | copy-start | bytes 1572868
  96.6 3.2 %copy-start.4 = (bf16[1,2048,128]{2,1,0:T(8,128)(2,1)S(1)}, bf16[1,2048,128]{2,1,0:T(8,128)(2,1)}, u32[]{:S(2)}) copy-start(bf16[1,2048,128]{2,1,0:T(8,128)(2,1)} %param.10) | copy-start | bytes 1572868
  159.6 25.0 %copy-start.5 = (s32[32,32]{1,0:T(8,128)S(1)}, s32[32,32]{1,0:T(8,128)}, u32[]{:S(2)}) copy-start(s32[32,32]{1,0:T(8,128)} %param.7) | copy-start | bytes 12292
  159.6 25.0 %copy-start.6 = (f32[32,32]{1,0:T(8,128)S(1)}, f32[32,32]{1,0:T(8,128)}, u32[]{:S(2)}) copy-start(f32[32,32]{1,0:T(8,128)} %param.8) | copy-start | bytes 12292
  163.1 43.6 %all-to-all-start.4 = ((bf16[128,1,32,32]{0,3,1,2:T(8,128)(2,1)}), bf16[128,1,32,32]{0,3,1,2:T(8,128)(2,1)S(1)}, u32[]{:S(2)}, u32[]{:S(2)}) async-start(bf16[128,1,32,32]{0,3,1,2:T(8,128)(2,1)} %bitcast.14), calls=%async_computation.4 | async-start | bytes 524288 | tf_op jit(solution)/shard_map/all_to_all | solution.py:78
where the time goes:
time: 215 us; the launch traced here: 214 us
  blocking collectives  135 us (63%)
  waiting for transfers between devices  22.1 us (10%)
  starting transfers between devices  21.3 us (10%)
  other arithmetic  13.9 us (6%)
  local copies, waits for them, and re-layouts  12.1 us (6%)
  matrix products  9.8 us (5%)
    all_to_all x1, blocking collectives, sent_to_all(): lax.all_to_all(jnp.broadcast_to(array[None], (peers, *array.shape)), axis...  53.3 us
    all_to_all x1, blocking collectives, summed_on_arrival(): parts = lax.all_to_all(in_blocks(array, dim, peers), axis, 0, 0, tiled=True)  47.9 us
    all_to_all x2, blocking collectives, moved_by_axis(): lax.all_to_all(parts, axes[k], split_axis=k, concat_axis=k, tiled=True)  33.8 us
    all_to_all x1, waiting for transfers between devices, per_device(): lax.all_to_all(summed, EP, split_axis=2, concat_axis=1, tiled=True)  22.1 us
    all_to_all x1, starting transfers between devices, per_device(): lax.all_to_all(summed, EP, split_axis=2, concat_axis=1, tiled=True)  21.3 us
    dot_general x1, matrix products, per_device(): jnp.einsum('efd,ecf->dec', w_down, hidden, preferred_element_type=jnp.flo...  8.52 us
    scatter-add x1, other arithmetic, per_device(): combined = jnp.zeros((local_tokens, feature_cols), jnp.float32).at[clampe...  7.04 us
    gather x1, local copies, waits for them, and re-layouts, per_device(): gathered = jnp.take(tokens, clamped, axis=0)  5.98 us
  transfers between devices with their start and end apart: 1, of which 1 were waited for; matrix products, arithmetic and copies ran while one was open for 0% of the time, Pallas kernels for 0%

commit v1 on v0

v1 whole, which is shorter than its diff:
```python
import jax
import jax.numpy as jnp
from jax import lax
from jax.experimental import pallas as pl
from jax.experimental.pallas import tpu as pltpu
from jax.sharding import Mesh
from jax.sharding import PartitionSpec as P

EP = ("ep_0", "ep_1")
BF = jnp.bfloat16
F32 = jnp.float32
EMPTY = 64.0
LIMIT = 32.0


def iota(shape, dim):
    return lax.broadcasted_iota(jnp.int32, shape, dim)


def dot(a, b):
    return jnp.dot(a, b, preferred_element_type=F32)


def one_hot(mask):
    return jnp.where(mask, 1.0, 0.0).astype(BF)


def pick_kernel(col_ref, selected_ref, affinity_ref, tokens_ref, rows_ref, mix_ref):
    experts, most = selected_ref.shape
    tok, width = tokens_ref.shape
    slots = experts * most
    sel = selected_ref[...].astype(F32).astype(BF)
    repeat = one_hot(iota((slots, experts), 0) // most == iota((slots, experts), 1))
    spread = dot(repeat, sel)
    own = iota((slots, most), 0) % most == iota((slots, most), 1)
    position = dot(jnp.where(own, spread, 0.0).astype(BF), jnp.ones((most, tok), BF))
    named = one_hot(position == iota((slots, tok), 1).astype(F32))
    rows = dot(named, tokens_ref[...])
    rows_ref[...] = jnp.where(position < 0.0, EMPTY, rows).astype(BF)
    tile = one_hot(iota((most, slots), 0) == iota((most, slots), 1) % most)
    mine = iota((experts, slots), 0) == iota((experts, slots), 1) // most

    def as_row(values):
        return jnp.sum(jnp.where(mine, dot(values, tile), 0.0), axis=0, keepdims=True)

    aff = affinity_ref[...]
    high = aff.astype(BF)
    low = (aff - high.astype(F32)).astype(BF)
    hit = as_row(sel) == iota((tok, slots), 0).astype(F32)
    mix_ref[0] = jnp.where(hit, as_row(high), 0.0).astype(BF)
    mix_ref[1] = jnp.where(hit, as_row(low), 0.0).astype(BF)


def compact_kernel(slots_ref, rows_ref):
    slots, width = slots_ref.shape
    count = rows_ref.shape[0]
    data = slots_ref[...]
    live = one_hot(data.astype(F32) < LIMIT)
    first = one_hot(iota((8, width), 1) == 0)
    live_row = lax.dot_general(first, live, (((1,), (1,)), ((), ())), preferred_element_type=F32)
    before = one_hot(iota((slots, slots), 0) < iota((slots, slots), 1))
    rank = dot(live_row.astype(BF), before)
    rank = jnp.where(live_row > 0.5, rank, -1.0)[0:1]
    take = one_hot(rank == iota((count, slots), 0).astype(F32))
    rows_ref[...] = dot(take, data).astype(BF)


def ffn_kernel(x_ref, gate_ref, up_ref, down_ref, out_ref):
    peers, rows, span = x_ref.shape
    x = jnp.concatenate([x_ref[k] for k in range(peers)], axis=1)
    gate = dot(x, gate_ref[0])
    up = dot(x, up_ref[0])
    hidden = (gate / (1.0 + jnp.exp(-gate)) * up).astype(BF)
    partial = dot(hidden, down_ref[0]).astype(BF)
    for k in range(peers):
        out_ref[k] = partial[:, k * span : (k + 1) * span]


def expand_kernel(parts_ref, slots_ref, out_ref):
    peers, count, width = parts_ref.shape
    slots = slots_ref.shape[0]
    total = parts_ref[0].astype(F32)
    for k in range(1, peers):
        total = total + parts_ref[k].astype(F32)
    live = one_hot(slots_ref[...].astype(F32) < LIMIT)
    before = one_hot(iota((slots, slots), 1) < iota((slots, slots), 0))
    rank = dot(before, live)
    rank = jnp.where(live > 0.5, rank, -1.0)
    lanes = iota((slots, width), 1).astype(F32)
    put = jnp.concatenate([one_hot(rank - k == lanes) for k in range(0, count, width)], axis=1)
    out_ref[...] = dot(put, total.astype(BF)).astype(BF)


def combine_kernel(mix_ref, rows_ref, out_ref):
    rows = rows_ref[...]
    out_ref[...] = (dot(mix_ref[0], rows) + dot(mix_ref[1], rows)).astype(BF)


def call(kernel, shapes, *args):
    return pl.pallas_call(kernel, out_shape=shapes)(*args)


def per_device(tokens, selected, affinity, w_gate, w_up, w_down):
    ep = lax.axis_size(EP)
    tp = lax.axis_size("tp")
    tok, width = tokens.shape
    experts, most = selected.shape
    slots = experts * most
    live = ep * most // 2
    span = width // tp
    col = lax.axis_index("tp").astype(jnp.int32).reshape(1)
    rows, mix = pl.pallas_call(
        pick_kernel,
        grid_spec=pltpu.PrefetchScalarGridSpec(
            num_scalar_prefetch=1,
            grid=(1,),
            in_specs=[
                pl.BlockSpec((experts, most), lambda i, c: (0, 0)),
                pl.BlockSpec((experts, most), lambda i, c: (0, 0)),
                pl.BlockSpec((tok, span), lambda i, c: (0, c[0])),
            ],
            out_specs=[
                pl.BlockSpec((slots, span), lambda i, c: (0, 0)),
                pl.BlockSpec((2, tok, slots), lambda i, c: (0, 0, 0)),
            ],
        ),
        out_shape=[
            jax.ShapeDtypeStruct((slots, span), BF),
            jax.ShapeDtypeStruct((2, tok, slots), BF),
        ],
    )(col, selected, affinity, tokens)
    arrived = lax.all_to_all(rows.reshape(experts, most, span), EP, 0, 0, tiled=True)
    arrived = arrived.reshape(ep * most, span)
    packed = call(compact_kernel, jax.ShapeDtypeStruct((live, span), BF), arrived)
    chosen = lax.all_to_all(
        jnp.broadcast_to(packed[None], (tp, live, span)), "tp", 0, 0, tiled=True
    )
    steps = 2
    part = live // steps
    partial = pl.pallas_call(
        ffn_kernel,
        grid=(steps,),
        in_specs=[
            pl.BlockSpec((tp, part, span), lambda i: (0, i, 0)),
            pl.BlockSpec(w_gate.shape, lambda i: (0, 0, 0)),
            pl.BlockSpec(w_up.shape, lambda i: (0, 0, 0)),
            pl.BlockSpec(w_down.shape, lambda i: (0, 0, 0)),
        ],
        out_specs=pl.BlockSpec((tp, part, span), lambda i: (0, i, 0)),
        out_shape=jax.ShapeDtypeStruct((tp, live, span), BF),
    )(chosen, w_gate, w_up, w_down)
    summands = lax.all_to_all(partial, "tp", 0, 0, tiled=True)
    result = call(
        expand_kernel, jax.ShapeDtypeStruct((ep * most, span), BF), summands, arrived
    )
    returned = lax.all_to_all(result.reshape(ep, most, span), EP, 0, 0, tiled=True)
    return call(
        combine_kernel,
        jax.ShapeDtypeStruct((tok, span), BF),
        mix,
        returned.reshape(slots, span),
    )


def solution(mesh):
    torus = Mesh(mesh.devices.reshape(16, 2, mesh.shape["tp"]), ("ep_0", "ep_1", "tp"))
    in_specs = (
        P(EP, None),
        P(None, EP),
        P(None, EP),
        P(EP, None, "tp"),
        P(EP, None, "tp"),
        P(EP, "tp", None),
    )
    return jax.shard_map(
        per_device, mesh=torus, in_specs=in_specs, out_specs=P(EP, "tp"), check_vma=False
    )
```

time: 215 us -> 151 us (0.70)
  waiting for transfers between devices: 22.1 us -> 0 us
  starting transfers between devices: 21.3 us -> 0 us
  Pallas kernels: 0 us -> 15.2 us
  other arithmetic: 13.9 us -> 0 us
  local copies, waits for them, and re-layouts: 12.1 us -> 1.3 us
  matrix products: 9.8 us -> 0 us
    all_to_all x1 -> x0, waiting for transfers between devices: 22.1 us -> none  [per_device(): lax.all_to_all(summed, EP, split_axis=2, concat_axis=1, tiled=True)]
    all_to_all x1 -> x0, starting transfers between devices: 21.3 us -> none  [per_device(): lax.all_to_all(summed, EP, split_axis=2, concat_axis=1, tiled=True)]
    pallas_call x0 -> x5, Pallas kernels: none -> 15.2 us  [the longest x3 8.14 us: call(): return pl.pallas_call(kernel, out_shape=shapes)(*args)]
    dot_general x2 -> x0, matrix products: 9.8 us -> none  [the longest x1 8.52 us: per_device(): jnp.einsum('efd,ecf->dec', w_down, hidden, preferred_element_type=jnp.flo...]
    scatter-add x1 -> x0, other arithmetic: 7.04 us -> none  [per_device(): combined = jnp.zeros((local_tokens, feature_cols), jnp.float32).at[clampe...]
    gather x1 -> x0, local copies, waits for them, and re-layouts: 5.98 us -> none  [per_device(): gathered = jnp.take(tokens, clamped, axis=0)]
    reduce_sum x1 -> x0, other arithmetic: 3.54 us -> none  [summed_on_arrival(): return jnp.sum(parts.astype(jnp.float32), axis=0)]
    reshape x2 -> x0, local copies, waits for them, and re-layouts: 3.34 us -> none  [the longest x1 3.26 us: in_blocks(): array.reshape(*dims[:dim], peers, dims[dim] // peers, *dims[dim + 1:])]
  transfers between devices with their start and end apart: 1 -> 0, of which waited for: 1 -> 0; matrix products, arithmetic and copies ran while one was open for 0% -> 0% of each run, Pallas kernels for 0% -> 0%
where the time goes in v1:
time: 151 us; the launch traced here: 150 us
  blocking collectives  134 us (89%)
  Pallas kernels  15.2 us (10%)
    all_to_all x1, blocking collectives, per_device(): lax.all_to_all(rows.reshape(experts, most, span), EP, 0, 0, tiled=True)  39.1 us
    all_to_all x1, blocking collectives, per_device(): lax.all_to_all(jnp.broadcast_to(packed[None], (tp, live, span)), 'tp', 0,...  34 us
    all_to_all x1, blocking collectives, per_device(): summands = lax.all_to_all(partial, 'tp', 0, 0, tiled=True)  31.3 us
    all_to_all x1, blocking collectives, per_device(): lax.all_to_all(result.reshape(ep, most, span), EP, 0, 0, tiled=True)  29.7 us
    pallas_call x3, Pallas kernels, call(): return pl.pallas_call(kernel, out_shape=shapes)(*args)  8.14 us
    pallas_call x1, Pallas kernels, per_device(): pl.pallas_call(ffn_kernel, grid=(steps,), in_specs=[pl.BlockSpec((tp, par...  4.79 us

profile of v1, /device:TPU:1, one launch (start us, length us, event | category | flops | bytes accessed | tf_op | source)
XLA Modules:
  0.0 150.4 jit_solution(6108974847265864317)
XLA Ops:
  0.0 2.2 %shard_map.64 = (bf16[1024,128]{1,0:T(8,128)(2,1)}, bf16[2,128,1024]{2,1,0:T(8,128)(2,1)}) custom-call(s32[1]{0:T(128)} %bitcast.col_ref, s32[32,32]{1,0:T(8,128)} %selected_ref.1, f32[32,32]{1,0:T(8,128)} %affinity_ref.1, bf16[128,2048]{1,0:T(8,128)(2,1)} %tokens_ref.1), custom_call_target="tpu_custom_call" | custom-call | tf_op jit(solution)/shard_map/pallas_call | solution.py:112
  2.2 39.1 %all_to_all.20 = bf16[32,32,128]{2,1,0:T(8,128)(2,1)} all-to-all(bf16[32,32,128]{2,1,0:T(8,128)(2,1)} %bitcast.9), channel_id=1, replica_groups=mesh['ep_0'=16,'ep_1'=2,'tp'=16] {'ep_0','ep_1'}, dimensions={0} | all-to-all | bytes 524288 | tf_op jit(solution)/shard_map/all_to_all | solution.py:132
  41.3 2.4 %shard_map.65 = bf16[512,128]{1,0:T(8,128)(2,1)} custom-call(bf16[1024,128]{1,0:T(8,128)(2,1)} %bitcast.5), custom_call_target="tpu_custom_call" | custom-call | tf_op jit(solution)/shard_map/pallas_call | solution.py:100
  43.7 1.3 broadcast_in_dim.2
  45.0 34.0 %all_to_all.21.x_ref = bf16[16,512,128]{2,1,0:T(8,128)(2,1)} all-to-all(bf16[16,512,128]{2,1,0:T(8,128)(2,1)S(1)} %broadcast_in_dim.2), channel_id=1, replica_groups=mesh['ep_0'=16,'ep_1'=2,'tp'=16] {'tp'}, dimensions={0} | all-to-all | bytes 4194304 | tf_op jit(solution)/shard_map/all_to_all | solution.py:135
  79.0 4.8 %shard_map.66 = bf16[16,512,128]{2,1,0:T(8,128)(2,1)} custom-call(bf16[16,512,128]{2,1,0:T(8,128)(2,1)} %all_to_all.21.x_ref, bf16[1,2048,128]{2,1,0:T(8,128)(2,1)} %gate_ref.1, bf16[1,2048,128]{2,1,0:T(8,128)(2,1)} %up_ref.1, bf16[1,128,2048]{2,1,0:T(8,128)(2,1)} %down_ref.1), custom_call_target="tpu_custom_call" | custom-call | tf_op jit(solution)/shard_map/pallas_call | solution.py:140
  83.8 31.3 %all_to_all.22.parts_ref = bf16[16,512,128]{2,1,0:T(8,128)(2,1)} all-to-all(bf16[16,512,128]{2,1,0:T(8,128)(2,1)} %shard_map.66), channel_id=1, replica_groups=mesh['ep_0'=16,'ep_1'=2,'tp'=16] {'tp'}, dimensions={0} | all-to-all | bytes 4194304 | tf_op jit(solution)/shard_map/all_to_all | solution.py:152
  115.0 3.8 %shard_map.67 = bf16[1024,128]{1,0:T(8,128)(2,1)} custom-call(bf16[16,512,128]{2,1,0:T(8,128)(2,1)} %all_to_all.22.parts_ref, bf16[1024,128]{1,0:T(8,128)(2,1)} %bitcast.6), custom_call_target="tpu_custom_call" | custom-call | tf_op jit(solution)/shard_map/pallas_call | solution.py:100
  118.8 29.7 %all_to_all.23 = bf16[32,32,128]{2,1,0:T(8,128)(2,1)} all-to-all(bf16[32,32,128]{2,1,0:T(8,128)(2,1)} %bitcast.8), channel_id=1, replica_groups=mesh['ep_0'=16,'ep_1'=2,'tp'=16] {'ep_0','ep_1'}, dimensions={0} | all-to-all | bytes 524288 | tf_op jit(solution)/shard_map/all_to_all | solution.py:156
  148.4 2.0 %shard_map.68 = bf16[128,128]{1,0:T(8,128)(2,1)} custom-call(bf16[2,128,1024]{2,1,0:T(8,128)(2,1)} %get-tuple-element.7.mix_ref, bf16[1024,128]{1,0:T(8,128)(2,1)} %bitcast.7), custom_call_target="tpu_custom_call" | custom-call | tf_op jit(solution)/shard_map/pallas_call | solution.py:100

commit v2 on v1

v2 whole, which is shorter than its diff:
```python
import jax
import jax.numpy as jnp
from jax import lax
from jax.experimental import pallas as pl
from jax.experimental.pallas import tpu as pltpu
from jax.sharding import Mesh
from jax.sharding import PartitionSpec as P

EP = ("z", "c")
TP = ("g", "yy", "x")
TEAM = ("c", "yy", "x")
BF = jnp.bfloat16
F32 = jnp.float32
EMPTY = 64.0
LIMIT = 32.0
TRADE = [(0, 0), (1, 1), (6, 6), (7, 7), (4, 3), (3, 4), (5, 2), (2, 5)]
PAIR = [(0, 3), (3, 0), (1, 2), (2, 1)]
CORES = [(0, 1), (1, 0)]


def iota(shape, dim):
    return lax.broadcasted_iota(jnp.int32, shape, dim)


def dot(a, b):
    return jnp.dot(a, b, preferred_element_type=F32)


def one_hot(mask):
    return jnp.where(mask, 1.0, 0.0).astype(BF)


def pack_kernel(gate_ref, up_ref, down_ref, out_ref):
    width = gate_ref.shape[1]
    span = gate_ref.shape[2]
    out_ref[:width] = gate_ref[0]
    out_ref[width : 2 * width] = up_ref[0]
    for k in range(width // span):
        at = 2 * width + k * span
        out_ref[at : at + span] = down_ref[0, :, k * span : (k + 1) * span]


def pick_kernel(place_ref, selected_ref, affinity_ref, first_ref, second_ref, rows_ref, mix_ref):
    g = place_ref[2]
    experts, most = selected_ref.shape
    tok, width = first_ref.shape
    here = experts // 2
    slots = here * most
    sel = selected_ref[...].astype(F32).astype(BF)
    repeat = one_hot(2 * (iota((slots, experts), 0) // most) + g == iota((slots, experts), 1))
    own = iota((slots, most), 0) % most == iota((slots, most), 1)
    spread = jnp.where(own, dot(repeat, sel), 0.0).astype(BF)
    position = dot(spread, jnp.ones((most, tok), BF))
    named = one_hot(position == iota((slots, tok), 1).astype(F32))
    for c, ref in enumerate((first_ref, second_ref)):
        rows = jnp.where(position < 0.0, EMPTY, dot(named, ref[...])).astype(BF)
        rows_ref[:, c] = rows.reshape(here, most, width)
    tile = one_hot(iota((most, slots), 0) == iota((most, slots), 1) % most)
    mine = iota((experts, slots), 0) == 2 * (iota((experts, slots), 1) // most) + g

    def as_row(values):
        return jnp.sum(jnp.where(mine, dot(values, tile), 0.0), axis=0, keepdims=True)

    aff = affinity_ref[...]
    high = aff.astype(BF)
    low = (aff - high.astype(F32)).astype(BF)
    hit = as_row(sel) == iota((tok, slots), 0).astype(F32)
    mix_ref[0] = jnp.where(hit, as_row(high), 0.0).astype(BF)
    mix_ref[1] = jnp.where(hit, as_row(low), 0.0).astype(BF)


def compact_kernel(slots_ref, rows_ref):
    blocks, most, width = slots_ref.shape
    cores, peers, part, _ = rows_ref.shape
    slots = blocks * most
    count = cores * part
    data = slots_ref[...].reshape(slots, width)
    live = one_hot(data.astype(F32) < LIMIT)
    first = one_hot(iota((8, width), 1) == 0)
    live_row = lax.dot_general(first, live, (((1,), (1,)), ((), ())), preferred_element_type=F32)
    in_block = one_hot(iota((slots, blocks), 0) // most == iota((slots, blocks), 1))
    before = one_hot(iota((blocks, slots), 0) < iota((blocks, slots), 1) // most)
    counts = dot(live_row.astype(BF), in_block)
    rank = dot(counts.astype(BF), before) + (iota((8, slots), 1) % most).astype(F32)
    rank = jnp.where(live_row > 0.5, rank, -1.0)[0:1]
    take = one_hot(rank == iota((count, slots), 0).astype(F32))
    rows = dot(take, data).astype(BF)
    for c in range(cores):
        for k in range(peers):
            rows_ref[c, k] = rows[c * part : (c + 1) * part]


def seat(block, g):
    y = block // 4
    yy = (0, 1, 1, 0)[y]
    return (y // 2) * 8 + 4 * (yy + g - 2 * yy * g) + block % 4


def ffn_kernel(place_ref, x_ref, mine_ref, other_ref, out_ref):
    g = place_ref[2]
    peers, rows, span = x_ref.shape
    width = peers * span
    pair = (mine_ref, other_ref)
    x = jnp.concatenate([x_ref[seat(k, g)] for k in range(peers)], axis=1)
    gate = dot(x, jnp.concatenate([w[:width] for w in pair], axis=1))
    up = dot(x, jnp.concatenate([w[width : 2 * width] for w in pair], axis=1))
    hidden = (gate / (1.0 + jnp.exp(-gate)) * up).astype(BF)
    for k in range(0, peers, 2):
        at = 2 * width + k * span
        tiles = [
            jnp.concatenate([w[at + j * span : at + (j + 1) * span] for w in pair], axis=0)
            for j in range(2)
        ]
        partial = dot(hidden, jnp.concatenate(tiles, axis=1)).astype(BF)
        for j in range(2):
            out_ref[seat(k + j, g)] = partial[:, j * span : (j + 1) * span]


def expand_kernel(parts_ref, slots_ref, out_ref):
    cores, peers, part, width = parts_ref.shape
    blocks, most, _ = slots_ref.shape
    slots = blocks * most
    halves = []
    for c in range(cores):
        total = parts_ref[c, 0].astype(F32)
        for k in range(1, peers):
            total = total + parts_ref[c, k].astype(F32)
        halves.append(total.astype(BF))
    live = one_hot(slots_ref[...].reshape(slots, width).astype(F32) < LIMIT)
    in_block = one_hot(iota((blocks, slots), 0) == iota((blocks, slots), 1) // most)
    before = one_hot(iota((slots, blocks), 1) < iota((slots, blocks), 0) // most)
    counts = dot(in_block, live).astype(BF)
    rank = dot(before, counts) + (iota((slots, width), 0) % most).astype(F32)
    rank = jnp.where(live > 0.5, rank, -1.0)
    lanes = iota((slots, width), 1).astype(F32)
    put = [one_hot(rank - k == lanes) for k in range(0, cores * part, width)]
    rows = dot(jnp.concatenate(put, axis=1), jnp.concatenate(halves, axis=0)).astype(BF)
    out_ref[...] = rows.reshape(blocks, most, width)


def combine_kernel(place_ref, mix_ref, rows_ref, keep_ref, send_ref):
    here, cores, most, width = rows_ref.shape
    both = [rows_ref[:, c].reshape(here * most, width) for c in range(cores)]
    both = jnp.concatenate(both, axis=1)
    total = dot(mix_ref[0], both) + dot(mix_ref[1], both)
    mine = place_ref[2] == 0
    keep_ref[...] = jnp.where(mine, total[:, :width], total[:, width:])
    send_ref[...] = jnp.where(mine, total[:, width:], total[:, :width])


def whole(shape):
    return pl.BlockSpec(shape, lambda i, place: (0,) * len(shape))


def placed_call(kernel, place, outs, *args, specs=None):
    specs = specs or [whole(a.shape) for a in args]
    return pl.pallas_call(
        kernel,
        grid_spec=pltpu.PrefetchScalarGridSpec(
            num_scalar_prefetch=1,
            grid=(1,),
            in_specs=specs,
            out_specs=jax.tree.map(lambda o: whole(o.shape), outs),
        ),
        out_shape=outs,
    )(place, *args)


def array(shape, dtype=BF):
    return jax.ShapeDtypeStruct(shape, dtype)


def per_device(tokens, selected, affinity, w_gate, w_up, w_down):
    ep = lax.axis_size(EP)
    layers = lax.axis_size("z")
    team = lax.axis_size(TEAM)
    tok, width = tokens.shape
    experts, most = selected.shape
    span = width // team
    part = ep * most // 4
    g = lax.axis_index("g")
    y = 2 * g + lax.axis_index("yy")
    x = lax.axis_index("x")
    place = jnp.stack([4 * jnp.minimum(y, 3 - y) + x, 4 * jnp.maximum(y, 3 - y) + x, g])
    place = place.astype(jnp.int32)
    packed = pl.pallas_call(pack_kernel, out_shape=array((3 * width, span)))(
        w_gate, w_up, w_down
    )
    mine = lax.ppermute(packed, ("c", "g", "yy"), TRADE)
    other = lax.ppermute(mine, "c", CORES)
    rows, mix = placed_call(
        pick_kernel,
        place,
        [array((layers, 2, most, span)), array((2, tok, layers * most))],
        selected,
        affinity,
        tokens,
        tokens,
        specs=[
            whole(selected.shape),
            whole(affinity.shape),
            pl.BlockSpec((tok, span), lambda i, place: (0, place[0])),
            pl.BlockSpec((tok, span), lambda i, place: (0, place[1])),
        ],
    )
    arrived = lax.all_to_all(rows.reshape(ep, most, span), EP, 0, 0, tiled=True)
    copies = pl.pallas_call(compact_kernel, out_shape=array((2, team // 2, part, span)))(arrived)
    chosen = lax.all_to_all(copies.reshape(team, part, span), TEAM, 0, 0, tiled=True)
    partial = placed_call(ffn_kernel, place, array((team, part, span)), chosen, mine, other)
    summands = lax.all_to_all(partial, TEAM, 0, 0, tiled=True)
    result = pl.pallas_call(expand_kernel, out_shape=array((ep, most, span)))(
        summands.reshape(2, team // 2, part, span), arrived
    )
    returned = lax.all_to_all(result, EP, 0, 0, tiled=True)
    keep, send = placed_call(
        combine_kernel,
        place,
        [array((tok, span), F32), array((tok, span), F32)],
        mix,
        returned.reshape(layers, 2, most, span),
    )
    return (keep + lax.ppermute(send, ("g", "yy"), PAIR)).astype(BF)


def solution(mesh):
    torus = Mesh(mesh.devices.reshape(16, 2, 2, 2, 4), ("z", "c", "g", "yy", "x"))
    in_specs = (
        P(EP, None),
        P(None, EP),
        P(None, EP),
        P(EP, None, TP),
        P(EP, None, TP),
        P(EP, TP, None),
    )
    return jax.shard_map(
        per_device, mesh=torus, in_specs=in_specs, out_specs=P(EP, TP), check_vma=False
    )
```

time: 151 us -> 141 us (0.934)
  blocking collectives: 134 us -> 67.9 us
  starting transfers between devices: 0 us -> 25.9 us
  waiting for transfers between devices: 0 us -> 24.1 us
  Pallas kernels: 15.2 us -> 18.6 us
  other arithmetic: 0 us -> 2.06 us
    all_to_all x4 -> x3, blocking collectives: 134 us -> 67.9 us  [the longest x1 26 us: per_device(): returned = lax.all_to_all(result, EP, 0, 0, tiled=True)]
    all_to_all x0 -> x1, waiting for transfers between devices: none -> 20.1 us  [per_device(): arrived = lax.all_to_all(rows.reshape(ep, most, span), EP, 0, 0, tiled=True)]
    all_to_all x0 -> x1, starting transfers between devices: none -> 15.4 us  [per_device(): arrived = lax.all_to_all(rows.reshape(ep, most, span), EP, 0, 0, tiled=True)]
    ppermute x0 -> x3, starting transfers between devices: none -> 10.6 us  [the longest x1 6.01 us: per_device(): mine = lax.ppermute(packed, ('c', 'g', 'yy'), TRADE)]
    ppermute x0 -> x3, waiting for transfers between devices: none -> 4.01 us  [the longest x1 4 us: per_device(): return (keep + lax.ppermute(send, ('g', 'yy'), PAIR)).astype(BF)]
    pallas_call x5 -> x6, Pallas kernels: 15.2 us -> 18.6 us  [the longest x3 10.2 us: placed_call(): pl.pallas_call(kernel, grid_spec=pltpu.PrefetchScalarGridSpec(num_scalar_...]
    unnamed x0 -> x6, local copies, waits for them, and re-layouts: none -> 1.85 us
  transfers between devices with their start and end apart: 0 -> 4, of which waited for: 0 -> 2; matrix products, arithmetic and copies ran while one was open for 0% -> 0% of each run, Pallas kernels for 0% -> 4%
where the time goes in v2:
time: 141 us; the launch traced here: 140 us
  blocking collectives  67.9 us (48%)
  starting transfers between devices  25.9 us (18%)
  waiting for transfers between devices  24.1 us (17%)
  Pallas kernels  18.6 us (13%)
  other arithmetic  2.06 us (1%)
  local copies, waits for them, and re-layouts  1.85 us (1%)
    all_to_all x1, blocking collectives, per_device(): returned = lax.all_to_all(result, EP, 0, 0, tiled=True)  26 us
    all_to_all x1, blocking collectives, per_device(): lax.all_to_all(copies.reshape(team, part, span), TEAM, 0, 0, tiled=True)  21.3 us
    all_to_all x1, blocking collectives, per_device(): summands = lax.all_to_all(partial, TEAM, 0, 0, tiled=True)  20.6 us
    all_to_all x1, waiting for transfers between devices, per_device(): arrived = lax.all_to_all(rows.reshape(ep, most, span), EP, 0, 0, tiled=True)  20.1 us
    all_to_all x1, starting transfers between devices, per_device(): arrived = lax.all_to_all(rows.reshape(ep, most, span), EP, 0, 0, tiled=True)  15.4 us
    pallas_call x3, Pallas kernels, placed_call(): pl.pallas_call(kernel, grid_spec=pltpu.PrefetchScalarGridSpec(num_scalar_...  10.2 us
    ppermute x1, starting transfers between devices, per_device(): mine = lax.ppermute(packed, ('c', 'g', 'yy'), TRADE)  6.01 us
    ppermute x1, waiting for transfers between devices, per_device(): return (keep + lax.ppermute(send, ('g', 'yy'), PAIR)).astype(BF)  4 us
  transfers between devices with their start and end apart: 4, of which 2 were waited for; matrix products, arithmetic and copies ran while one was open for 0% of the time, Pallas kernels for 4%

profile of v2, /device:TPU:1, one launch (start us, length us, event | category | flops | bytes accessed | tf_op | source)
XLA Modules:
  0.0 140.5 jit_solution(13288922619905705492)
XLA Ops:
  0.0 2.7 %shard_map.66 = bf16[6144,128]{1,0:T(8,128)(2,1)} custom-call(bf16[1,2048,128]{2,1,0:T(8,128)(2,1)} %gate_ref.1, bf16[1,2048,128]{2,1,0:T(8,128)(2,1)} %up_ref.1, bf16[1,128,2048]{2,1,0:T(8,128)(2,1)} %down_ref.1), custom_call_target="tpu_custom_call" | custom-call | tf_op jit(solution)/shard_map/pallas_call | solution.py:186
  2.7 6.0 %collective-permute-start = (bf16[6144,128]{1,0:T(8,128)(2,1)}, bf16[6144,128]{1,0:T(8,128)(2,1)S(1)}, u32[]{:S(2)}, u32[]{:S(2)}) collective-permute-start(bf16[6144,128]{1,0:T(8,128)(2,1)} %shard_map.66), channel_id=1, source_target_pairs={{0,0},{4,4},{24,24},{28,28},{16,12},{12,16},{20,8},{8,20},{1,1},{5... | collective-permute-start | bytes 4718600 | tf_op jit(solution)/shard_map/ppermute | solution.py:189
  8.7 0.6 pad_add_fusion.place_ref
  9.3 2.7 %shard_map.64 = (bf16[16,2,32,128]{3,2,1,0:T(8,128)(2,1)}, bf16[2,128,512]{2,1,0:T(8,128)(2,1)}) custom-call(s32[3]{0:T(128)} %pad_add_fusion.place_ref, s32[32,32]{1,0:T(8,128)} %selected_ref.1, f32[32,32]{1,0:T(8,128)} %affinity_ref.1, bf16[128,2048]{1,0:T(8,128)(2,1)} %second_ref.1, bf16[128,2048]{1,0:T(8,128)(2,1)} %second_ref.1), custom_call_target="tpu_custom_call" | custom-call | tf_op jit(solution)/shard_map/pallas_call | solution.py:157
  12.0 15.4 %all-to-all-start = ((bf16[32,32,128]{2,1,0:T(8,128)(2,1)}), bf16[32,32,128]{2,1,0:T(8,128)(2,1)S(1)}, u32[]{:S(2)}, u32[]{:S(2)}) async-start(bf16[32,32,128]{2,1,0:T(8,128)(2,1)} %bitcast.10), calls=%async_computation | async-start | bytes 524288 | tf_op jit(solution)/shard_map/all_to_all | solution.py:206
  27.4 0.0 collective-permute-done.mine_ref
  27.4 0.0 copy-start.1
  27.4 2.1 %collective-permute-start.1 = (bf16[6144,128]{1,0:T(8,128)(2,1)S(1)}, bf16[6144,128]{1,0:T(8,128)(2,1)S(1)}, u32[]{:S(2)}, u32[]{:S(2)}) collective-permute-start(bf16[6144,128]{1,0:T(8,128)(2,1)S(1)} %collective-permute-done.mine_ref), channel_id=1, source_target_pairs={{0,16},{16,0},{1,17},{17,1},{2,18},{18,2},{3,19},{19,3},{4,20},{20... | collective-permute-start | bytes 4718600 | tf_op jit(solution)/shard_map/ppermute | solution.py:190
  29.6 20.1 %all-to-all-done.slots_ref = bf16[32,32,128]{2,1,0:T(8,128)(2,1)S(1)} async-done(((bf16[32,32,128]{2,1,0:T(8,128)(2,1)}), bf16[32,32,128]{2,1,0:T(8,128)(2,1)S(1)}, u32[]{:S(2)}, u32[]{:S(2)}) %all-to-all-start) | async-done | bytes 262176 | tf_op jit(solution)/shard_map/all_to_all | solution.py:206
  49.7 0.0 copy-start
  49.7 0.7 copy-done
  50.4 2.8 %shard_map.65 = bf16[2,8,256,128]{3,2,1,0:T(8,128)(2,1)} custom-call(bf16[32,32,128]{2,1,0:T(8,128)(2,1)} %copy-done), custom_call_target="tpu_custom_call" | custom-call | tf_op jit(solution)/shard_map/pallas_call | solution.py:207
  53.1 21.3 %all_to_all.20.x_ref = bf16[16,256,128]{2,1,0:T(8,128)(2,1)} all-to-all(bf16[16,256,128]{2,1,0:T(8,128)(2,1)} %bitcast.7), channel_id=1, replica_groups=mesh['z'=16,'c'=2,'g'=2,'yy'=2,'x'=4] {'c','yy','x'}, dimensions={0} | all-to-all | bytes 2097152 | tf_op jit(solution)/shard_map/all_to_all | solution.py:208
  74.4 0.0 collective-permute-done.1.other_ref
  74.4 0.0 copy-done.1
  74.4 0.0 copy-start.2
  74.4 1.1 copy-done.2
  75.6 4.9 %shard_map.67 = bf16[16,256,128]{2,1,0:T(8,128)(2,1)} custom-call(s32[3]{0:T(128)} %pad_add_fusion.place_ref, bf16[16,256,128]{2,1,0:T(8,128)(2,1)} %all_to_all.20.x_ref, bf16[6144,128]{1,0:T(8,128)(2,1)} %copy-done.1, bf16[6144,128]{1,0:T(8,128)(2,1)} %copy-done.2), custom_call_target="tpu_custom_call" | custom-call | tf_op jit(solution)/shard_map/pallas_call | solution.py:157
  80.5 20.6 %all_to_all.21 = bf16[16,256,128]{2,1,0:T(8,128)(2,1)} all-to-all(bf16[16,256,128]{2,1,0:T(8,128)(2,1)} %shard_map.67), channel_id=1, replica_groups=mesh['z'=16,'c'=2,'g'=2,'yy'=2,'x'=4] {'c','yy','x'}, dimensions={0} | all-to-all | bytes 2097152 | tf_op jit(solution)/shard_map/all_to_all | solution.py:210
  101.1 3.0 %shard_map.68 = bf16[32,32,128]{2,1,0:T(8,128)(2,1)} custom-call(bf16[2,8,256,128]{3,2,1,0:T(8,128)(2,1)} %bitcast.8, bf16[32,32,128]{2,1,0:T(8,128)(2,1)} %copy-done), custom_call_target="tpu_custom_call" | custom-call | tf_op jit(solution)/shard_map/pallas_call | solution.py:211
  104.0 26.0 %all_to_all.22 = bf16[32,32,128]{2,1,0:T(8,128)(2,1)} all-to-all(bf16[32,32,128]{2,1,0:T(8,128)(2,1)} %shard_map.68), channel_id=1, replica_groups=mesh['z'=16,'c'=2,'g'=2,'yy'=2,'x'=4] {'z','c'}, dimensions={0} | all-to-all | bytes 524288 | tf_op jit(solution)/shard_map/all_to_all | solution.py:214
  130.0 2.6 %shard_map.69 = (f32[128,128]{1,0:T(8,128)}, f32[128,128]{1,0:T(8,128)}) custom-call(s32[3]{0:T(128)} %pad_add_fusion.place_ref, bf16[2,128,512]{2,1,0:T(8,128)(2,1)} %get-tuple-element.9.mix_ref, bf16[16,2,32,128]{3,2,1,0:T(8,128)(2,1)} %bitcast.9), custom_call_target="tpu_custom_call" | custom-call | tf_op jit(solution)/shard_map/pallas_call | solution.py:157
  132.6 2.4 %collective-permute-start.2 = (f32[128,128]{1,0:T(8,128)}, f32[128,128]{1,0:T(8,128)S(1)}, u32[]{:S(2)}, u32[]{:S(2)}) collective-permute-start(f32[128,128]{1,0:T(8,128)} %get-tuple-element.12), channel_id=1, source_target_pairs={{0,12},{12,0},{4,8},{8,4},{1,13},{13,1},{5,9},{9,5},{2,14},{14,2},... | collective-permute-start | bytes 196616 | tf_op jit(solution)/shard_map/ppermute | solution.py:222
  135.0 4.0 %collective-permute-done.2 = f32[128,128]{1,0:T(8,128)S(1)} collective-permute-done((f32[128,128]{1,0:T(8,128)}, f32[128,128]{1,0:T(8,128)S(1)}, u32[]{:S(2)}, u32[]{:S(2)}) %collective-permute-start.2) | collective-permute-done | bytes 65568 | tf_op jit(solution)/shard_map/ppermute | solution.py:222
  139.0 1.5 %add_convert_fusion = bf16[128,128]{1,0:T(8,128)(2,1)} fusion(f32[128,128]{1,0:T(8,128)} %get-tuple-element.11, f32[128,128]{1,0:T(8,128)S(1)} %collective-permute-done.2), kind=kLoop, calls=%fused_computation | loop fusion | flops 32768 | bytes 163840 | tf_op jit(solution)/shard_map/convert_element_type | solution.py:222
Async XLA Ops:
  2.7 24.7 %collective-permute-start = (bf16[6144,128]{1,0:T(8,128)(2,1)}, bf16[6144,128]{1,0:T(8,128)(2,1)S(1)}, u32[]{:S(2)}, u32[]{:S(2)}) collective-permute-start(bf16[6144,128]{1,0:T(8,128)(2,1)} %shard_map.66), channel_id=1, source_target_pairs={{0,0},{4,4},{24,24},{28,28},{16,12},{12,16},{20,8},{8,20},{1,1},{5... | collective-permute-start | bytes 4718600 | tf_op jit(solution)/shard_map/ppermute | solution.py:189
  12.0 37.6 %all-to-all-start = ((bf16[32,32,128]{2,1,0:T(8,128)(2,1)}), bf16[32,32,128]{2,1,0:T(8,128)(2,1)S(1)}, u32[]{:S(2)}, u32[]{:S(2)}) async-start(bf16[32,32,128]{2,1,0:T(8,128)(2,1)} %bitcast.10), calls=%async_computation | async-start | bytes 524288 | tf_op jit(solution)/shard_map/all_to_all | solution.py:206
  27.4 47.0 %copy-start.1 = (bf16[6144,128]{1,0:T(8,128)(2,1)}, bf16[6144,128]{1,0:T(8,128)(2,1)S(1)}, u32[]{:S(2)}) copy-start(bf16[6144,128]{1,0:T(8,128)(2,1)S(1)} %collective-permute-done.mine_ref) | copy-start | bytes 4718596
  27.4 47.0 %collective-permute-start.1 = (bf16[6144,128]{1,0:T(8,128)(2,1)S(1)}, bf16[6144,128]{1,0:T(8,128)(2,1)S(1)}, u32[]{:S(2)}, u32[]{:S(2)}) collective-permute-start(bf16[6144,128]{1,0:T(8,128)(2,1)S(1)} %collective-permute-done.mine_ref), channel_id=1, source_target_pairs={{0,16},{16,0},{1,17},{17,1},{2,18},{18,2},{3,19},{19,3},{4,20},{20... | collective-permute-start | bytes 4718600 | tf_op jit(solution)/shard_map/ppermute | solution.py:190
  49.7 0.7 copy-start
  74.4 1.1 copy-start.2
  132.6 6.4 %collective-permute-start.2 = (f32[128,128]{1,0:T(8,128)}, f32[128,128]{1,0:T(8,128)S(1)}, u32[]{:S(2)}, u32[]{:S(2)}) collective-permute-start(f32[128,128]{1,0:T(8,128)} %get-tuple-element.12), channel_id=1, source_target_pairs={{0,12},{12,0},{4,8},{8,4},{1,13},{13,1},{5,9},{9,5},{2,14},{14,2},... | collective-permute-start | bytes 196616 | tf_op jit(solution)/shard_map/ppermute | solution.py:222

commit v3 on v2

--- a/solution.py
+++ b/solution.py
@@ -30,20 +30,36 @@
     return jnp.where(mask, 1.0, 0.0).astype(BF)
 
 
-def pack_kernel(gate_ref, up_ref, down_ref, out_ref):
-    width = gate_ref.shape[1]
-    span = gate_ref.shape[2]
-    out_ref[:width] = gate_ref[0]
-    out_ref[width : 2 * width] = up_ref[0]
+def whereabouts(place_ref):
+    place = place_ref[0]
+    return place // 8, place // 4, place % 4
+
+
+def pack_kernel(gate_ref, up_ref, down_ref, out_ref, sems):
+    _, width, span = gate_ref.shape
+    copies = [(gate_ref.at[0], out_ref.at[:width]), (up_ref.at[0], out_ref.at[width : 2 * width])]
     for k in range(width // span):
         at = 2 * width + k * span
-        out_ref[at : at + span] = down_ref[0, :, k * span : (k + 1) * span]
-
-
-def pick_kernel(place_ref, selected_ref, affinity_ref, first_ref, second_ref, rows_ref, mix_ref):
-    g = place_ref[2]
+        copies.append((down_ref.at[0, :, k * span : (k + 1) * span], out_ref.at[at : at + span]))
+    copies = [pltpu.make_async_copy(*c, sems.at[k]) for k, c in enumerate(copies)]
+    for copy in copies:
+        copy.start()
+    for copy in copies:
+        copy.wait()
+
+
+def pick_kernel(place_ref, selected_ref, affinity_ref, tokens_ref, rows_ref, mix_ref, tile_ref, sems):
+    g, y, x = whereabouts(place_ref)
     experts, most = selected_ref.shape
-    tok, width = first_ref.shape
+    _, tok, width = tile_ref.shape
+    copies = []
+    for c in range(2):
+        block = 4 * ((jnp.minimum, jnp.maximum)[c](y, 3 - y)) + x
+        at = pl.multiple_of(block * width, width)
+        copies.append(
+            pltpu.make_async_copy(tokens_ref.at[:, pl.ds(at, width)], tile_ref.at[c], sems.at[c])
+        )
+        copies[c].start()
     here = experts // 2
     slots = here * most
     sel = selected_ref[...].astype(F32).astype(BF)
@@ -52,9 +68,6 @@
     spread = jnp.where(own, dot(repeat, sel), 0.0).astype(BF)
     position = dot(spread, jnp.ones((most, tok), BF))
     named = one_hot(position == iota((slots, tok), 1).astype(F32))
-    for c, ref in enumerate((first_ref, second_ref)):
-        rows = jnp.where(position < 0.0, EMPTY, dot(named, ref[...])).astype(BF)
-        rows_ref[:, c] = rows.reshape(here, most, width)
     tile = one_hot(iota((most, slots), 0) == iota((most, slots), 1) % most)
     mine = iota((experts, slots), 0) == 2 * (iota((experts, slots), 1) // most) + g
 
@@ -67,6 +80,10 @@
     hit = as_row(sel) == iota((tok, slots), 0).astype(F32)
     mix_ref[0] = jnp.where(hit, as_row(high), 0.0).astype(BF)
     mix_ref[1] = jnp.where(hit, as_row(low), 0.0).astype(BF)
+    for c in range(2):
+        copies[c].wait()
+        rows = jnp.where(position < 0.0, EMPTY, dot(named, tile_ref[c])).astype(BF)
+        rows_ref[:, c] = rows.reshape(here, most, width)
 
 
 def compact_kernel(slots_ref, rows_ref):
@@ -97,7 +114,7 @@
 
 
 def ffn_kernel(place_ref, x_ref, mine_ref, other_ref, out_ref):
-    g = place_ref[2]
+    g, _, _ = whereabouts(place_ref)
     peers, rows, span = x_ref.shape
     width = peers * span
     pair = (mine_ref, other_ref)
@@ -143,31 +160,34 @@
     both = [rows_ref[:, c].reshape(here * most, width) for c in range(cores)]
     both = jnp.concatenate(both, axis=1)
     total = dot(mix_ref[0], both) + dot(mix_ref[1], both)
-    mine = place_ref[2] == 0
+    mine = whereabouts(place_ref)[0] == 0
     keep_ref[...] = jnp.where(mine, total[:, :width], total[:, width:])
-    send_ref[...] = jnp.where(mine, total[:, width:], total[:, :width])
-
-
-def whole(shape):
-    return pl.BlockSpec(shape, lambda i, place: (0,) * len(shape))
-
-
-def placed_call(kernel, place, outs, *args, specs=None):
-    specs = specs or [whole(a.shape) for a in args]
+    send_ref[...] = jnp.where(mine, total[:, width:], total[:, :width]).astype(BF)
+
+
+def local_call(kernel, outs, *args, place=None, params=(), hbm=(), scratch=()):
+    vmem = pl.BlockSpec(memory_space=pltpu.VMEM)
+    specs = [pl.BlockSpec()] * len(params) + [vmem] * len(args)
+    specs += [pl.BlockSpec(memory_space=pltpu.HBM)] * len(hbm)
+    args = [pltpu.with_memory_space_constraint(a, pltpu.VMEM) for a in args]
+    args = [*params, *args, *(pltpu.with_memory_space_constraint(a, pltpu.HBM) for a in hbm)]
+    if place is not None:
+        specs = [pl.BlockSpec(memory_space=pltpu.SMEM)] + specs
+        args = [place] + args
     return pl.pallas_call(
         kernel,
-        grid_spec=pltpu.PrefetchScalarGridSpec(
-            num_scalar_prefetch=1,
-            grid=(1,),
-            in_specs=specs,
-            out_specs=jax.tree.map(lambda o: whole(o.shape), outs),
+        in_specs=specs,
+        out_specs=jax.tree.map(
+            lambda o: pl.BlockSpec() if isinstance(o, jax.ShapeDtypeStruct) else vmem, outs
         ),
         out_shape=outs,
-    )(place, *args)
+        scratch_shapes=scratch,
+        compiler_params=pltpu.CompilerParams(vmem_limit_bytes=24 * 2**20),
+    )(*args)
 
 
 def array(shape, dtype=BF):
-    return jax.ShapeDtypeStruct(shape, dtype)
+    return pltpu.VMEM(shape, dtype)
 
 
 def per_device(tokens, selected, affinity, w_gate, w_up, w_down):
@@ -178,48 +198,46 @@
     experts, most = selected.shape
     span = width // team
     part = ep * most // 4
-    g = lax.axis_index("g")
-    y = 2 * g + lax.axis_index("yy")
-    x = lax.axis_index("x")
-    place = jnp.stack([4 * jnp.minimum(y, 3 - y) + x, 4 * jnp.maximum(y, 3 - y) + x, g])
-    place = place.astype(jnp.int32)
-    packed = pl.pallas_call(pack_kernel, out_shape=array((3 * width, span)))(
-        w_gate, w_up, w_down
+    place = lax.axis_index(TP).astype(jnp.int32).reshape(1)
+    packed = local_call(
+        pack_kernel,
+        array((3 * width, span)),
+        hbm=(w_gate, w_up, w_down),
+        scratch=[pltpu.SemaphoreType.DMA((2 + team,))],
     )
     mine = lax.ppermute(packed, ("c", "g", "yy"), TRADE)
     other = lax.ppermute(mine, "c", CORES)
-    rows, mix = placed_call(
+    rows, mix = local_call(
         pick_kernel,
-        place,
-        [array((layers, 2, most, span)), array((2, tok, layers * most))],
-        selected,
-        affinity,
-        tokens,
-        tokens,
-        specs=[
-            whole(selected.shape),
-            whole(affinity.shape),
-            pl.BlockSpec((tok, span), lambda i, place: (0, place[0])),
-            pl.BlockSpec((tok, span), lambda i, place: (0, place[1])),
+        [
+            jax.ShapeDtypeStruct((layers, 2, most, span), BF),
+            jax.ShapeDtypeStruct((2, tok, layers * most), BF),
         ],
+        place=place,
+        params=(selected, affinity),
+        hbm=(tokens,),
+        scratch=[pltpu.VMEM((2, tok, span), BF), pltpu.SemaphoreType.DMA((2,))],
     )
     arrived = lax.all_to_all(rows.reshape(ep, most, span), EP, 0, 0, tiled=True)
-    copies = pl.pallas_call(compact_kernel, out_shape=array((2, team // 2, part, span)))(arrived)
+    copies = local_call(compact_kernel, array((2, team // 2, part, span)), arrived)
     chosen = lax.all_to_all(copies.reshape(team, part, span), TEAM, 0, 0, tiled=True)
-    partial = placed_call(ffn_kernel, place, array((team, part, span)), chosen, mine, other)
+    partial = local_call(ffn_kernel, array((team, part, span)), chosen, mine, other, place=place)
     summands = lax.all_to_all(partial, TEAM, 0, 0, tiled=True)
-    result = pl.pallas_call(expand_kernel, out_shape=array((ep, most, span)))(
-        summands.reshape(2, team // 2, part, span), arrived
+    result = local_call(
+        expand_kernel,
+        array((ep, most, span)),
+        summands.reshape(2, team // 2, part, span),
+        arrived,
     )
     returned = lax.all_to_all(result, EP, 0, 0, tiled=True)
-    keep, send = placed_call(
+    keep, send = local_call(
         combine_kernel,
-        place,
-        [array((tok, span), F32), array((tok, span), F32)],
+        [array((tok, span), F32), array((tok, span))],
         mix,
         returned.reshape(layers, 2, most, span),
-    )
-    return (keep + lax.ppermute(send, ("g", "yy"), PAIR)).astype(BF)
+        place=place,
+    )
+    return (keep + lax.ppermute(send, ("g", "yy"), PAIR).astype(F32)).astype(BF)
 
 
 def solution(mesh):

time: 141 us -> 123 us (0.87)
  Pallas kernels: 18.6 us -> 5.82 us
  blocking collectives: 67.9 us -> 64.6 us
  other arithmetic: 2.06 us -> 0.62 us
    pallas_call x6, Pallas kernels: 18.6 us -> 5.82 us  [local_call(): pl.pallas_call(kernel, in_specs=specs, out_specs=jax.tree.map(lambda o: p...]
    all_to_all x1, blocking collectives: 26 us -> 24.4 us  [per_device(): returned = lax.all_to_all(result, EP, 0, 0, tiled=True)]
  transfers between devices with their start and end apart: 4 -> 4, of which waited for: 2 -> 2; matrix products, arithmetic and copies ran while one was open for 0% -> 0% of each run, Pallas kernels for 4% -> 2%
where the time goes in v3:
time: 123 us; the launch traced here: 122 us
  blocking collectives  64.6 us (53%)
  starting transfers between devices  26 us (21%)
  waiting for transfers between devices  23.5 us (19%)
  Pallas kernels  5.82 us (5%)
  local copies, waits for them, and re-layouts  1.4 us (1%)
    all_to_all x1, blocking collectives, per_device(): returned = lax.all_to_all(result, EP, 0, 0, tiled=True)  24.4 us
    all_to_all x1, blocking collectives, per_device(): lax.all_to_all(copies.reshape(team, part, span), TEAM, 0, 0, tiled=True)  21 us
    all_to_all x1, waiting for transfers between devices, per_device(): arrived = lax.all_to_all(rows.reshape(ep, most, span), EP, 0, 0, tiled=True)  20.1 us
    all_to_all x1, blocking collectives, per_device(): summands = lax.all_to_all(partial, TEAM, 0, 0, tiled=True)  19.2 us
    all_to_all x1, starting transfers between devices, per_device(): arrived = lax.all_to_all(rows.reshape(ep, most, span), EP, 0, 0, tiled=True)  15.4 us
    ppermute x1, starting transfers between devices, per_device(): mine = lax.ppermute(packed, ('c', 'g', 'yy'), TRADE)  6.02 us
    pallas_call x6, Pallas kernels, local_call(): pl.pallas_call(kernel, in_specs=specs, out_specs=jax.tree.map(lambda o: p...  5.82 us
    ppermute x1, waiting for transfers between devices, per_device(): return (keep + lax.ppermute(send, ('g', 'yy'), PAIR).astype(F32)).astype(BF)  3.37 us
  transfers between devices with their start and end apart: 4, of which 2 were waited for; matrix products, arithmetic and copies ran while one was open for 0% of the time, Pallas kernels for 2%

profile of v3, /device:TPU:1, one launch (start us, length us, event | category | flops | bytes accessed | tf_op | source)
XLA Modules:
  0.0 122.0 jit_solution(722547854075861366)
XLA Ops:
  0.0 0.0 copy-start.4
  0.0 0.0 copy-start.3
  0.0 1.4 %shard_map.66 = bf16[6144,128]{1,0:T(8,128)(2,1)S(1)} custom-call(bf16[1,2048,128]{2,1,0:T(8,128)(2,1)} %gate_ref.1, bf16[1,2048,128]{2,1,0:T(8,128)(2,1)} %up_ref.1, bf16[1,128,2048]{2,1,0:T(8,128)(2,1)} %down_ref.1), custom_call_target="tpu_custom_call" | custom-call | tf_op jit(solution)/shard_map/pallas_call | solution.py:177
  1.5 6.0 %collective-permute-start = (bf16[6144,128]{1,0:T(8,128)(2,1)S(1)}, bf16[6144,128]{1,0:T(8,128)(2,1)S(1)}, u32[]{:S(2)}, u32[]{:S(2)}) collective-permute-start(bf16[6144,128]{1,0:T(8,128)(2,1)S(1)} %shard_map.66), channel_id=1, source_target_pairs={{0,0},{4,4},{24,24},{28,28},{16,12},{12,16},{20,8},{8,20},{1,1},{5... | collective-permute-start | bytes 4718600 | tf_op jit(solution)/shard_map/ppermute | solution.py:208
  7.5 0.0 copy-done.4
  7.5 0.0 copy-done.3
  7.5 1.2 %shard_map.64 = (bf16[16,2,32,128]{3,2,1,0:T(8,128)(2,1)S(1)}, bf16[2,128,512]{2,1,0:T(8,128)(2,1)S(1)}) custom-call(s32[1]{0:T(128)} %bitcast.place_ref, s32[32,32]{1,0:T(8,128)S(1)} %copy-done.3, f32[32,32]{1,0:T(8,128)S(1)} %copy-done.4, bf16[128,2048]{1,0:T(8,128)(2,1)} %tokens_ref.1), custom_call_target="tpu_custom_call" | custom-call | tf_op jit(solution)/shard_map/pallas_call | solution.py:177
  8.8 0.0 copy-start
  8.8 0.7 copy-done
  9.5 0.0 copy-start.2
  9.5 0.7 copy-done.2
  10.2 15.4 %all-to-all-start = ((bf16[32,32,128]{2,1,0:T(8,128)(2,1)}), bf16[32,32,128]{2,1,0:T(8,128)(2,1)S(1)}, u32[]{:S(2)}, u32[]{:S(2)}) async-start(bf16[32,32,128]{2,1,0:T(8,128)(2,1)} %bitcast.8), calls=%async_computation | async-start | bytes 524288 | tf_op jit(solution)/shard_map/all_to_all | solution.py:221
  25.5 0.0 collective-permute-done.mine_ref
  25.6 2.1 %collective-permute-start.1 = (bf16[6144,128]{1,0:T(8,128)(2,1)S(1)}, bf16[6144,128]{1,0:T(8,128)(2,1)S(1)}, u32[]{:S(2)}, u32[]{:S(2)}) collective-permute-start(bf16[6144,128]{1,0:T(8,128)(2,1)S(1)} %collective-permute-done.mine_ref), channel_id=1, source_target_pairs={{0,16},{16,0},{1,17},{17,1},{2,18},{18,2},{3,19},{19,3},{4,20},{20... | collective-permute-start | bytes 4718600 | tf_op jit(solution)/shard_map/ppermute | solution.py:209
  27.7 20.1 %all-to-all-done.slots_ref = bf16[32,32,128]{2,1,0:T(8,128)(2,1)S(1)} async-done(((bf16[32,32,128]{2,1,0:T(8,128)(2,1)}), bf16[32,32,128]{2,1,0:T(8,128)(2,1)S(1)}, u32[]{:S(2)}, u32[]{:S(2)}) %all-to-all-start) | async-done | bytes 262176 | tf_op jit(solution)/shard_map/all_to_all | solution.py:221
  47.8 0.8 shard_map.65
  48.6 21.0 %all_to_all.20.x_ref = bf16[16,256,128]{2,1,0:T(8,128)(2,1)S(1)} all-to-all(bf16[16,256,128]{2,1,0:T(8,128)(2,1)S(1)} %bitcast.5), channel_id=1, replica_groups=mesh['z'=16,'c'=2,'g'=2,'yy'=2,'x'=4] {'c','yy','x'}, dimensions={0} | all-to-all | bytes 2097152 | tf_op jit(solution)/shard_map/all_to_all | solution.py:223
  69.6 0.0 collective-permute-done.1.other_ref
  69.6 1.1 shard_map.67
  70.7 19.2 %all_to_all.21 = bf16[16,256,128]{2,1,0:T(8,128)(2,1)S(1)} all-to-all(bf16[16,256,128]{2,1,0:T(8,128)(2,1)S(1)} %shard_map.67), channel_id=1, replica_groups=mesh['z'=16,'c'=2,'g'=2,'yy'=2,'x'=4] {'c','yy','x'}, dimensions={0} | all-to-all | bytes 2097152 | tf_op jit(solution)/shard_map/all_to_all | solution.py:225
  89.9 0.0 copy-start.1
  89.9 1.0 shard_map.68
  90.9 24.4 %all_to_all.22 = bf16[32,32,128]{2,1,0:T(8,128)(2,1)S(1)} all-to-all(bf16[32,32,128]{2,1,0:T(8,128)(2,1)S(1)} %shard_map.68), channel_id=1, replica_groups=mesh['z'=16,'c'=2,'g'=2,'yy'=2,'x'=4] {'z','c'}, dimensions={0} | all-to-all | bytes 524288 | tf_op jit(solution)/shard_map/all_to_all | solution.py:232
  115.3 0.0 copy-done.1
  115.3 0.2 shard_map.69
  115.5 2.5 %collective-permute-start.2 = (bf16[128,128]{1,0:T(8,128)(2,1)S(1)}, bf16[128,128]{1,0:T(8,128)(2,1)S(1)}, u32[]{:S(2)}, u32[]{:S(2)}) collective-permute-start(bf16[128,128]{1,0:T(8,128)(2,1)S(1)} %get-tuple-element.12), channel_id=1, source_target_pairs={{0,12},{12,0},{4,8},{8,4},{1,13},{13,1},{5,9},{9,5},{2,14},{14,2},... | collective-permute-start | bytes 98312 | tf_op jit(solution)/shard_map/ppermute | solution.py:240
  118.0 3.4 %collective-permute-done.2 = bf16[128,128]{1,0:T(8,128)(2,1)S(1)} collective-permute-done((bf16[128,128]{1,0:T(8,128)(2,1)S(1)}, bf16[128,128]{1,0:T(8,128)(2,1)S(1)}, u32[]{:S(2)}, u32[]{:S(2)}) %collective-permute-start.2) | collective-permute-done | bytes 32800 | tf_op jit(solution)/shard_map/ppermute | solution.py:240
  121.4 0.6 add_convert_fusion
Async XLA Ops:
  0.0 7.5 %copy-start.4 = (f32[32,32]{1,0:T(8,128)S(1)}, f32[32,32]{1,0:T(8,128)}, u32[]{:S(2)}) copy-start(f32[32,32]{1,0:T(8,128)} %affinity_ref.1) | copy-start | bytes 12292
  0.0 7.5 %copy-start.3 = (s32[32,32]{1,0:T(8,128)S(1)}, s32[32,32]{1,0:T(8,128)}, u32[]{:S(2)}) copy-start(s32[32,32]{1,0:T(8,128)} %selected_ref.1) | copy-start | bytes 12292
  1.5 24.1 %collective-permute-start = (bf16[6144,128]{1,0:T(8,128)(2,1)S(1)}, bf16[6144,128]{1,0:T(8,128)(2,1)S(1)}, u32[]{:S(2)}, u32[]{:S(2)}) collective-permute-start(bf16[6144,128]{1,0:T(8,128)(2,1)S(1)} %shard_map.66), channel_id=1, source_target_pairs={{0,0},{4,4},{24,24},{28,28},{16,12},{12,16},{20,8},{8,20},{1,1},{5... | collective-permute-start | bytes 4718600 | tf_op jit(solution)/shard_map/ppermute | solution.py:208
  8.8 0.7 copy-start
  9.5 0.7 copy-start.2
  10.2 37.6 %all-to-all-start = ((bf16[32,32,128]{2,1,0:T(8,128)(2,1)}), bf16[32,32,128]{2,1,0:T(8,128)(2,1)S(1)}, u32[]{:S(2)}, u32[]{:S(2)}) async-start(bf16[32,32,128]{2,1,0:T(8,128)(2,1)} %bitcast.8), calls=%async_computation | async-start | bytes 524288 | tf_op jit(solution)/shard_map/all_to_all | solution.py:221
  25.6 44.1 %collective-permute-start.1 = (bf16[6144,128]{1,0:T(8,128)(2,1)S(1)}, bf16[6144,128]{1,0:T(8,128)(2,1)S(1)}, u32[]{:S(2)}, u32[]{:S(2)}) collective-permute-start(bf16[6144,128]{1,0:T(8,128)(2,1)S(1)} %collective-permute-done.mine_ref), channel_id=1, source_target_pairs={{0,16},{16,0},{1,17},{17,1},{2,18},{18,2},{3,19},{19,3},{4,20},{20... | collective-permute-start | bytes 4718600 | tf_op jit(solution)/shard_map/ppermute | solution.py:209
  89.9 25.4 %copy-start.1 = (bf16[2,128,512]{2,1,0:T(8,128)(2,1)S(1)}, bf16[2,128,512]{2,1,0:T(8,128)(2,1)}, u32[]{:S(2)}) copy-start(bf16[2,128,512]{2,1,0:T(8,128)(2,1)} %copy-done) | copy-start | bytes 786436
  115.5 5.9 %collective-permute-start.2 = (bf16[128,128]{1,0:T(8,128)(2,1)S(1)}, bf16[128,128]{1,0:T(8,128)(2,1)S(1)}, u32[]{:S(2)}, u32[]{:S(2)}) collective-permute-start(bf16[128,128]{1,0:T(8,128)(2,1)S(1)} %get-tuple-element.12), channel_id=1, source_target_pairs={{0,12},{12,0},{4,8},{8,4},{1,13},{13,1},{5,9},{9,5},{2,14},{14,2},... | collective-permute-start | bytes 98312 | tf_op jit(solution)/shard_map/ppermute | solution.py:240

commit v4 on v3

--- a/solution.py
+++ b/solution.py
@@ -15,6 +15,7 @@
 LIMIT = 32.0
 TRADE = [(0, 0), (1, 1), (6, 6), (7, 7), (4, 3), (3, 4), (5, 2), (2, 5)]
 PAIR = [(0, 3), (3, 0), (1, 2), (2, 1)]
+ACROSS = [(0, 1), (1, 0), (2, 3), (3, 2), (4, 7), (7, 4), (5, 6), (6, 5)]
 CORES = [(0, 1), (1, 0)]
 
 
@@ -48,18 +49,18 @@
         copy.wait()
 
 
-def pick_kernel(place_ref, selected_ref, affinity_ref, tokens_ref, rows_ref, mix_ref, tile_ref, sems):
+def pick_kernel(place_ref, selected_ref, tokens_ref, rows_ref, tile_ref, out_ref, sems):
     g, y, x = whereabouts(place_ref)
     experts, most = selected_ref.shape
     _, tok, width = tile_ref.shape
-    copies = []
+    loads = []
     for c in range(2):
         block = 4 * ((jnp.minimum, jnp.maximum)[c](y, 3 - y)) + x
         at = pl.multiple_of(block * width, width)
-        copies.append(
+        loads.append(
             pltpu.make_async_copy(tokens_ref.at[:, pl.ds(at, width)], tile_ref.at[c], sems.at[c])
         )
-        copies[c].start()
+        loads[c].start()
     here = experts // 2
     slots = here * most
     sel = selected_ref[...].astype(F32).astype(BF)
@@ -68,6 +69,22 @@
     spread = jnp.where(own, dot(repeat, sel), 0.0).astype(BF)
     position = dot(spread, jnp.ones((most, tok), BF))
     named = one_hot(position == iota((slots, tok), 1).astype(F32))
+    stores = []
+    for c in range(2):
+        loads[c].wait()
+        rows = jnp.where(position < 0.0, EMPTY, dot(named, tile_ref[c])).astype(BF)
+        out_ref[c] = rows.reshape(here, most, width)
+        stores.append(pltpu.make_async_copy(out_ref.at[c], rows_ref.at[:, c], sems.at[2 + c]))
+        stores[c].start()
+    for store in stores:
+        store.wait()
+
+
+def mix_kernel(place_ref, selected_ref, affinity_ref, mix_ref):
+    g, _, _ = whereabouts(place_ref)
+    experts, most = selected_ref.shape
+    _, tok, slots = mix_ref.shape
+    sel = selected_ref[...].astype(F32).astype(BF)
     tile = one_hot(iota((most, slots), 0) == iota((most, slots), 1) % most)
     mine = iota((experts, slots), 0) == 2 * (iota((experts, slots), 1) // most) + g
 
@@ -80,17 +97,13 @@
     hit = as_row(sel) == iota((tok, slots), 0).astype(F32)
     mix_ref[0] = jnp.where(hit, as_row(high), 0.0).astype(BF)
     mix_ref[1] = jnp.where(hit, as_row(low), 0.0).astype(BF)
-    for c in range(2):
-        copies[c].wait()
-        rows = jnp.where(position < 0.0, EMPTY, dot(named, tile_ref[c])).astype(BF)
-        rows_ref[:, c] = rows.reshape(here, most, width)
 
 
 def compact_kernel(slots_ref, rows_ref):
     blocks, most, width = slots_ref.shape
-    cores, peers, part, _ = rows_ref.shape
+    cores, lines, peers, part, _ = rows_ref.shape
     slots = blocks * most
-    count = cores * part
+    count = 2 * cores * part
     data = slots_ref[...].reshape(slots, width)
     live = one_hot(data.astype(F32) < LIMIT)
     first = one_hot(iota((8, width), 1) == 0)
@@ -103,8 +116,10 @@
     take = one_hot(rank == iota((count, slots), 0).astype(F32))
     rows = dot(take, data).astype(BF)
     for c in range(cores):
-        for k in range(peers):
-            rows_ref[c, k] = rows[c * part : (c + 1) * part]
+        for k in range(lines):
+            for x in range(peers):
+                at = (2 * (x % 2) + c) * part
+                rows_ref[c, k, x] = rows[at : at + part]
 
 
 def seat(block, g):
@@ -113,19 +128,19 @@
     return (y // 2) * 8 + 4 * (yy + g - 2 * yy * g) + block % 4
 
 
-def ffn_kernel(place_ref, x_ref, mine_ref, other_ref, out_ref):
+def ffn_kernel(place_ref, x_ref, *refs):
+    *weights, out_ref = refs
     g, _, _ = whereabouts(place_ref)
-    peers, rows, span = x_ref.shape
+    peers, _, span = x_ref.shape
     width = peers * span
-    pair = (mine_ref, other_ref)
     x = jnp.concatenate([x_ref[seat(k, g)] for k in range(peers)], axis=1)
-    gate = dot(x, jnp.concatenate([w[:width] for w in pair], axis=1))
-    up = dot(x, jnp.concatenate([w[width : 2 * width] for w in pair], axis=1))
+    gate = dot(x, jnp.concatenate([w[:width] for w in weights], axis=1))
+    up = dot(x, jnp.concatenate([w[width : 2 * width] for w in weights], axis=1))
     hidden = (gate / (1.0 + jnp.exp(-gate)) * up).astype(BF)
     for k in range(0, peers, 2):
         at = 2 * width + k * span
         tiles = [
-            jnp.concatenate([w[at + j * span : at + (j + 1) * span] for w in pair], axis=0)
+            jnp.concatenate([w[at + j * span : at + (j + 1) * span] for w in weights], axis=0)
             for j in range(2)
         ]
         partial = dot(hidden, jnp.concatenate(tiles, axis=1)).astype(BF)
@@ -134,15 +149,16 @@
 
 
 def expand_kernel(parts_ref, slots_ref, out_ref):
-    cores, peers, part, width = parts_ref.shape
+    cores, lines, _, part, width = parts_ref.shape
     blocks, most, _ = slots_ref.shape
     slots = blocks * most
-    halves = []
-    for c in range(cores):
-        total = parts_ref[c, 0].astype(F32)
-        for k in range(1, peers):
-            total = total + parts_ref[c, k].astype(F32)
-        halves.append(total.astype(BF))
+    quarters = []
+    for x in range(2):
+        for c in range(cores):
+            total = parts_ref[c, 0, x].astype(F32)
+            for k in range(1, 2 * lines):
+                total = total + parts_ref[c, k % lines, x + 2 * (k // lines)].astype(F32)
+            quarters.append(total.astype(BF))
     live = one_hot(slots_ref[...].reshape(slots, width).astype(F32) < LIMIT)
     in_block = one_hot(iota((blocks, slots), 0) == iota((blocks, slots), 1) // most)
     before = one_hot(iota((slots, blocks), 1) < iota((slots, blocks), 0) // most)
@@ -150,8 +166,8 @@
     rank = dot(before, counts) + (iota((slots, width), 0) % most).astype(F32)
     rank = jnp.where(live > 0.5, rank, -1.0)
     lanes = iota((slots, width), 1).astype(F32)
-    put = [one_hot(rank - k == lanes) for k in range(0, cores * part, width)]
-    rows = dot(jnp.concatenate(put, axis=1), jnp.concatenate(halves, axis=0)).astype(BF)
+    put = [one_hot(rank - k == lanes) for k in range(0, 2 * cores * part, width)]
+    rows = dot(jnp.concatenate(put, axis=1), jnp.concatenate(quarters, axis=0)).astype(BF)
     out_ref[...] = rows.reshape(blocks, most, width)
 
 
@@ -177,9 +193,7 @@
     return pl.pallas_call(
         kernel,
         in_specs=specs,
-        out_specs=jax.tree.map(
-            lambda o: pl.BlockSpec() if isinstance(o, jax.ShapeDtypeStruct) else vmem, outs
-        ),
+        out_specs=jax.tree.map(lambda o: pl.BlockSpec(memory_space=o.memory_space), outs),
         out_shape=outs,
         scratch_shapes=scratch,
         compiler_params=pltpu.CompilerParams(vmem_limit_bytes=24 * 2**20),
@@ -195,9 +209,11 @@
     layers = lax.axis_size("z")
     team = lax.axis_size(TEAM)
     tok, width = tokens.shape
-    experts, most = selected.shape
+    _, most = selected.shape
     span = width // team
-    part = ep * most // 4
+    part = ep * most // 8
+    lines = lax.axis_size("yy")
+    peers = lax.axis_size("x")
     place = lax.axis_index(TP).astype(jnp.int32).reshape(1)
     packed = local_call(
         pack_kernel,
@@ -206,27 +222,45 @@
         scratch=[pltpu.SemaphoreType.DMA((2 + team,))],
     )
     mine = lax.ppermute(packed, ("c", "g", "yy"), TRADE)
+    rows = local_call(
+        pick_kernel,
+        pltpu.HBM((layers, 2, most, span), BF),
+        place=place,
+        params=(selected,),
+        hbm=(tokens,),
+        scratch=[
+            pltpu.VMEM((2, tok, span), BF),
+            pltpu.VMEM((2, layers, most, span), BF),
+            pltpu.SemaphoreType.DMA((4,)),
+        ],
+    )
+    arrived = lax.all_to_all(rows.reshape(ep, most, span), EP, 0, 0, tiled=True)
+    mix = local_call(
+        mix_kernel,
+        array((2, tok, layers * most)),
+        place=place,
+        params=(selected, affinity),
+    )
+    third = lax.ppermute(mine, ("c", "x"), ACROSS)
     other = lax.ppermute(mine, "c", CORES)
-    rows, mix = local_call(
-        pick_kernel,
-        [
-            jax.ShapeDtypeStruct((layers, 2, most, span), BF),
-            jax.ShapeDtypeStruct((2, tok, layers * most), BF),
-        ],
-        place=place,
-        params=(selected, affinity),
-        hbm=(tokens,),
-        scratch=[pltpu.VMEM((2, tok, span), BF), pltpu.SemaphoreType.DMA((2,))],
-    )
-    arrived = lax.all_to_all(rows.reshape(ep, most, span), EP, 0, 0, tiled=True)
-    copies = local_call(compact_kernel, array((2, team // 2, part, span)), arrived)
+    copies = local_call(compact_kernel, array((2, lines, peers, part, span)), arrived)
     chosen = lax.all_to_all(copies.reshape(team, part, span), TEAM, 0, 0, tiled=True)
-    partial = local_call(ffn_kernel, array((team, part, span)), chosen, mine, other, place=place)
+    fourth = lax.ppermute(third, "c", CORES)
+    partial = local_call(
+        ffn_kernel,
+        array((team, part, span)),
+        chosen,
+        mine,
+        other,
+        third,
+        fourth,
+        place=place,
+    )
     summands = lax.all_to_all(partial, TEAM, 0, 0, tiled=True)
     result = local_call(
         expand_kernel,
         array((ep, most, span)),
-        summands.reshape(2, team // 2, part, span),
+        summands.reshape(2, lines, peers, part, span),
         arrived,
     )
     returned = lax.all_to_all(result, EP, 0, 0, tiled=True)
@@ -250,6 +284,7 @@
         P(EP, None, TP),
         P(EP, TP, None),
     )
+
     return jax.shard_map(
         per_device, mesh=torus, in_specs=in_specs, out_specs=P(EP, TP), check_vma=False
     )

time: 123 us -> 158 us (1.28)
  waiting for transfers between devices: 23.5 us -> 56.8 us
  Pallas kernels: 5.82 us -> 9.25 us
  starting transfers between devices: 26 us -> 23.2 us
  blocking collectives: 64.6 us -> 66.6 us
    ppermute x1, waiting for transfers between devices: 0.03 us -> 18.1 us  [per_device(): mine = lax.ppermute(packed, ('c', 'g', 'yy'), TRADE)]
    ppermute x0 -> x2, waiting for transfers between devices: none -> 16 us  [the longest x1 16 us: per_device(): third = lax.ppermute(mine, ('c', 'x'), ACROSS)]
    all_to_all x1, blocking collectives: 24.4 us -> 38 us  [per_device(): arrived = lax.all_to_all(rows.reshape(ep, most, span), EP, 0, 0, tiled=True)]
    all_to_all x1, starting transfers between devices: 15.4 us -> 3.66 us  [per_device(): returned = lax.all_to_all(result, EP, 0, 0, tiled=True)]
    ppermute x0 -> x2, starting transfers between devices: none -> 6.29 us  [the longest x1 4.38 us: per_device(): third = lax.ppermute(mine, ('c', 'x'), ACROSS)]
    all_to_all x1, blocking collectives: 21 us -> 15.1 us  [per_device(): lax.all_to_all(copies.reshape(team, part, span), TEAM, 0, 0, tiled=True)]
    all_to_all x1, blocking collectives: 19.2 us -> 13.5 us  [per_device(): summands = lax.all_to_all(partial, TEAM, 0, 0, tiled=True)]
    pallas_call x6 -> x7, Pallas kernels: 5.82 us -> 9.25 us  [local_call(): pl.pallas_call(kernel, in_specs=specs, out_specs=jax.tree.map(lambda o: p...]
  transfers between devices with their start and end apart: 4 -> 6, of which waited for: 2 -> 4; matrix products, arithmetic and copies ran while one was open for 0% -> 0% of each run, Pallas kernels for 2% -> 2%
where the time goes in v4:
time: 158 us; the launch traced here: 157 us
  blocking collectives  66.6 us (42%)
  waiting for transfers between devices  56.8 us (36%)
  starting transfers between devices  23.2 us (15%)
  Pallas kernels  9.25 us (6%)
    all_to_all x1, blocking collectives, per_device(): arrived = lax.all_to_all(rows.reshape(ep, most, span), EP, 0, 0, tiled=True)  38 us
    all_to_all x1, waiting for transfers between devices, per_device(): returned = lax.all_to_all(result, EP, 0, 0, tiled=True)  21.4 us
    ppermute x1, waiting for transfers between devices, per_device(): mine = lax.ppermute(packed, ('c', 'g', 'yy'), TRADE)  18.1 us
    ppermute x1, waiting for transfers between devices, per_device(): third = lax.ppermute(mine, ('c', 'x'), ACROSS)  16 us
    all_to_all x1, blocking collectives, per_device(): lax.all_to_all(copies.reshape(team, part, span), TEAM, 0, 0, tiled=True)  15.1 us
    all_to_all x1, blocking collectives, per_device(): summands = lax.all_to_all(partial, TEAM, 0, 0, tiled=True)  13.5 us
    pallas_call x7, Pallas kernels, local_call(): pl.pallas_call(kernel, in_specs=specs, out_specs=jax.tree.map(lambda o: p...  9.25 us
    ppermute x1, starting transfers between devices, per_device(): mine = lax.ppermute(packed, ('c', 'g', 'yy'), TRADE)  6.02 us
  transfers between devices with their start and end apart: 6, of which 4 were waited for; matrix products, arithmetic and copies ran while one was open for 0% of the time, Pallas kernels for 2%

profile of v4, /device:TPU:1, one launch (start us, length us, event | category | flops | bytes accessed | tf_op | source)
XLA Modules:
  0.0 156.6 jit_solution(11689910784451824911)
XLA Ops:
  0.0 0.0 copy-start
  0.0 1.4 shard_map.67
  1.4 6.0 %collective-permute-start = (bf16[6144,128]{1,0:T(8,128)(2,1)S(1)}, bf16[6144,128]{1,0:T(8,128)(2,1)S(1)}, u32[]{:S(2)}, u32[]{:S(2)}) collective-permute-start(bf16[6144,128]{1,0:T(8,128)(2,1)S(1)} %shard_map.67), channel_id=1, source_target_pairs={{0,0},{4,4},{24,24},{28,28},{16,12},{12,16},{20,8},{8,20},{1,1},{5... | collective-permute-start | bytes 4718600 | tf_op jit(solution)/shard_map/ppermute | solution.py:224
  7.5 18.1 %collective-permute-done.refs_0_ = bf16[6144,128]{1,0:T(8,128)(2,1)S(1)} collective-permute-done((bf16[6144,128]{1,0:T(8,128)(2,1)S(1)}, bf16[6144,128]{1,0:T(8,128)(2,1)S(1)}, u32[]{:S(2)}, u32[]{:S(2)}) %collective-permute-start) | collective-permute-done | bytes 1572896 | tf_op jit(solution)/shard_map/ppermute | solution.py:224
  25.5 4.4 %collective-permute-start.2 = (bf16[6144,128]{1,0:T(8,128)(2,1)S(1)}, bf16[6144,128]{1,0:T(8,128)(2,1)S(1)}, u32[]{:S(2)}, u32[]{:S(2)}) collective-permute-start(bf16[6144,128]{1,0:T(8,128)(2,1)S(1)} %collective-permute-done.refs_0_), channel_id=1, source_target_pairs={{0,1},{1,0},{2,3},{3,2},{16,19},{19,16},{17,18},{18,17},{4,5},{5,4... | collective-permute-start | bytes 4718600 | tf_op jit(solution)/shard_map/ppermute | solution.py:244
  29.9 1.9 %collective-permute-start.1 = (bf16[6144,128]{1,0:T(8,128)(2,1)S(1)}, bf16[6144,128]{1,0:T(8,128)(2,1)}, u32[]{:S(2)}, u32[]{:S(2)}) collective-permute-start(bf16[6144,128]{1,0:T(8,128)(2,1)S(1)} %collective-permute-done.refs_0_), channel_id=1, source_target_pairs={{0,16},{16,0},{1,17},{17,1},{2,18},{18,2},{3,19},{19,3},{4,20},{20... | collective-permute-start | bytes 4718600 | tf_op jit(solution)/shard_map/ppermute | solution.py:245
  31.9 16.0 %collective-permute-done.2.refs_2_ = bf16[6144,128]{1,0:T(8,128)(2,1)S(1)} collective-permute-done((bf16[6144,128]{1,0:T(8,128)(2,1)S(1)}, bf16[6144,128]{1,0:T(8,128)(2,1)S(1)}, u32[]{:S(2)}, u32[]{:S(2)}) %collective-permute-start.2) | collective-permute-done | bytes 1572896 | tf_op jit(solution)/shard_map/ppermute | solution.py:244
  47.9 1.9 %collective-permute-start.3 = (bf16[6144,128]{1,0:T(8,128)(2,1)S(1)}, bf16[6144,128]{1,0:T(8,128)(2,1)}, u32[]{:S(2)}, u32[]{:S(2)}) collective-permute-start(bf16[6144,128]{1,0:T(8,128)(2,1)S(1)} %collective-permute-done.2.refs_2_), channel_id=1, source_target_pairs={{0,16},{16,0},{1,17},{17,1},{2,18},{18,2},{3,19},{19,3},{4,20},{20... | collective-permute-start | bytes 4718600 | tf_op jit(solution)/shard_map/ppermute | solution.py:248
  49.8 0.0 copy-done
  49.8 1.9 %shard_map.65 = bf16[16,2,32,128]{3,2,1,0:T(8,128)(2,1)} custom-call(s32[1]{0:T(128)} %bitcast.place_ref, s32[32,32]{1,0:T(8,128)S(1)} %copy-done, bf16[128,2048]{1,0:T(8,128)(2,1)} %tokens_ref.1), custom_call_target="tpu_custom_call" | custom-call | tf_op jit(solution)/shard_map/pallas_call | solution.py:193
  51.7 38.0 %all_to_all.20.slots_ref = bf16[32,32,128]{2,1,0:T(8,128)(2,1)S(1)} all-to-all(bf16[32,32,128]{2,1,0:T(8,128)(2,1)} %bitcast.8), channel_id=1, replica_groups=mesh['z'=16,'c'=2,'g'=2,'yy'=2,'x'=4] {'z','c'}, dimensions={0} | all-to-all | bytes 524288 | tf_op jit(solution)/shard_map/all_to_all | solution.py:237
  89.7 0.8 shard_map.66
  90.6 15.1 %all_to_all.21.x_ref = bf16[16,128,128]{2,1,0:T(8,128)(2,1)S(1)} all-to-all(bf16[16,128,128]{2,1,0:T(8,128)(2,1)S(1)} %bitcast.6), channel_id=1, replica_groups=mesh['z'=16,'c'=2,'g'=2,'yy'=2,'x'=4] {'c','yy','x'}, dimensions={0} | all-to-all | bytes 1048576 | tf_op jit(solution)/shard_map/all_to_all | solution.py:247
  105.7 0.0 collective-permute-done.1.refs_1_
  105.7 0.0 collective-permute-done.3.refs_3_
  105.7 3.0 %shard_map.68 = bf16[16,128,128]{2,1,0:T(8,128)(2,1)S(1)} custom-call(s32[1]{0:T(128)} %bitcast.place_ref, bf16[16,128,128]{2,1,0:T(8,128)(2,1)S(1)} %all_to_all.21.x_ref, bf16[6144,128]{1,0:T(8,128)(2,1)S(1)} %collective-permute-done.refs_0_, bf16[6144,128]{1,0:T(8,128)(2,1)} %collective-permute-done.1.refs_1_, ...), custom_call_target="tpu_custom_call" | custom-call | tf_op jit(solution)/shard_map/pallas_call | solution.py:193
  108.7 0.0 copy-start.1
  108.7 13.5 %all_to_all.22 = bf16[16,128,128]{2,1,0:T(8,128)(2,1)S(1)} all-to-all(bf16[16,128,128]{2,1,0:T(8,128)(2,1)S(1)} %shard_map.68), channel_id=1, replica_groups=mesh['z'=16,'c'=2,'g'=2,'yy'=2,'x'=4] {'c','yy','x'}, dimensions={0} | all-to-all | bytes 1048576 | tf_op jit(solution)/shard_map/all_to_all | solution.py:259
  122.2 1.7 %shard_map.69 = bf16[32,32,128]{2,1,0:T(8,128)(2,1)} custom-call(bf16[2,2,4,128,128]{4,3,2,1,0:T(8,128)(2,1)S(1)} %bitcast.5, bf16[32,32,128]{2,1,0:T(8,128)(2,1)S(1)} %all_to_all.20.slots_ref), custom_call_target="tpu_custom_call" | custom-call | tf_op jit(solution)/shard_map/pallas_call | solution.py:193
  123.9 3.7 %all-to-all-start.3 = ((bf16[32,32,128]{2,1,0:T(8,128)(2,1)}), bf16[32,32,128]{2,1,0:T(8,128)(2,1)S(1)}, u32[]{:S(2)}, u32[]{:S(2)}) async-start(bf16[32,32,128]{2,1,0:T(8,128)(2,1)} %shard_map.69), calls=%async_computation.3 | async-start | bytes 524288 | tf_op jit(solution)/shard_map/all_to_all | solution.py:266
  127.5 0.0 copy-done.1
  127.5 0.2 shard_map.64.mix_ref
  127.8 21.4 %all-to-all-done.3 = bf16[32,32,128]{2,1,0:T(8,128)(2,1)S(1)} async-done(((bf16[32,32,128]{2,1,0:T(8,128)(2,1)}), bf16[32,32,128]{2,1,0:T(8,128)(2,1)S(1)}, u32[]{:S(2)}, u32[]{:S(2)}) %all-to-all-start.3) | async-done | bytes 262176 | tf_op jit(solution)/shard_map/all_to_all | solution.py:266
  149.1 0.2 shard_map.70
  149.4 5.3 %collective-permute-start.4 = (bf16[128,128]{1,0:T(8,128)(2,1)S(1)}, bf16[128,128]{1,0:T(8,128)(2,1)S(1)}, u32[]{:S(2)}, u32[]{:S(2)}) collective-permute-start(bf16[128,128]{1,0:T(8,128)(2,1)S(1)} %get-tuple-element.8), channel_id=1, source_target_pairs={{0,12},{12,0},{4,8},{8,4},{1,13},{13,1},{5,9},{9,5},{2,14},{14,2},... | collective-permute-start | bytes 98312 | tf_op jit(solution)/shard_map/ppermute | solution.py:274
  154.7 1.3 collective-permute-done.4
  156.0 0.6 add_convert_fusion
Async XLA Ops:
  0.0 49.8 %copy-start = (s32[32,32]{1,0:T(8,128)S(1)}, s32[32,32]{1,0:T(8,128)}, u32[]{:S(2)}) copy-start(s32[32,32]{1,0:T(8,128)} %selected_ref.3) | copy-start | bytes 12292
  1.4 24.1 %collective-permute-start = (bf16[6144,128]{1,0:T(8,128)(2,1)S(1)}, bf16[6144,128]{1,0:T(8,128)(2,1)S(1)}, u32[]{:S(2)}, u32[]{:S(2)}) collective-permute-start(bf16[6144,128]{1,0:T(8,128)(2,1)S(1)} %shard_map.67), channel_id=1, source_target_pairs={{0,0},{4,4},{24,24},{28,28},{16,12},{12,16},{20,8},{8,20},{1,1},{5... | collective-permute-start | bytes 4718600 | tf_op jit(solution)/shard_map/ppermute | solution.py:224
  25.5 22.4 %collective-permute-start.2 = (bf16[6144,128]{1,0:T(8,128)(2,1)S(1)}, bf16[6144,128]{1,0:T(8,128)(2,1)S(1)}, u32[]{:S(2)}, u32[]{:S(2)}) collective-permute-start(bf16[6144,128]{1,0:T(8,128)(2,1)S(1)} %collective-permute-done.refs_0_), channel_id=1, source_target_pairs={{0,1},{1,0},{2,3},{3,2},{16,19},{19,16},{17,18},{18,17},{4,5},{5,4... | collective-permute-start | bytes 4718600 | tf_op jit(solution)/shard_map/ppermute | solution.py:244
  29.9 75.7 %collective-permute-start.1 = (bf16[6144,128]{1,0:T(8,128)(2,1)S(1)}, bf16[6144,128]{1,0:T(8,128)(2,1)}, u32[]{:S(2)}, u32[]{:S(2)}) collective-permute-start(bf16[6144,128]{1,0:T(8,128)(2,1)S(1)} %collective-permute-done.refs_0_), channel_id=1, source_target_pairs={{0,16},{16,0},{1,17},{17,1},{2,18},{18,2},{3,19},{19,3},{4,20},{20... | collective-permute-start | bytes 4718600 | tf_op jit(solution)/shard_map/ppermute | solution.py:245
  47.9 57.8 %collective-permute-start.3 = (bf16[6144,128]{1,0:T(8,128)(2,1)S(1)}, bf16[6144,128]{1,0:T(8,128)(2,1)}, u32[]{:S(2)}, u32[]{:S(2)}) collective-permute-start(bf16[6144,128]{1,0:T(8,128)(2,1)S(1)} %collective-permute-done.2.refs_2_), channel_id=1, source_target_pairs={{0,16},{16,0},{1,17},{17,1},{2,18},{18,2},{3,19},{19,3},{4,20},{20... | collective-permute-start | bytes 4718600 | tf_op jit(solution)/shard_map/ppermute | solution.py:248
  108.7 18.8 %copy-start.1 = (f32[32,32]{1,0:T(8,128)S(1)}, f32[32,32]{1,0:T(8,128)}, u32[]{:S(2)}) copy-start(f32[32,32]{1,0:T(8,128)} %affinity_ref.1) | copy-start | bytes 12292
  123.9 25.3 %all-to-all-start.3 = ((bf16[32,32,128]{2,1,0:T(8,128)(2,1)}), bf16[32,32,128]{2,1,0:T(8,128)(2,1)S(1)}, u32[]{:S(2)}, u32[]{:S(2)}) async-start(bf16[32,32,128]{2,1,0:T(8,128)(2,1)} %shard_map.69), calls=%async_computation.3 | async-start | bytes 524288 | tf_op jit(solution)/shard_map/all_to_all | solution.py:266
  149.4 6.6 %collective-permute-start.4 = (bf16[128,128]{1,0:T(8,128)(2,1)S(1)}, bf16[128,128]{1,0:T(8,128)(2,1)S(1)}, u32[]{:S(2)}, u32[]{:S(2)}) collective-permute-start(bf16[128,128]{1,0:T(8,128)(2,1)S(1)} %get-tuple-element.8), channel_id=1, source_target_pairs={{0,12},{12,0},{4,8},{8,4},{1,13},{13,1},{5,9},{9,5},{2,14},{14,2},... | collective-permute-start | bytes 98312 | tf_op jit(solution)/shard_map/ppermute | solution.py:274

commit v5 on v4

--- a/solution.py
+++ b/solution.py
@@ -15,7 +15,7 @@
 LIMIT = 32.0
 TRADE = [(0, 0), (1, 1), (6, 6), (7, 7), (4, 3), (3, 4), (5, 2), (2, 5)]
 PAIR = [(0, 3), (3, 0), (1, 2), (2, 1)]
-ACROSS = [(0, 1), (1, 0), (2, 3), (3, 2), (4, 7), (7, 4), (5, 6), (6, 5)]
+ACROSS = [(k, k ^ 4) for k in range(8)] + [(k, k ^ 1) for k in range(8, 16)]
 CORES = [(0, 1), (1, 0)]
 
 
@@ -118,7 +118,7 @@
     for c in range(cores):
         for k in range(lines):
             for x in range(peers):
-                at = (2 * (x % 2) + c) * part
+                at = (2 * ((k + x) % 2) + c) * part
                 rows_ref[c, k, x] = rows[at : at + part]
 
 
@@ -149,15 +149,16 @@
 
 
 def expand_kernel(parts_ref, slots_ref, out_ref):
-    cores, lines, _, part, width = parts_ref.shape
+    cores, lines, peers, part, width = parts_ref.shape
     blocks, most, _ = slots_ref.shape
     slots = blocks * most
     quarters = []
-    for x in range(2):
+    for half in range(2):
         for c in range(cores):
-            total = parts_ref[c, 0, x].astype(F32)
-            for k in range(1, 2 * lines):
-                total = total + parts_ref[c, k % lines, x + 2 * (k // lines)].astype(F32)
+            total = jnp.zeros((part, width), F32)
+            for k in range(lines):
+                for x in range((half + k) % 2, peers, 2):
+                    total = total + parts_ref[c, k, x].astype(F32)
             quarters.append(total.astype(BF))
     live = one_hot(slots_ref[...].reshape(slots, width).astype(F32) < LIMIT)
     in_block = one_hot(iota((blocks, slots), 0) == iota((blocks, slots), 1) // most)
@@ -241,7 +242,7 @@
         place=place,
         params=(selected, affinity),
     )
-    third = lax.ppermute(mine, ("c", "x"), ACROSS)
+    third = lax.ppermute(mine, ("c", "yy", "x"), ACROSS)
     other = lax.ppermute(mine, "c", CORES)
     copies = local_call(compact_kernel, array((2, lines, peers, part, span)), arrived)
     chosen = lax.all_to_all(copies.reshape(team, part, span), TEAM, 0, 0, tiled=True)

time: 158 us -> 158 us (level)
  no operation moved by 1% of the time
where the time goes in v5:
time: 158 us; the launch traced here: 157 us
  blocking collectives  66.9 us (42%)
  waiting for transfers between devices  56.9 us (36%)
  starting transfers between devices  22.9 us (14%)
  Pallas kernels  9.24 us (6%)
    all_to_all x1, blocking collectives, per_device(): arrived = lax.all_to_all(rows.reshape(ep, most, span), EP, 0, 0, tiled=True)  38 us
    all_to_all x1, waiting for transfers between devices, per_device(): returned = lax.all_to_all(result, EP, 0, 0, tiled=True)  21.4 us
    ppermute x1, waiting for transfers between devices, per_device(): mine = lax.ppermute(packed, ('c', 'g', 'yy'), TRADE)  18.1 us
    ppermute x1, waiting for transfers between devices, per_device(): third = lax.ppermute(mine, ('c', 'yy', 'x'), ACROSS)  16.1 us
    all_to_all x1, blocking collectives, per_device(): lax.all_to_all(copies.reshape(team, part, span), TEAM, 0, 0, tiled=True)  15.3 us
    all_to_all x1, blocking collectives, per_device(): summands = lax.all_to_all(partial, TEAM, 0, 0, tiled=True)  13.5 us
    pallas_call x7, Pallas kernels, local_call(): pl.pallas_call(kernel, in_specs=specs, out_specs=jax.tree.map(lambda o: p...  9.24 us
    ppermute x1, starting transfers between devices, per_device(): return (keep + lax.ppermute(send, ('g', 'yy'), PAIR).astype(F32)).astype(BF)  6.29 us
  transfers between devices with their start and end apart: 6, of which 4 were waited for; matrix products, arithmetic and copies ran while one was open for 0% of the time, Pallas kernels for 2%

profile of v5, /device:TPU:1, one launch (start us, length us, event | category | flops | bytes accessed | tf_op | source)
XLA Modules:
  0.0 156.6 jit_solution(17875657302725751974)
XLA Ops:
  0.0 0.0 copy-start
  0.0 1.4 shard_map.67
  1.4 6.0 %collective-permute-start = (bf16[6144,128]{1,0:T(8,128)(2,1)S(1)}, bf16[6144,128]{1,0:T(8,128)(2,1)S(1)}, u32[]{:S(2)}, u32[]{:S(2)}) collective-permute-start(bf16[6144,128]{1,0:T(8,128)(2,1)S(1)} %shard_map.67), channel_id=1, source_target_pairs={{0,0},{4,4},{24,24},{28,28},{16,12},{12,16},{20,8},{8,20},{1,1},{5... | collective-permute-start | bytes 4718600 | tf_op jit(solution)/shard_map/ppermute | solution.py:225
  7.5 18.1 %collective-permute-done.refs_0_ = bf16[6144,128]{1,0:T(8,128)(2,1)S(1)} collective-permute-done((bf16[6144,128]{1,0:T(8,128)(2,1)S(1)}, bf16[6144,128]{1,0:T(8,128)(2,1)S(1)}, u32[]{:S(2)}, u32[]{:S(2)}) %collective-permute-start) | collective-permute-done | bytes 1572896 | tf_op jit(solution)/shard_map/ppermute | solution.py:225
  25.5 3.1 %collective-permute-start.2 = (bf16[6144,128]{1,0:T(8,128)(2,1)S(1)}, bf16[6144,128]{1,0:T(8,128)(2,1)S(1)}, u32[]{:S(2)}, u32[]{:S(2)}) collective-permute-start(bf16[6144,128]{1,0:T(8,128)(2,1)S(1)} %collective-permute-done.refs_0_), channel_id=1, source_target_pairs={{0,4},{1,5},{2,6},{3,7},{4,0},{5,1},{6,2},{7,3},{16,17},{17,16},{1... | collective-permute-start | bytes 4718600 | tf_op jit(solution)/shard_map/ppermute | solution.py:245
  28.7 1.9 %collective-permute-start.1 = (bf16[6144,128]{1,0:T(8,128)(2,1)S(1)}, bf16[6144,128]{1,0:T(8,128)(2,1)}, u32[]{:S(2)}, u32[]{:S(2)}) collective-permute-start(bf16[6144,128]{1,0:T(8,128)(2,1)S(1)} %collective-permute-done.refs_0_), channel_id=1, source_target_pairs={{0,16},{16,0},{1,17},{17,1},{2,18},{18,2},{3,19},{19,3},{4,20},{20... | collective-permute-start | bytes 4718600 | tf_op jit(solution)/shard_map/ppermute | solution.py:246
  30.6 16.1 %collective-permute-done.2.refs_2_ = bf16[6144,128]{1,0:T(8,128)(2,1)S(1)} collective-permute-done((bf16[6144,128]{1,0:T(8,128)(2,1)S(1)}, bf16[6144,128]{1,0:T(8,128)(2,1)S(1)}, u32[]{:S(2)}, u32[]{:S(2)}) %collective-permute-start.2) | collective-permute-done | bytes 1572896 | tf_op jit(solution)/shard_map/ppermute | solution.py:245
  46.7 1.9 %collective-permute-start.3 = (bf16[6144,128]{1,0:T(8,128)(2,1)S(1)}, bf16[6144,128]{1,0:T(8,128)(2,1)}, u32[]{:S(2)}, u32[]{:S(2)}) collective-permute-start(bf16[6144,128]{1,0:T(8,128)(2,1)S(1)} %collective-permute-done.2.refs_2_), channel_id=1, source_target_pairs={{0,16},{16,0},{1,17},{17,1},{2,18},{18,2},{3,19},{19,3},{4,20},{20... | collective-permute-start | bytes 4718600 | tf_op jit(solution)/shard_map/ppermute | solution.py:249
  48.6 0.0 copy-done
  48.6 1.9 %shard_map.65 = bf16[16,2,32,128]{3,2,1,0:T(8,128)(2,1)} custom-call(s32[1]{0:T(128)} %bitcast.place_ref, s32[32,32]{1,0:T(8,128)S(1)} %copy-done, bf16[128,2048]{1,0:T(8,128)(2,1)} %tokens_ref.1), custom_call_target="tpu_custom_call" | custom-call | tf_op jit(solution)/shard_map/pallas_call | solution.py:194
  50.5 38.0 %all_to_all.20.slots_ref = bf16[32,32,128]{2,1,0:T(8,128)(2,1)S(1)} all-to-all(bf16[32,32,128]{2,1,0:T(8,128)(2,1)} %bitcast.8), channel_id=1, replica_groups=mesh['z'=16,'c'=2,'g'=2,'yy'=2,'x'=4] {'z','c'}, dimensions={0} | all-to-all | bytes 524288 | tf_op jit(solution)/shard_map/all_to_all | solution.py:238
  88.5 0.8 shard_map.66
  89.4 15.3 %all_to_all.21.x_ref = bf16[16,128,128]{2,1,0:T(8,128)(2,1)S(1)} all-to-all(bf16[16,128,128]{2,1,0:T(8,128)(2,1)S(1)} %bitcast.6), channel_id=1, replica_groups=mesh['z'=16,'c'=2,'g'=2,'yy'=2,'x'=4] {'c','yy','x'}, dimensions={0} | all-to-all | bytes 1048576 | tf_op jit(solution)/shard_map/all_to_all | solution.py:248
  104.7 0.0 collective-permute-done.1.refs_1_
  104.7 0.0 collective-permute-done.3.refs_3_
  104.7 3.0 %shard_map.68 = bf16[16,128,128]{2,1,0:T(8,128)(2,1)S(1)} custom-call(s32[1]{0:T(128)} %bitcast.place_ref, bf16[16,128,128]{2,1,0:T(8,128)(2,1)S(1)} %all_to_all.21.x_ref, bf16[6144,128]{1,0:T(8,128)(2,1)S(1)} %collective-permute-done.refs_0_, bf16[6144,128]{1,0:T(8,128)(2,1)} %collective-permute-done.1.refs_1_, ...), custom_call_target="tpu_custom_call" | custom-call | tf_op jit(solution)/shard_map/pallas_call | solution.py:194
  107.7 0.0 copy-start.1
  107.7 13.5 %all_to_all.22 = bf16[16,128,128]{2,1,0:T(8,128)(2,1)S(1)} all-to-all(bf16[16,128,128]{2,1,0:T(8,128)(2,1)S(1)} %shard_map.68), channel_id=1, replica_groups=mesh['z'=16,'c'=2,'g'=2,'yy'=2,'x'=4] {'c','yy','x'}, dimensions={0} | all-to-all | bytes 1048576 | tf_op jit(solution)/shard_map/all_to_all | solution.py:260
  121.3 1.7 %shard_map.69 = bf16[32,32,128]{2,1,0:T(8,128)(2,1)} custom-call(bf16[2,2,4,128,128]{4,3,2,1,0:T(8,128)(2,1)S(1)} %bitcast.5, bf16[32,32,128]{2,1,0:T(8,128)(2,1)S(1)} %all_to_all.20.slots_ref), custom_call_target="tpu_custom_call" | custom-call | tf_op jit(solution)/shard_map/pallas_call | solution.py:194
  122.9 3.7 %all-to-all-start.3 = ((bf16[32,32,128]{2,1,0:T(8,128)(2,1)}), bf16[32,32,128]{2,1,0:T(8,128)(2,1)S(1)}, u32[]{:S(2)}, u32[]{:S(2)}) async-start(bf16[32,32,128]{2,1,0:T(8,128)(2,1)} %shard_map.69), calls=%async_computation.3 | async-start | bytes 524288 | tf_op jit(solution)/shard_map/all_to_all | solution.py:267
  126.6 0.0 copy-done.1
  126.6 0.2 shard_map.64.mix_ref
  126.8 21.4 %all-to-all-done.3 = bf16[32,32,128]{2,1,0:T(8,128)(2,1)S(1)} async-done(((bf16[32,32,128]{2,1,0:T(8,128)(2,1)}), bf16[32,32,128]{2,1,0:T(8,128)(2,1)S(1)}, u32[]{:S(2)}, u32[]{:S(2)}) %all-to-all-start.3) | async-done | bytes 262176 | tf_op jit(solution)/shard_map/all_to_all | solution.py:267
  148.2 0.2 shard_map.70
  148.4 6.3 %collective-permute-start.4 = (bf16[128,128]{1,0:T(8,128)(2,1)S(1)}, bf16[128,128]{1,0:T(8,128)(2,1)S(1)}, u32[]{:S(2)}, u32[]{:S(2)}) collective-permute-start(bf16[128,128]{1,0:T(8,128)(2,1)S(1)} %get-tuple-element.8), channel_id=1, source_target_pairs={{0,12},{12,0},{4,8},{8,4},{1,13},{13,1},{5,9},{9,5},{2,14},{14,2},... | collective-permute-start | bytes 98312 | tf_op jit(solution)/shard_map/ppermute | solution.py:275
  154.7 1.3 collective-permute-done.4
  156.0 0.6 add_convert_fusion
Async XLA Ops:
  0.0 48.6 %copy-start = (s32[32,32]{1,0:T(8,128)S(1)}, s32[32,32]{1,0:T(8,128)}, u32[]{:S(2)}) copy-start(s32[32,32]{1,0:T(8,128)} %selected_ref.3) | copy-start | bytes 12292
  1.4 24.1 %collective-permute-start = (bf16[6144,128]{1,0:T(8,128)(2,1)S(1)}, bf16[6144,128]{1,0:T(8,128)(2,1)S(1)}, u32[]{:S(2)}, u32[]{:S(2)}) collective-permute-start(bf16[6144,128]{1,0:T(8,128)(2,1)S(1)} %shard_map.67), channel_id=1, source_target_pairs={{0,0},{4,4},{24,24},{28,28},{16,12},{12,16},{20,8},{8,20},{1,1},{5... | collective-permute-start | bytes 4718600 | tf_op jit(solution)/shard_map/ppermute | solution.py:225
  25.5 21.1 %collective-permute-start.2 = (bf16[6144,128]{1,0:T(8,128)(2,1)S(1)}, bf16[6144,128]{1,0:T(8,128)(2,1)S(1)}, u32[]{:S(2)}, u32[]{:S(2)}) collective-permute-start(bf16[6144,128]{1,0:T(8,128)(2,1)S(1)} %collective-permute-done.refs_0_), channel_id=1, source_target_pairs={{0,4},{1,5},{2,6},{3,7},{4,0},{5,1},{6,2},{7,3},{16,17},{17,16},{1... | collective-permute-start | bytes 4718600 | tf_op jit(solution)/shard_map/ppermute | solution.py:245
  28.7 76.0 %collective-permute-start.1 = (bf16[6144,128]{1,0:T(8,128)(2,1)S(1)}, bf16[6144,128]{1,0:T(8,128)(2,1)}, u32[]{:S(2)}, u32[]{:S(2)}) collective-permute-start(bf16[6144,128]{1,0:T(8,128)(2,1)S(1)} %collective-permute-done.refs_0_), channel_id=1, source_target_pairs={{0,16},{16,0},{1,17},{17,1},{2,18},{18,2},{3,19},{19,3},{4,20},{20... | collective-permute-start | bytes 4718600 | tf_op jit(solution)/shard_map/ppermute | solution.py:246
  46.7 58.0 %collective-permute-start.3 = (bf16[6144,128]{1,0:T(8,128)(2,1)S(1)}, bf16[6144,128]{1,0:T(8,128)(2,1)}, u32[]{:S(2)}, u32[]{:S(2)}) collective-permute-start(bf16[6144,128]{1,0:T(8,128)(2,1)S(1)} %collective-permute-done.2.refs_2_), channel_id=1, source_target_pairs={{0,16},{16,0},{1,17},{17,1},{2,18},{18,2},{3,19},{19,3},{4,20},{20... | collective-permute-start | bytes 4718600 | tf_op jit(solution)/shard_map/ppermute | solution.py:249
  107.7 18.8 %copy-start.1 = (f32[32,32]{1,0:T(8,128)S(1)}, f32[32,32]{1,0:T(8,128)}, u32[]{:S(2)}) copy-start(f32[32,32]{1,0:T(8,128)} %affinity_ref.1) | copy-start | bytes 12292
  122.9 25.3 %all-to-all-start.3 = ((bf16[32,32,128]{2,1,0:T(8,128)(2,1)}), bf16[32,32,128]{2,1,0:T(8,128)(2,1)S(1)}, u32[]{:S(2)}, u32[]{:S(2)}) async-start(bf16[32,32,128]{2,1,0:T(8,128)(2,1)} %shard_map.69), calls=%async_computation.3 | async-start | bytes 524288 | tf_op jit(solution)/shard_map/all_to_all | solution.py:267
  148.4 7.6 %collective-permute-start.4 = (bf16[128,128]{1,0:T(8,128)(2,1)S(1)}, bf16[128,128]{1,0:T(8,128)(2,1)S(1)}, u32[]{:S(2)}, u32[]{:S(2)}) collective-permute-start(bf16[128,128]{1,0:T(8,128)(2,1)S(1)} %get-tuple-element.8), channel_id=1, source_target_pairs={{0,12},{12,0},{4,8},{8,4},{1,13},{13,1},{5,9},{9,5},{2,14},{14,2},... | collective-permute-start | bytes 98312 | tf_op jit(solution)/shard_map/ppermute | solution.py:275

commit v6 on v5

--- a/solution.py
+++ b/solution.py
@@ -15,7 +15,6 @@
 LIMIT = 32.0
 TRADE = [(0, 0), (1, 1), (6, 6), (7, 7), (4, 3), (3, 4), (5, 2), (2, 5)]
 PAIR = [(0, 3), (3, 0), (1, 2), (2, 1)]
-ACROSS = [(k, k ^ 4) for k in range(8)] + [(k, k ^ 1) for k in range(8, 16)]
 CORES = [(0, 1), (1, 0)]
 
 
@@ -49,10 +48,12 @@
         copy.wait()
 
 
-def pick_kernel(place_ref, selected_ref, tokens_ref, rows_ref, tile_ref, out_ref, sems):
+def pick_kernel(place_ref, selected_ref, tokens_ref, rows_ref, sel_ref, tile_ref, out_ref, sems):
     g, y, x = whereabouts(place_ref)
     experts, most = selected_ref.shape
     _, tok, width = tile_ref.shape
+    first = pltpu.make_async_copy(selected_ref, sel_ref, sems.at[4])
+    first.start()
     loads = []
     for c in range(2):
         block = 4 * ((jnp.minimum, jnp.maximum)[c](y, 3 - y)) + x
@@ -63,7 +64,8 @@
         loads[c].start()
     here = experts // 2
     slots = here * most
-    sel = selected_ref[...].astype(F32).astype(BF)
+    first.wait()
+    sel = sel_ref[...].astype(F32).astype(BF)
     repeat = one_hot(2 * (iota((slots, experts), 0) // most) + g == iota((slots, experts), 1))
     own = iota((slots, most), 0) % most == iota((slots, most), 1)
     spread = jnp.where(own, dot(repeat, sel), 0.0).astype(BF)
@@ -103,7 +105,7 @@
     blocks, most, width = slots_ref.shape
     cores, lines, peers, part, _ = rows_ref.shape
     slots = blocks * most
-    count = 2 * cores * part
+    count = cores * part
     data = slots_ref[...].reshape(slots, width)
     live = one_hot(data.astype(F32) < LIMIT)
     first = one_hot(iota((8, width), 1) == 0)
@@ -118,8 +120,7 @@
     for c in range(cores):
         for k in range(lines):
             for x in range(peers):
-                at = (2 * ((k + x) % 2) + c) * part
-                rows_ref[c, k, x] = rows[at : at + part]
+                rows_ref[c, k, x] = rows[c * part : (c + 1) * part]
 
 
 def seat(block, g):
@@ -152,14 +153,13 @@
     cores, lines, peers, part, width = parts_ref.shape
     blocks, most, _ = slots_ref.shape
     slots = blocks * most
-    quarters = []
-    for half in range(2):
-        for c in range(cores):
-            total = jnp.zeros((part, width), F32)
-            for k in range(lines):
-                for x in range((half + k) % 2, peers, 2):
-                    total = total + parts_ref[c, k, x].astype(F32)
-            quarters.append(total.astype(BF))
+    halves = []
+    for c in range(cores):
+        total = jnp.zeros((part, width), F32)
+        for k in range(lines):
+            for x in range(peers):
+                total = total + parts_ref[c, k, x].astype(F32)
+        halves.append(total.astype(BF))
     live = one_hot(slots_ref[...].reshape(slots, width).astype(F32) < LIMIT)
     in_block = one_hot(iota((blocks, slots), 0) == iota((blocks, slots), 1) // most)
     before = one_hot(iota((slots, blocks), 1) < iota((slots, blocks), 0) // most)
@@ -167,8 +167,8 @@
     rank = dot(before, counts) + (iota((slots, width), 0) % most).astype(F32)
     rank = jnp.where(live > 0.5, rank, -1.0)
     lanes = iota((slots, width), 1).astype(F32)
-    put = [one_hot(rank - k == lanes) for k in range(0, 2 * cores * part, width)]
-    rows = dot(jnp.concatenate(put, axis=1), jnp.concatenate(quarters, axis=0)).astype(BF)
+    put = [one_hot(rank - k == lanes) for k in range(0, cores * part, width)]
+    rows = dot(jnp.concatenate(put, axis=1), jnp.concatenate(halves, axis=0)).astype(BF)
     out_ref[...] = rows.reshape(blocks, most, width)
 
 
@@ -210,9 +210,9 @@
     layers = lax.axis_size("z")
     team = lax.axis_size(TEAM)
     tok, width = tokens.shape
-    _, most = selected.shape
+    experts, most = selected.shape
     span = width // team
-    part = ep * most // 8
+    part = ep * most // 4
     lines = lax.axis_size("yy")
     peers = lax.axis_size("x")
     place = lax.axis_index(TP).astype(jnp.int32).reshape(1)
@@ -227,12 +227,12 @@
         pick_kernel,
         pltpu.HBM((layers, 2, most, span), BF),
         place=place,
-        params=(selected,),
-        hbm=(tokens,),
+        hbm=(selected, tokens),
         scratch=[
+            pltpu.VMEM((experts, most), jnp.int32),
             pltpu.VMEM((2, tok, span), BF),
             pltpu.VMEM((2, layers, most, span), BF),
-            pltpu.SemaphoreType.DMA((4,)),
+            pltpu.SemaphoreType.DMA((5,)),
         ],
     )
     arrived = lax.all_to_all(rows.reshape(ep, most, span), EP, 0, 0, tiled=True)
@@ -242,21 +242,10 @@
         place=place,
         params=(selected, affinity),
     )
-    third = lax.ppermute(mine, ("c", "yy", "x"), ACROSS)
     other = lax.ppermute(mine, "c", CORES)
     copies = local_call(compact_kernel, array((2, lines, peers, part, span)), arrived)
     chosen = lax.all_to_all(copies.reshape(team, part, span), TEAM, 0, 0, tiled=True)
-    fourth = lax.ppermute(third, "c", CORES)
-    partial = local_call(
-        ffn_kernel,
-        array((team, part, span)),
-        chosen,
-        mine,
-        other,
-        third,
-        fourth,
-        place=place,
-    )
+    partial = local_call(ffn_kernel, array((team, part, span)), chosen, mine, other, place=place)
     summands = lax.all_to_all(partial, TEAM, 0, 0, tiled=True)
     result = local_call(
         expand_kernel,

time: 158 us -> 124 us (0.78)
  blocking collectives: 66.9 us -> 40.2 us
  waiting for transfers between devices: 56.9 us -> 45.1 us
  starting transfers between devices: 22.9 us -> 29.4 us
  Pallas kernels: 9.24 us -> 7.63 us
    all_to_all x1 -> x0, blocking collectives: 38 us -> none  [per_device(): arrived = lax.all_to_all(rows.reshape(ep, most, span), EP, 0, 0, tiled=True)]
    all_to_all x0 -> x1, waiting for transfers between devices: none -> 19.8 us  [per_device(): arrived = lax.all_to_all(rows.reshape(ep, most, span), EP, 0, 0, tiled=True)]
    ppermute x1, waiting for transfers between devices: 18.1 us -> 0.53 us  [per_device(): mine = lax.ppermute(packed, ('c', 'g', 'yy'), TRADE)]
    ppermute x2 -> x0, waiting for transfers between devices: 16.1 us -> none  [the longest x1 16.1 us: per_device(): third = lax.ppermute(mine, ('c', 'yy', 'x'), ACROSS)]
    all_to_all x0 -> x1, starting transfers between devices: none -> 15.4 us  [per_device(): arrived = lax.all_to_all(rows.reshape(ep, most, span), EP, 0, 0, tiled=True)]
    all_to_all x1, blocking collectives: 15.3 us -> 21 us  [per_device(): lax.all_to_all(copies.reshape(team, part, span), TEAM, 0, 0, tiled=True)]
    all_to_all x1, blocking collectives: 13.5 us -> 19.2 us  [per_device(): summands = lax.all_to_all(partial, TEAM, 0, 0, tiled=True)]
    ppermute x2 -> x0, starting transfers between devices: 5.02 us -> none  [the longest x1 3.11 us: per_device(): third = lax.ppermute(mine, ('c', 'yy', 'x'), ACROSS)]
  transfers between devices with their start and end apart: 6 -> 5, of which waited for: 4 -> 4; matrix products, arithmetic and copies ran while one was open for 0% -> 0% of each run, Pallas kernels for 2% -> 3%
where the time goes in v6:
time: 124 us; the launch traced here: 123 us
  waiting for transfers between devices  45.1 us (36%)
  blocking collectives  40.2 us (32%)
  starting transfers between devices  29.4 us (24%)
  Pallas kernels  7.63 us (6%)
    all_to_all x1, waiting for transfers between devices, per_device(): returned = lax.all_to_all(result, EP, 0, 0, tiled=True)  21.4 us
    all_to_all x1, blocking collectives, per_device(): lax.all_to_all(copies.reshape(team, part, span), TEAM, 0, 0, tiled=True)  21 us
    all_to_all x1, waiting for transfers between devices, per_device(): arrived = lax.all_to_all(rows.reshape(ep, most, span), EP, 0, 0, tiled=True)  19.8 us
    all_to_all x1, blocking collectives, per_device(): summands = lax.all_to_all(partial, TEAM, 0, 0, tiled=True)  19.2 us
    all_to_all x1, starting transfers between devices, per_device(): arrived = lax.all_to_all(rows.reshape(ep, most, span), EP, 0, 0, tiled=True)  15.4 us
    pallas_call x7, Pallas kernels, local_call(): pl.pallas_call(kernel, in_specs=specs, out_specs=jax.tree.map(lambda o: p...  7.63 us
    ppermute x1, starting transfers between devices, per_device(): mine = lax.ppermute(packed, ('c', 'g', 'yy'), TRADE)  6.02 us
    all_to_all x1, starting transfers between devices, per_device(): returned = lax.all_to_all(result, EP, 0, 0, tiled=True)  3.66 us
  transfers between devices with their start and end apart: 5, of which 4 were waited for; matrix products, arithmetic and copies ran while one was open for 0% of the time, Pallas kernels for 3%

profile of v6, /device:TPU:1, one launch (start us, length us, event | category | flops | bytes accessed | tf_op | source)
XLA Modules:
  0.0 123.1 jit_solution(8496825455458174278)
XLA Ops:
  0.0 1.4 %shard_map.67 = bf16[6144,128]{1,0:T(8,128)(2,1)S(1)} custom-call(bf16[1,2048,128]{2,1,0:T(8,128)(2,1)} %gate_ref.1, bf16[1,2048,128]{2,1,0:T(8,128)(2,1)} %up_ref.1, bf16[1,128,2048]{2,1,0:T(8,128)(2,1)} %down_ref.1), custom_call_target="tpu_custom_call" | custom-call | tf_op jit(solution)/shard_map/pallas_call | solution.py:194
  1.4 6.0 %collective-permute-start = (bf16[6144,128]{1,0:T(8,128)(2,1)S(1)}, bf16[6144,128]{1,0:T(8,128)(2,1)S(1)}, u32[]{:S(2)}, u32[]{:S(2)}) collective-permute-start(bf16[6144,128]{1,0:T(8,128)(2,1)S(1)} %shard_map.67), channel_id=1, source_target_pairs={{0,0},{4,4},{24,24},{28,28},{16,12},{12,16},{20,8},{8,20},{1,1},{5... | collective-permute-start | bytes 4718600 | tf_op jit(solution)/shard_map/ppermute | solution.py:225
  7.5 2.2 %shard_map.65 = bf16[16,2,32,128]{3,2,1,0:T(8,128)(2,1)} custom-call(s32[1]{0:T(128)} %bitcast.place_ref, s32[32,32]{1,0:T(8,128)} %selected_ref.3, bf16[128,2048]{1,0:T(8,128)(2,1)} %tokens_ref.1), custom_call_target="tpu_custom_call" | custom-call | tf_op jit(solution)/shard_map/pallas_call | solution.py:194
  9.6 15.4 %all-to-all-start = ((bf16[32,32,128]{2,1,0:T(8,128)(2,1)}), bf16[32,32,128]{2,1,0:T(8,128)(2,1)S(1)}, u32[]{:S(2)}, u32[]{:S(2)}) async-start(bf16[32,32,128]{2,1,0:T(8,128)(2,1)} %bitcast.8), calls=%async_computation | async-start | bytes 524288 | tf_op jit(solution)/shard_map/all_to_all | solution.py:238
  25.0 0.5 collective-permute-done.refs_0_
  25.5 1.9 %collective-permute-start.1 = (bf16[6144,128]{1,0:T(8,128)(2,1)S(1)}, bf16[6144,128]{1,0:T(8,128)(2,1)S(1)}, u32[]{:S(2)}, u32[]{:S(2)}) collective-permute-start(bf16[6144,128]{1,0:T(8,128)(2,1)S(1)} %collective-permute-done.refs_0_), channel_id=1, source_target_pairs={{0,16},{16,0},{1,17},{17,1},{2,18},{18,2},{3,19},{19,3},{4,20},{20... | collective-permute-start | bytes 4718600 | tf_op jit(solution)/shard_map/ppermute | solution.py:245
  27.5 19.8 %all-to-all-done.slots_ref = bf16[32,32,128]{2,1,0:T(8,128)(2,1)S(1)} async-done(((bf16[32,32,128]{2,1,0:T(8,128)(2,1)}), bf16[32,32,128]{2,1,0:T(8,128)(2,1)S(1)}, u32[]{:S(2)}, u32[]{:S(2)}) %all-to-all-start) | async-done | bytes 262176 | tf_op jit(solution)/shard_map/all_to_all | solution.py:238
  47.3 0.8 shard_map.66
  48.1 21.0 %all_to_all.20.x_ref = bf16[16,256,128]{2,1,0:T(8,128)(2,1)S(1)} all-to-all(bf16[16,256,128]{2,1,0:T(8,128)(2,1)S(1)} %bitcast.5), channel_id=1, replica_groups=mesh['z'=16,'c'=2,'g'=2,'yy'=2,'x'=4] {'c','yy','x'}, dimensions={0} | all-to-all | bytes 2097152 | tf_op jit(solution)/shard_map/all_to_all | solution.py:247
  69.1 0.0 collective-permute-done.1.refs_1_
  69.1 1.1 shard_map.68
  70.2 19.2 %all_to_all.21 = bf16[16,256,128]{2,1,0:T(8,128)(2,1)S(1)} all-to-all(bf16[16,256,128]{2,1,0:T(8,128)(2,1)S(1)} %shard_map.68), channel_id=1, replica_groups=mesh['z'=16,'c'=2,'g'=2,'yy'=2,'x'=4] {'c','yy','x'}, dimensions={0} | all-to-all | bytes 2097152 | tf_op jit(solution)/shard_map/all_to_all | solution.py:249
  89.4 0.0 copy-start
  89.4 0.0 copy-start.1
  89.4 1.7 %shard_map.69 = bf16[32,32,128]{2,1,0:T(8,128)(2,1)} custom-call(bf16[2,2,4,256,128]{4,3,2,1,0:T(8,128)(2,1)S(1)} %bitcast.6, bf16[32,32,128]{2,1,0:T(8,128)(2,1)S(1)} %all-to-all-done.slots_ref), custom_call_target="tpu_custom_call" | custom-call | tf_op jit(solution)/shard_map/pallas_call | solution.py:194
  91.1 3.7 %all-to-all-start.3 = ((bf16[32,32,128]{2,1,0:T(8,128)(2,1)}), bf16[32,32,128]{2,1,0:T(8,128)(2,1)S(1)}, u32[]{:S(2)}, u32[]{:S(2)}) async-start(bf16[32,32,128]{2,1,0:T(8,128)(2,1)} %shard_map.69), calls=%async_computation.3 | async-start | bytes 524288 | tf_op jit(solution)/shard_map/all_to_all | solution.py:256
  94.7 0.0 copy-done
  94.7 0.0 copy-done.1
  94.8 0.2 shard_map.64.mix_ref
  95.0 21.4 %all-to-all-done.3 = bf16[32,32,128]{2,1,0:T(8,128)(2,1)S(1)} async-done(((bf16[32,32,128]{2,1,0:T(8,128)(2,1)}), bf16[32,32,128]{2,1,0:T(8,128)(2,1)S(1)}, u32[]{:S(2)}, u32[]{:S(2)}) %all-to-all-start.3) | async-done | bytes 262176 | tf_op jit(solution)/shard_map/all_to_all | solution.py:256
  116.4 0.2 shard_map.70
  116.6 2.5 %collective-permute-start.2 = (bf16[128,128]{1,0:T(8,128)(2,1)S(1)}, bf16[128,128]{1,0:T(8,128)(2,1)S(1)}, u32[]{:S(2)}, u32[]{:S(2)}) collective-permute-start(bf16[128,128]{1,0:T(8,128)(2,1)S(1)} %get-tuple-element.8), channel_id=1, source_target_pairs={{0,12},{12,0},{4,8},{8,4},{1,13},{13,1},{5,9},{9,5},{2,14},{14,2},... | collective-permute-start | bytes 98312 | tf_op jit(solution)/shard_map/ppermute | solution.py:264
  119.1 3.4 %collective-permute-done.2 = bf16[128,128]{1,0:T(8,128)(2,1)S(1)} collective-permute-done((bf16[128,128]{1,0:T(8,128)(2,1)S(1)}, bf16[128,128]{1,0:T(8,128)(2,1)S(1)}, u32[]{:S(2)}, u32[]{:S(2)}) %collective-permute-start.2) | collective-permute-done | bytes 32800 | tf_op jit(solution)/shard_map/ppermute | solution.py:264
  122.5 0.6 add_convert_fusion
Async XLA Ops:
  1.4 24.1 %collective-permute-start = (bf16[6144,128]{1,0:T(8,128)(2,1)S(1)}, bf16[6144,128]{1,0:T(8,128)(2,1)S(1)}, u32[]{:S(2)}, u32[]{:S(2)}) collective-permute-start(bf16[6144,128]{1,0:T(8,128)(2,1)S(1)} %shard_map.67), channel_id=1, source_target_pairs={{0,0},{4,4},{24,24},{28,28},{16,12},{12,16},{20,8},{8,20},{1,1},{5... | collective-permute-start | bytes 4718600 | tf_op jit(solution)/shard_map/ppermute | solution.py:225
  9.6 37.6 %all-to-all-start = ((bf16[32,32,128]{2,1,0:T(8,128)(2,1)}), bf16[32,32,128]{2,1,0:T(8,128)(2,1)S(1)}, u32[]{:S(2)}, u32[]{:S(2)}) async-start(bf16[32,32,128]{2,1,0:T(8,128)(2,1)} %bitcast.8), calls=%async_computation | async-start | bytes 524288 | tf_op jit(solution)/shard_map/all_to_all | solution.py:238
  25.5 43.6 %collective-permute-start.1 = (bf16[6144,128]{1,0:T(8,128)(2,1)S(1)}, bf16[6144,128]{1,0:T(8,128)(2,1)S(1)}, u32[]{:S(2)}, u32[]{:S(2)}) collective-permute-start(bf16[6144,128]{1,0:T(8,128)(2,1)S(1)} %collective-permute-done.refs_0_), channel_id=1, source_target_pairs={{0,16},{16,0},{1,17},{17,1},{2,18},{18,2},{3,19},{19,3},{4,20},{20... | collective-permute-start | bytes 4718600 | tf_op jit(solution)/shard_map/ppermute | solution.py:245
  89.4 5.4 %copy-start = (s32[32,32]{1,0:T(8,128)S(1)}, s32[32,32]{1,0:T(8,128)}, u32[]{:S(2)}) copy-start(s32[32,32]{1,0:T(8,128)} %selected_ref.3) | copy-start | bytes 12292
  89.4 5.4 %copy-start.1 = (f32[32,32]{1,0:T(8,128)S(1)}, f32[32,32]{1,0:T(8,128)}, u32[]{:S(2)}) copy-start(f32[32,32]{1,0:T(8,128)} %affinity_ref.1) | copy-start | bytes 12292
  91.1 25.3 %all-to-all-start.3 = ((bf16[32,32,128]{2,1,0:T(8,128)(2,1)}), bf16[32,32,128]{2,1,0:T(8,128)(2,1)S(1)}, u32[]{:S(2)}, u32[]{:S(2)}) async-start(bf16[32,32,128]{2,1,0:T(8,128)(2,1)} %shard_map.69), calls=%async_computation.3 | async-start | bytes 524288 | tf_op jit(solution)/shard_map/all_to_all | solution.py:256
  116.6 5.9 %collective-permute-start.2 = (bf16[128,128]{1,0:T(8,128)(2,1)S(1)}, bf16[128,128]{1,0:T(8,128)(2,1)S(1)}, u32[]{:S(2)}, u32[]{:S(2)}) collective-permute-start(bf16[128,128]{1,0:T(8,128)(2,1)S(1)} %get-tuple-element.8), channel_id=1, source_target_pairs={{0,12},{12,0},{4,8},{8,4},{1,13},{13,1},{5,9},{9,5},{2,14},{14,2},... | collective-permute-start | bytes 98312 | tf_op jit(solution)/shard_map/ppermute | solution.py:264

commit v7 on v6

--- a/solution.py
+++ b/solution.py
@@ -101,7 +101,7 @@
     mix_ref[1] = jnp.where(hit, as_row(low), 0.0).astype(BF)
 
 
-def compact_kernel(slots_ref, rows_ref):
+def compact_kernel(slots_ref, rows_ref, half_ref, sems):
     blocks, most, width = slots_ref.shape
     cores, lines, peers, part, _ = rows_ref.shape
     slots = blocks * most
@@ -116,11 +116,16 @@
     rank = dot(counts.astype(BF), before) + (iota((8, slots), 1) % most).astype(F32)
     rank = jnp.where(live_row > 0.5, rank, -1.0)[0:1]
     take = one_hot(rank == iota((count, slots), 0).astype(F32))
-    rows = dot(take, data).astype(BF)
+    copies = []
     for c in range(cores):
+        half_ref[c] = dot(take[c * part : (c + 1) * part], data).astype(BF)
         for k in range(lines):
             for x in range(peers):
-                rows_ref[c, k, x] = rows[c * part : (c + 1) * part]
+                sem = sems.at[len(copies)]
+                copies.append(pltpu.make_async_copy(half_ref.at[c], rows_ref.at[c, k, x], sem))
+                copies[-1].start()
+    for copy in copies:
+        copy.wait()
 
 
 def seat(block, g):
@@ -129,19 +134,32 @@
     return (y // 2) * 8 + 4 * (yy + g - 2 * yy * g) + block % 4
 
 
-def ffn_kernel(place_ref, x_ref, *refs):
-    *weights, out_ref = refs
+def ffn_kernel(place_ref, x_ref, mine_ref, other_ref, out_ref, local_ref, sems):
     g, _, _ = whereabouts(place_ref)
     peers, _, span = x_ref.shape
     width = peers * span
+    loads = []
+    for k in range(3):
+        part = pl.ds(k * width, width)
+        loads.append(pltpu.make_async_copy(other_ref.at[part], local_ref.at[part], sems.at[k]))
+        loads[k].start()
     x = jnp.concatenate([x_ref[seat(k, g)] for k in range(peers)], axis=1)
-    gate = dot(x, jnp.concatenate([w[:width] for w in weights], axis=1))
-    up = dot(x, jnp.concatenate([w[width : 2 * width] for w in weights], axis=1))
-    hidden = (gate / (1.0 + jnp.exp(-gate)) * up).astype(BF)
+    hidden = []
+    for w in (mine_ref, local_ref):
+        if w is local_ref:
+            loads[0].wait()
+            loads[1].wait()
+        both = dot(x, jnp.concatenate([w[:width], w[width : 2 * width]], axis=1))
+        gate = both[:, :span]
+        hidden.append((gate / (1.0 + jnp.exp(-gate)) * both[:, span:]).astype(BF))
+    hidden = jnp.concatenate(hidden, axis=1)
+    loads[2].wait()
     for k in range(0, peers, 2):
         at = 2 * width + k * span
         tiles = [
-            jnp.concatenate([w[at + j * span : at + (j + 1) * span] for w in weights], axis=0)
+            jnp.concatenate(
+                [w[at + j * span : at + (j + 1) * span] for w in (mine_ref, local_ref)], axis=0
+            )
             for j in range(2)
         ]
         partial = dot(hidden, jnp.concatenate(tiles, axis=1)).astype(BF)
@@ -218,7 +236,7 @@
     place = lax.axis_index(TP).astype(jnp.int32).reshape(1)
     packed = local_call(
         pack_kernel,
-        array((3 * width, span)),
+        pltpu.HBM((3 * width, span), BF),
         hbm=(w_gate, w_up, w_down),
         scratch=[pltpu.SemaphoreType.DMA((2 + team,))],
     )
@@ -243,9 +261,22 @@
         params=(selected, affinity),
     )
     other = lax.ppermute(mine, "c", CORES)
-    copies = local_call(compact_kernel, array((2, lines, peers, part, span)), arrived)
+    copies = local_call(
+        compact_kernel,
+        pltpu.HBM((2, lines, peers, part, span), BF),
+        arrived,
+        scratch=[pltpu.VMEM((2, part, span), BF), pltpu.SemaphoreType.DMA((team,))],
+    )
     chosen = lax.all_to_all(copies.reshape(team, part, span), TEAM, 0, 0, tiled=True)
-    partial = local_call(ffn_kernel, array((team, part, span)), chosen, mine, other, place=place)
+    partial = local_call(
+        ffn_kernel,
+        array((team, part, span)),
+        chosen,
+        mine,
+        place=place,
+        hbm=(other,),
+        scratch=[pltpu.VMEM((3 * width, span), BF), pltpu.SemaphoreType.DMA((3,))],
+    )
     summands = lax.all_to_all(partial, TEAM, 0, 0, tiled=True)
     result = local_call(
         expand_kernel,

time: 124 us -> 176 us (1.42)
  Pallas kernels: 7.63 us -> 57.9 us
    pallas_call x7, Pallas kernels: 7.63 us -> 57.9 us  [local_call(): pl.pallas_call(kernel, in_specs=specs, out_specs=jax.tree.map(lambda o: p...]
  transfers between devices with their start and end apart: 5 -> 5, of which waited for: 4 -> 4; matrix products, arithmetic and copies ran while one was open for 0% -> 0% of each run, Pallas kernels for 3% -> 2%
where the time goes in v7:
time: 176 us; the launch traced here: 175 us
  Pallas kernels  57.9 us (33%)
  waiting for transfers between devices  45.1 us (26%)
  blocking collectives  40.4 us (23%)
  starting transfers between devices  29.4 us (17%)
    pallas_call x7, Pallas kernels, local_call(): pl.pallas_call(kernel, in_specs=specs, out_specs=jax.tree.map(lambda o: p...  57.9 us
    all_to_all x1, waiting for transfers between devices, per_device(): returned = lax.all_to_all(result, EP, 0, 0, tiled=True)  21.4 us
    all_to_all x1, blocking collectives, per_device(): lax.all_to_all(copies.reshape(team, part, span), TEAM, 0, 0, tiled=True)  21.2 us
    all_to_all x1, waiting for transfers between devices, per_device(): arrived = lax.all_to_all(rows.reshape(ep, most, span), EP, 0, 0, tiled=True)  19.6 us
    all_to_all x1, blocking collectives, per_device(): summands = lax.all_to_all(partial, TEAM, 0, 0, tiled=True)  19.2 us
    all_to_all x1, starting transfers between devices, per_device(): arrived = lax.all_to_all(rows.reshape(ep, most, span), EP, 0, 0, tiled=True)  15.4 us
    ppermute x1, starting transfers between devices, per_device(): mine = lax.ppermute(packed, ('c', 'g', 'yy'), TRADE)  6.02 us
    all_to_all x1, starting transfers between devices, per_device(): returned = lax.all_to_all(result, EP, 0, 0, tiled=True)  3.66 us
  transfers between devices with their start and end apart: 5, of which 4 were waited for; matrix products, arithmetic and copies ran while one was open for 0% of the time, Pallas kernels for 2%

profile of v7, /device:TPU:1, one launch (start us, length us, event | category | flops | bytes accessed | tf_op | source)
XLA Modules:
  0.0 174.8 jit_solution(9637211080877667755)
XLA Ops:
  0.0 48.9 %shard_map.67 = bf16[6144,128]{1,0:T(8,128)(2,1)} custom-call(bf16[1,2048,128]{2,1,0:T(8,128)(2,1)} %gate_ref.1, bf16[1,2048,128]{2,1,0:T(8,128)(2,1)} %up_ref.1, bf16[1,128,2048]{2,1,0:T(8,128)(2,1)} %down_ref.1), custom_call_target="tpu_custom_call" | custom-call | tf_op jit(solution)/shard_map/pallas_call | solution.py:212
  48.9 6.0 %collective-permute-start = (bf16[6144,128]{1,0:T(8,128)(2,1)}, bf16[6144,128]{1,0:T(8,128)(2,1)S(1)}, u32[]{:S(2)}, u32[]{:S(2)}) collective-permute-start(bf16[6144,128]{1,0:T(8,128)(2,1)} %shard_map.67), channel_id=1, source_target_pairs={{0,0},{4,4},{24,24},{28,28},{16,12},{12,16},{20,8},{8,20},{1,1},{5... | collective-permute-start | bytes 4718600 | tf_op jit(solution)/shard_map/ppermute | solution.py:243
  55.0 2.1 %shard_map.65 = bf16[16,2,32,128]{3,2,1,0:T(8,128)(2,1)} custom-call(s32[1]{0:T(128)} %bitcast.place_ref, s32[32,32]{1,0:T(8,128)} %selected_ref.3, bf16[128,2048]{1,0:T(8,128)(2,1)} %tokens_ref.1), custom_call_target="tpu_custom_call" | custom-call | tf_op jit(solution)/shard_map/pallas_call | solution.py:212
  57.1 15.4 %all-to-all-start = ((bf16[32,32,128]{2,1,0:T(8,128)(2,1)}), bf16[32,32,128]{2,1,0:T(8,128)(2,1)S(1)}, u32[]{:S(2)}, u32[]{:S(2)}) async-start(bf16[32,32,128]{2,1,0:T(8,128)(2,1)} %bitcast.8), calls=%async_computation | async-start | bytes 524288 | tf_op jit(solution)/shard_map/all_to_all | solution.py:256
  72.5 0.8 collective-permute-done.mine_ref
  73.2 1.9 %collective-permute-start.1 = (bf16[6144,128]{1,0:T(8,128)(2,1)S(1)}, bf16[6144,128]{1,0:T(8,128)(2,1)S(1)}, u32[]{:S(2)}, u32[]{:S(2)}) collective-permute-start(bf16[6144,128]{1,0:T(8,128)(2,1)S(1)} %collective-permute-done.mine_ref), channel_id=1, source_target_pairs={{0,16},{16,0},{1,17},{17,1},{2,18},{18,2},{3,19},{19,3},{4,20},{20... | collective-permute-start | bytes 4718600 | tf_op jit(solution)/shard_map/ppermute | solution.py:263
  75.2 19.6 %all-to-all-done.slots_ref = bf16[32,32,128]{2,1,0:T(8,128)(2,1)S(1)} async-done(((bf16[32,32,128]{2,1,0:T(8,128)(2,1)}), bf16[32,32,128]{2,1,0:T(8,128)(2,1)S(1)}, u32[]{:S(2)}, u32[]{:S(2)}) %all-to-all-start) | async-done | bytes 262176 | tf_op jit(solution)/shard_map/all_to_all | solution.py:256
  94.7 1.8 %shard_map.66 = bf16[2,2,4,256,128]{4,3,2,1,0:T(8,128)(2,1)} custom-call(bf16[32,32,128]{2,1,0:T(8,128)(2,1)S(1)} %all-to-all-done.slots_ref), custom_call_target="tpu_custom_call" | custom-call | tf_op jit(solution)/shard_map/pallas_call | solution.py:212
  96.6 21.2 %all_to_all.20.x_ref = bf16[16,256,128]{2,1,0:T(8,128)(2,1)S(1)} all-to-all(bf16[16,256,128]{2,1,0:T(8,128)(2,1)} %bitcast.7), channel_id=1, replica_groups=mesh['z'=16,'c'=2,'g'=2,'yy'=2,'x'=4] {'c','yy','x'}, dimensions={0} | all-to-all | bytes 2097152 | tf_op jit(solution)/shard_map/all_to_all | solution.py:270
  117.8 0.0 collective-permute-done.1.other_ref
  117.8 0.0 copy-start.2
  117.8 1.2 copy-done.2
  118.9 2.9 %shard_map.68 = bf16[16,256,128]{2,1,0:T(8,128)(2,1)S(1)} custom-call(s32[1]{0:T(128)} %bitcast.place_ref, bf16[16,256,128]{2,1,0:T(8,128)(2,1)S(1)} %all_to_all.20.x_ref, bf16[6144,128]{1,0:T(8,128)(2,1)S(1)} %collective-permute-done.mine_ref, bf16[6144,128]{1,0:T(8,128)(2,1)} %copy-done.2), custom_call_target="tpu_custom_call" | custom-call | tf_op jit(solution)/shard_map/pallas_call | solution.py:212
  121.9 19.2 %all_to_all.21 = bf16[16,256,128]{2,1,0:T(8,128)(2,1)S(1)} all-to-all(bf16[16,256,128]{2,1,0:T(8,128)(2,1)S(1)} %shard_map.68), channel_id=1, replica_groups=mesh['z'=16,'c'=2,'g'=2,'yy'=2,'x'=4] {'c','yy','x'}, dimensions={0} | all-to-all | bytes 2097152 | tf_op jit(solution)/shard_map/all_to_all | solution.py:280
  141.0 0.0 copy-start
  141.0 0.0 copy-start.1
  141.0 1.7 shard_map.69
  142.8 3.7 %all-to-all-start.3 = ((bf16[32,32,128]{2,1,0:T(8,128)(2,1)}), bf16[32,32,128]{2,1,0:T(8,128)(2,1)S(1)}, u32[]{:S(2)}, u32[]{:S(2)}) async-start(bf16[32,32,128]{2,1,0:T(8,128)(2,1)} %shard_map.69), calls=%async_computation.3 | async-start | bytes 524288 | tf_op jit(solution)/shard_map/all_to_all | solution.py:287
  146.4 0.0 copy-done
  146.4 0.0 copy-done.1
  146.4 0.2 shard_map.64.mix_ref
  146.7 21.4 %all-to-all-done.3 = bf16[32,32,128]{2,1,0:T(8,128)(2,1)S(1)} async-done(((bf16[32,32,128]{2,1,0:T(8,128)(2,1)}), bf16[32,32,128]{2,1,0:T(8,128)(2,1)S(1)}, u32[]{:S(2)}, u32[]{:S(2)}) %all-to-all-start.3) | async-done | bytes 262176 | tf_op jit(solution)/shard_map/all_to_all | solution.py:287
  168.0 0.2 shard_map.70
  168.3 2.5 %collective-permute-start.2 = (bf16[128,128]{1,0:T(8,128)(2,1)S(1)}, bf16[128,128]{1,0:T(8,128)(2,1)S(1)}, u32[]{:S(2)}, u32[]{:S(2)}) collective-permute-start(bf16[128,128]{1,0:T(8,128)(2,1)S(1)} %get-tuple-element.8), channel_id=1, source_target_pairs={{0,12},{12,0},{4,8},{8,4},{1,13},{13,1},{5,9},{9,5},{2,14},{14,2},... | collective-permute-start | bytes 98312 | tf_op jit(solution)/shard_map/ppermute | solution.py:295
  170.8 3.4 %collective-permute-done.2 = bf16[128,128]{1,0:T(8,128)(2,1)S(1)} collective-permute-done((bf16[128,128]{1,0:T(8,128)(2,1)S(1)}, bf16[128,128]{1,0:T(8,128)(2,1)S(1)}, u32[]{:S(2)}, u32[]{:S(2)}) %collective-permute-start.2) | collective-permute-done | bytes 32800 | tf_op jit(solution)/shard_map/ppermute | solution.py:295
  174.2 0.6 add_convert_fusion
Async XLA Ops:
  48.9 24.3 %collective-permute-start = (bf16[6144,128]{1,0:T(8,128)(2,1)}, bf16[6144,128]{1,0:T(8,128)(2,1)S(1)}, u32[]{:S(2)}, u32[]{:S(2)}) collective-permute-start(bf16[6144,128]{1,0:T(8,128)(2,1)} %shard_map.67), channel_id=1, source_target_pairs={{0,0},{4,4},{24,24},{28,28},{16,12},{12,16},{20,8},{8,20},{1,1},{5... | collective-permute-start | bytes 4718600 | tf_op jit(solution)/shard_map/ppermute | solution.py:243
  57.1 37.6 %all-to-all-start = ((bf16[32,32,128]{2,1,0:T(8,128)(2,1)}), bf16[32,32,128]{2,1,0:T(8,128)(2,1)S(1)}, u32[]{:S(2)}, u32[]{:S(2)}) async-start(bf16[32,32,128]{2,1,0:T(8,128)(2,1)} %bitcast.8), calls=%async_computation | async-start | bytes 524288 | tf_op jit(solution)/shard_map/all_to_all | solution.py:256
  73.2 44.5 %collective-permute-start.1 = (bf16[6144,128]{1,0:T(8,128)(2,1)S(1)}, bf16[6144,128]{1,0:T(8,128)(2,1)S(1)}, u32[]{:S(2)}, u32[]{:S(2)}) collective-permute-start(bf16[6144,128]{1,0:T(8,128)(2,1)S(1)} %collective-permute-done.mine_ref), channel_id=1, source_target_pairs={{0,16},{16,0},{1,17},{17,1},{2,18},{18,2},{3,19},{19,3},{4,20},{20... | collective-permute-start | bytes 4718600 | tf_op jit(solution)/shard_map/ppermute | solution.py:263
  117.8 1.2 copy-start.2
  141.0 5.4 %copy-start = (s32[32,32]{1,0:T(8,128)S(1)}, s32[32,32]{1,0:T(8,128)}, u32[]{:S(2)}) copy-start(s32[32,32]{1,0:T(8,128)} %selected_ref.3) | copy-start | bytes 12292
  141.0 5.4 %copy-start.1 = (f32[32,32]{1,0:T(8,128)S(1)}, f32[32,32]{1,0:T(8,128)}, u32[]{:S(2)}) copy-start(f32[32,32]{1,0:T(8,128)} %affinity_ref.1) | copy-start | bytes 12292
  142.8 25.3 %all-to-all-start.3 = ((bf16[32,32,128]{2,1,0:T(8,128)(2,1)}), bf16[32,32,128]{2,1,0:T(8,128)(2,1)S(1)}, u32[]{:S(2)}, u32[]{:S(2)}) async-start(bf16[32,32,128]{2,1,0:T(8,128)(2,1)} %shard_map.69), calls=%async_computation.3 | async-start | bytes 524288 | tf_op jit(solution)/shard_map/all_to_all | solution.py:287
  168.3 5.9 %collective-permute-start.2 = (bf16[128,128]{1,0:T(8,128)(2,1)S(1)}, bf16[128,128]{1,0:T(8,128)(2,1)S(1)}, u32[]{:S(2)}, u32[]{:S(2)}) collective-permute-start(bf16[128,128]{1,0:T(8,128)(2,1)S(1)} %get-tuple-element.8), channel_id=1, source_target_pairs={{0,12},{12,0},{4,8},{8,4},{1,13},{13,1},{5,9},{9,5},{2,14},{14,2},... | collective-permute-start | bytes 98312 | tf_op jit(solution)/shard_map/ppermute | solution.py:295

commit v8 on v6

--- a/solution.py
+++ b/solution.py
@@ -35,20 +35,21 @@
     return place // 8, place // 4, place % 4
 
 
-def pack_kernel(gate_ref, up_ref, down_ref, out_ref, sems):
-    _, width, span = gate_ref.shape
-    copies = [(gate_ref.at[0], out_ref.at[:width]), (up_ref.at[0], out_ref.at[width : 2 * width])]
-    for k in range(width // span):
-        at = 2 * width + k * span
-        copies.append((down_ref.at[0, :, k * span : (k + 1) * span], out_ref.at[at : at + span]))
-    copies = [pltpu.make_async_copy(*c, sems.at[k]) for k, c in enumerate(copies)]
-    for copy in copies:
-        copy.start()
-    for copy in copies:
-        copy.wait()
-
-
-def pick_kernel(place_ref, selected_ref, tokens_ref, rows_ref, sel_ref, tile_ref, out_ref, sems):
+def pick_kernel(
+    place_ref,
+    selected_ref,
+    tokens_ref,
+    gate_ref,
+    up_ref,
+    down_ref,
+    rows_ref,
+    packed_ref,
+    sel_ref,
+    tile_ref,
+    out_ref,
+    sems,
+    pack_sems,
+):
     g, y, x = whereabouts(place_ref)
     experts, most = selected_ref.shape
     _, tok, width = tile_ref.shape
@@ -62,6 +63,16 @@
             pltpu.make_async_copy(tokens_ref.at[:, pl.ds(at, width)], tile_ref.at[c], sems.at[c])
         )
         loads[c].start()
+    _, full, span = gate_ref.shape
+    pieces = [(gate_ref.at[0], packed_ref.at[:full])]
+    pieces.append((up_ref.at[0], packed_ref.at[full : 2 * full]))
+    for k in range(full // span):
+        at = 2 * full + k * span
+        piece = down_ref.at[0, :, k * span : (k + 1) * span]
+        pieces.append((piece, packed_ref.at[at : at + span]))
+    pieces = [pltpu.make_async_copy(*p, pack_sems.at[k]) for k, p in enumerate(pieces)]
+    for piece in pieces:
+        piece.start()
     here = experts // 2
     slots = here * most
     first.wait()
@@ -78,8 +89,8 @@
         out_ref[c] = rows.reshape(here, most, width)
         stores.append(pltpu.make_async_copy(out_ref.at[c], rows_ref.at[:, c], sems.at[2 + c]))
         stores[c].start()
-    for store in stores:
-        store.wait()
+    for copy in stores + pieces:
+        copy.wait()
 
 
 def mix_kernel(place_ref, selected_ref, affinity_ref, mix_ref):
@@ -216,25 +227,20 @@
     lines = lax.axis_size("yy")
     peers = lax.axis_size("x")
     place = lax.axis_index(TP).astype(jnp.int32).reshape(1)
-    packed = local_call(
-        pack_kernel,
-        array((3 * width, span)),
-        hbm=(w_gate, w_up, w_down),
-        scratch=[pltpu.SemaphoreType.DMA((2 + team,))],
-    )
-    mine = lax.ppermute(packed, ("c", "g", "yy"), TRADE)
-    rows = local_call(
+    rows, packed = local_call(
         pick_kernel,
-        pltpu.HBM((layers, 2, most, span), BF),
+        [pltpu.HBM((layers, 2, most, span), BF), array((3 * width, span))],
         place=place,
-        hbm=(selected, tokens),
+        hbm=(selected, tokens, w_gate, w_up, w_down),
         scratch=[
             pltpu.VMEM((experts, most), jnp.int32),
             pltpu.VMEM((2, tok, span), BF),
             pltpu.VMEM((2, layers, most, span), BF),
             pltpu.SemaphoreType.DMA((5,)),
+            pltpu.SemaphoreType.DMA((2 + team,)),
         ],
     )
+    mine = lax.ppermute(packed, ("c", "g", "yy"), TRADE)
     arrived = lax.all_to_all(rows.reshape(ep, most, span), EP, 0, 0, tiled=True)
     mix = local_call(
         mix_kernel,

time: 124 us -> 123 us (level)
    ppermute x1, waiting for transfers between devices: 0.53 us -> 2.71 us  [per_device(): mine = lax.ppermute(packed, ('c', 'g', 'yy'), TRADE)]
    all_to_all x1, waiting for transfers between devices: 19.8 us -> 17.6 us  [per_device(): arrived = lax.all_to_all(rows.reshape(ep, most, span), EP, 0, 0, tiled=True)]
    pallas_call x7 -> x6, Pallas kernels: 7.63 us -> 6.92 us  [local_call(): pl.pallas_call(kernel, in_specs=specs, out_specs=jax.tree.map(lambda o: p...]
  transfers between devices with their start and end apart: 5 -> 5, of which waited for: 4 -> 4; matrix products, arithmetic and copies ran while one was open for 0% -> 0% of each run, Pallas kernels for 3% -> 1%
where the time goes in v8:
time: 123 us; the launch traced here: 122 us
  waiting for transfers between devices  45.1 us (37%)
  blocking collectives  40.2 us (33%)
  starting transfers between devices  29.5 us (24%)
  Pallas kernels  6.92 us (6%)
    all_to_all x1, waiting for transfers between devices, per_device(): returned = lax.all_to_all(result, EP, 0, 0, tiled=True)  21.4 us
    all_to_all x1, blocking collectives, per_device(): lax.all_to_all(copies.reshape(team, part, span), TEAM, 0, 0, tiled=True)  21 us
    all_to_all x1, blocking collectives, per_device(): summands = lax.all_to_all(partial, TEAM, 0, 0, tiled=True)  19.2 us
    all_to_all x1, waiting for transfers between devices, per_device(): arrived = lax.all_to_all(rows.reshape(ep, most, span), EP, 0, 0, tiled=True)  17.6 us
    all_to_all x1, starting transfers between devices, per_device(): arrived = lax.all_to_all(rows.reshape(ep, most, span), EP, 0, 0, tiled=True)  15.4 us
    pallas_call x6, Pallas kernels, local_call(): pl.pallas_call(kernel, in_specs=specs, out_specs=jax.tree.map(lambda o: p...  6.92 us
    ppermute x1, starting transfers between devices, per_device(): mine = lax.ppermute(packed, ('c', 'g', 'yy'), TRADE)  6.02 us
    all_to_all x1, starting transfers between devices, per_device(): returned = lax.all_to_all(result, EP, 0, 0, tiled=True)  3.65 us
  transfers between devices with their start and end apart: 5, of which 4 were waited for; matrix products, arithmetic and copies ran while one was open for 0% of the time, Pallas kernels for 1%

profile of v8, /device:TPU:1, one launch (start us, length us, event | category | flops | bytes accessed | tf_op | source)
XLA Modules:
  0.0 122.4 jit_solution(677267264373799268)
XLA Ops:
  0.0 2.9 %shard_map.65 = (bf16[16,2,32,128]{3,2,1,0:T(8,128)(2,1)}, bf16[6144,128]{1,0:T(8,128)(2,1)S(1)}) custom-call(s32[1]{0:T(128)} %bitcast.place_ref, s32[32,32]{1,0:T(8,128)} %selected_ref.3, bf16[128,2048]{1,0:T(8,128)(2,1)} %tokens_ref.1, bf16[1,2048,128]{2,1,0:T(8,128)(2,1)} %gate_ref.1, bf16[1,2048,128]{2,1,0:T(8,128)(2,1)} %up_ref.1, ...), custom_call_target="tpu_custom_call" | custom-call | tf_op jit(solution)/shard_map/pallas_call | solution.py:205
  2.9 6.0 %collective-permute-start = (bf16[6144,128]{1,0:T(8,128)(2,1)S(1)}, bf16[6144,128]{1,0:T(8,128)(2,1)S(1)}, u32[]{:S(2)}, u32[]{:S(2)}) collective-permute-start(bf16[6144,128]{1,0:T(8,128)(2,1)S(1)} %get-tuple-element.10), channel_id=1, source_target_pairs={{0,0},{4,4},{24,24},{28,28},{16,12},{12,16},{20,8},{8,20},{1,1},{5... | collective-permute-start | bytes 4718600 | tf_op jit(solution)/shard_map/ppermute | solution.py:243
  8.9 15.4 %all-to-all-start = ((bf16[32,32,128]{2,1,0:T(8,128)(2,1)}), bf16[32,32,128]{2,1,0:T(8,128)(2,1)S(1)}, u32[]{:S(2)}, u32[]{:S(2)}) async-start(bf16[32,32,128]{2,1,0:T(8,128)(2,1)} %bitcast.8), calls=%async_computation | async-start | bytes 524288 | tf_op jit(solution)/shard_map/all_to_all | solution.py:244
  24.3 2.7 %collective-permute-done.refs_0_ = bf16[6144,128]{1,0:T(8,128)(2,1)S(1)} collective-permute-done((bf16[6144,128]{1,0:T(8,128)(2,1)S(1)}, bf16[6144,128]{1,0:T(8,128)(2,1)S(1)}, u32[]{:S(2)}, u32[]{:S(2)}) %collective-permute-start) | collective-permute-done | bytes 1572896 | tf_op jit(solution)/shard_map/ppermute | solution.py:243
  27.0 1.9 %collective-permute-start.1 = (bf16[6144,128]{1,0:T(8,128)(2,1)S(1)}, bf16[6144,128]{1,0:T(8,128)(2,1)S(1)}, u32[]{:S(2)}, u32[]{:S(2)}) collective-permute-start(bf16[6144,128]{1,0:T(8,128)(2,1)S(1)} %collective-permute-done.refs_0_), channel_id=1, source_target_pairs={{0,16},{16,0},{1,17},{17,1},{2,18},{18,2},{3,19},{19,3},{4,20},{20... | collective-permute-start | bytes 4718600 | tf_op jit(solution)/shard_map/ppermute | solution.py:251
  28.9 17.6 %all-to-all-done.slots_ref = bf16[32,32,128]{2,1,0:T(8,128)(2,1)S(1)} async-done(((bf16[32,32,128]{2,1,0:T(8,128)(2,1)}), bf16[32,32,128]{2,1,0:T(8,128)(2,1)S(1)}, u32[]{:S(2)}, u32[]{:S(2)}) %all-to-all-start) | async-done | bytes 262176 | tf_op jit(solution)/shard_map/all_to_all | solution.py:244
  46.5 0.8 shard_map.66
  47.4 21.0 %all_to_all.20.x_ref = bf16[16,256,128]{2,1,0:T(8,128)(2,1)S(1)} all-to-all(bf16[16,256,128]{2,1,0:T(8,128)(2,1)S(1)} %bitcast.5), channel_id=1, replica_groups=mesh['z'=16,'c'=2,'g'=2,'yy'=2,'x'=4] {'c','yy','x'}, dimensions={0} | all-to-all | bytes 2097152 | tf_op jit(solution)/shard_map/all_to_all | solution.py:253
  68.4 0.0 collective-permute-done.1.refs_1_
  68.4 1.1 shard_map.67
  69.4 19.2 %all_to_all.21 = bf16[16,256,128]{2,1,0:T(8,128)(2,1)S(1)} all-to-all(bf16[16,256,128]{2,1,0:T(8,128)(2,1)S(1)} %shard_map.67), channel_id=1, replica_groups=mesh['z'=16,'c'=2,'g'=2,'yy'=2,'x'=4] {'c','yy','x'}, dimensions={0} | all-to-all | bytes 2097152 | tf_op jit(solution)/shard_map/all_to_all | solution.py:255
  88.6 0.0 copy-start
  88.6 0.0 copy-start.1
  88.6 1.7 %shard_map.68 = bf16[32,32,128]{2,1,0:T(8,128)(2,1)} custom-call(bf16[2,2,4,256,128]{4,3,2,1,0:T(8,128)(2,1)S(1)} %bitcast.6, bf16[32,32,128]{2,1,0:T(8,128)(2,1)S(1)} %all-to-all-done.slots_ref), custom_call_target="tpu_custom_call" | custom-call | tf_op jit(solution)/shard_map/pallas_call | solution.py:205
  90.3 3.7 %all-to-all-start.3 = ((bf16[32,32,128]{2,1,0:T(8,128)(2,1)}), bf16[32,32,128]{2,1,0:T(8,128)(2,1)S(1)}, u32[]{:S(2)}, u32[]{:S(2)}) async-start(bf16[32,32,128]{2,1,0:T(8,128)(2,1)} %shard_map.68), calls=%async_computation.3 | async-start | bytes 524288 | tf_op jit(solution)/shard_map/all_to_all | solution.py:262
  94.0 0.0 copy-done
  94.0 0.0 copy-done.1
  94.0 0.2 shard_map.64.mix_ref
  94.2 21.4 %all-to-all-done.3 = bf16[32,32,128]{2,1,0:T(8,128)(2,1)S(1)} async-done(((bf16[32,32,128]{2,1,0:T(8,128)(2,1)}), bf16[32,32,128]{2,1,0:T(8,128)(2,1)S(1)}, u32[]{:S(2)}, u32[]{:S(2)}) %all-to-all-start.3) | async-done | bytes 262176 | tf_op jit(solution)/shard_map/all_to_all | solution.py:262
  115.6 0.2 shard_map.69
  115.9 2.5 %collective-permute-start.2 = (bf16[128,128]{1,0:T(8,128)(2,1)S(1)}, bf16[128,128]{1,0:T(8,128)(2,1)S(1)}, u32[]{:S(2)}, u32[]{:S(2)}) collective-permute-start(bf16[128,128]{1,0:T(8,128)(2,1)S(1)} %get-tuple-element.12), channel_id=1, source_target_pairs={{0,12},{12,0},{4,8},{8,4},{1,13},{13,1},{5,9},{9,5},{2,14},{14,2},... | collective-permute-start | bytes 98312 | tf_op jit(solution)/shard_map/ppermute | solution.py:270
  118.4 3.4 %collective-permute-done.2 = bf16[128,128]{1,0:T(8,128)(2,1)S(1)} collective-permute-done((bf16[128,128]{1,0:T(8,128)(2,1)S(1)}, bf16[128,128]{1,0:T(8,128)(2,1)S(1)}, u32[]{:S(2)}, u32[]{:S(2)}) %collective-permute-start.2) | collective-permute-done | bytes 32800 | tf_op jit(solution)/shard_map/ppermute | solution.py:270
  121.7 0.6 add_convert_fusion
Async XLA Ops:
  2.9 24.1 %collective-permute-start = (bf16[6144,128]{1,0:T(8,128)(2,1)S(1)}, bf16[6144,128]{1,0:T(8,128)(2,1)S(1)}, u32[]{:S(2)}, u32[]{:S(2)}) collective-permute-start(bf16[6144,128]{1,0:T(8,128)(2,1)S(1)} %get-tuple-element.10), channel_id=1, source_target_pairs={{0,0},{4,4},{24,24},{28,28},{16,12},{12,16},{20,8},{8,20},{1,1},{5... | collective-permute-start | bytes 4718600 | tf_op jit(solution)/shard_map/ppermute | solution.py:243
  8.9 37.6 %all-to-all-start = ((bf16[32,32,128]{2,1,0:T(8,128)(2,1)}), bf16[32,32,128]{2,1,0:T(8,128)(2,1)S(1)}, u32[]{:S(2)}, u32[]{:S(2)}) async-start(bf16[32,32,128]{2,1,0:T(8,128)(2,1)} %bitcast.8), calls=%async_computation | async-start | bytes 524288 | tf_op jit(solution)/shard_map/all_to_all | solution.py:244
  27.0 41.4 %collective-permute-start.1 = (bf16[6144,128]{1,0:T(8,128)(2,1)S(1)}, bf16[6144,128]{1,0:T(8,128)(2,1)S(1)}, u32[]{:S(2)}, u32[]{:S(2)}) collective-permute-start(bf16[6144,128]{1,0:T(8,128)(2,1)S(1)} %collective-permute-done.refs_0_), channel_id=1, source_target_pairs={{0,16},{16,0},{1,17},{17,1},{2,18},{18,2},{3,19},{19,3},{4,20},{20... | collective-permute-start | bytes 4718600 | tf_op jit(solution)/shard_map/ppermute | solution.py:251
  88.6 5.4 %copy-start = (s32[32,32]{1,0:T(8,128)S(1)}, s32[32,32]{1,0:T(8,128)}, u32[]{:S(2)}) copy-start(s32[32,32]{1,0:T(8,128)} %selected_ref.3) | copy-start | bytes 12292
  88.6 5.4 %copy-start.1 = (f32[32,32]{1,0:T(8,128)S(1)}, f32[32,32]{1,0:T(8,128)}, u32[]{:S(2)}) copy-start(f32[32,32]{1,0:T(8,128)} %affinity_ref.1) | copy-start | bytes 12292
  90.3 25.3 %all-to-all-start.3 = ((bf16[32,32,128]{2,1,0:T(8,128)(2,1)}), bf16[32,32,128]{2,1,0:T(8,128)(2,1)S(1)}, u32[]{:S(2)}, u32[]{:S(2)}) async-start(bf16[32,32,128]{2,1,0:T(8,128)(2,1)} %shard_map.68), calls=%async_computation.3 | async-start | bytes 524288 | tf_op jit(solution)/shard_map/all_to_all | solution.py:262
  115.9 5.9 %collective-permute-start.2 = (bf16[128,128]{1,0:T(8,128)(2,1)S(1)}, bf16[128,128]{1,0:T(8,128)(2,1)S(1)}, u32[]{:S(2)}, u32[]{:S(2)}) collective-permute-start(bf16[128,128]{1,0:T(8,128)(2,1)S(1)} %get-tuple-element.12), channel_id=1, source_target_pairs={{0,12},{12,0},{4,8},{8,4},{1,13},{13,1},{5,9},{9,5},{2,14},{14,2},... | collective-permute-start | bytes 98312 | tf_op jit(solution)/shard_map/ppermute | solution.py:270

commit v9 on v6

--- a/solution.py
+++ b/solution.py
@@ -14,7 +14,6 @@
 EMPTY = 64.0
 LIMIT = 32.0
 TRADE = [(0, 0), (1, 1), (6, 6), (7, 7), (4, 3), (3, 4), (5, 2), (2, 5)]
-PAIR = [(0, 3), (3, 0), (1, 2), (2, 1)]
 CORES = [(0, 1), (1, 0)]
 
 
@@ -82,13 +81,12 @@
         store.wait()
 
 
-def mix_kernel(place_ref, selected_ref, affinity_ref, mix_ref):
-    g, _, _ = whereabouts(place_ref)
+def mix_kernel(selected_ref, affinity_ref, mix_ref):
     experts, most = selected_ref.shape
     _, tok, slots = mix_ref.shape
     sel = selected_ref[...].astype(F32).astype(BF)
     tile = one_hot(iota((most, slots), 0) == iota((most, slots), 1) % most)
-    mine = iota((experts, slots), 0) == 2 * (iota((experts, slots), 1) // most) + g
+    mine = iota((experts, slots), 0) == iota((experts, slots), 1) // most
 
     def as_row(values):
         return jnp.sum(jnp.where(mine, dot(values, tile), 0.0), axis=0, keepdims=True)
@@ -101,7 +99,7 @@
     mix_ref[1] = jnp.where(hit, as_row(low), 0.0).astype(BF)
 
 
-def compact_kernel(slots_ref, rows_ref):
+def compact_kernel(slots_ref, rows_ref, counts_ref):
     blocks, most, width = slots_ref.shape
     cores, lines, peers, part, _ = rows_ref.shape
     slots = blocks * most
@@ -110,10 +108,11 @@
     live = one_hot(data.astype(F32) < LIMIT)
     first = one_hot(iota((8, width), 1) == 0)
     live_row = lax.dot_general(first, live, (((1,), (1,)), ((), ())), preferred_element_type=F32)
-    in_block = one_hot(iota((slots, blocks), 0) // most == iota((slots, blocks), 1))
-    before = one_hot(iota((blocks, slots), 0) < iota((blocks, slots), 1) // most)
-    counts = dot(live_row.astype(BF), in_block)
-    rank = dot(counts.astype(BF), before) + (iota((8, slots), 1) % most).astype(F32)
+    in_block = one_hot(iota((slots, width), 0) // most == iota((slots, width), 1))
+    before = one_hot(iota((width, slots), 0) < iota((width, slots), 1) // most)
+    counts = dot(live_row.astype(BF), in_block).astype(BF)
+    counts_ref[...] = jnp.broadcast_to(counts[0:1], counts_ref.shape)
+    rank = dot(counts, before) + (iota((8, slots), 1) % most).astype(F32)
     rank = jnp.where(live_row > 0.5, rank, -1.0)[0:1]
     take = one_hot(rank == iota((count, slots), 0).astype(F32))
     rows = dot(take, data).astype(BF)
@@ -149,37 +148,38 @@
             out_ref[seat(k + j, g)] = partial[:, j * span : (j + 1) * span]
 
 
-def expand_kernel(parts_ref, slots_ref, out_ref):
+def sum_kernel(parts_ref, out_ref):
     cores, lines, peers, part, width = parts_ref.shape
-    blocks, most, _ = slots_ref.shape
-    slots = blocks * most
-    halves = []
     for c in range(cores):
         total = jnp.zeros((part, width), F32)
         for k in range(lines):
             for x in range(peers):
                 total = total + parts_ref[c, k, x].astype(F32)
-        halves.append(total.astype(BF))
-    live = one_hot(slots_ref[...].reshape(slots, width).astype(F32) < LIMIT)
-    in_block = one_hot(iota((blocks, slots), 0) == iota((blocks, slots), 1) // most)
-    before = one_hot(iota((slots, blocks), 1) < iota((slots, blocks), 0) // most)
-    counts = dot(in_block, live).astype(BF)
-    rank = dot(before, counts) + (iota((slots, width), 0) % most).astype(F32)
-    rank = jnp.where(live > 0.5, rank, -1.0)
-    lanes = iota((slots, width), 1).astype(F32)
-    put = [one_hot(rank - k == lanes) for k in range(0, cores * part, width)]
-    rows = dot(jnp.concatenate(put, axis=1), jnp.concatenate(halves, axis=0)).astype(BF)
+        out_ref[c * part : (c + 1) * part] = total.astype(BF)
+
+
+def expand_kernel(rows_ref, counts_ref, out_ref):
+    count, width = rows_ref.shape
+    blocks, most, _ = out_ref.shape
+    slots = blocks * most
+    block = iota((slots, width), 0) // most
+    place = (iota((slots, width), 0) % most).astype(F32)
+
+    def spread(table):
+        dims = (((1,), (1,)), ((), ()))
+        return lax.dot_general(table, counts_ref[...], dims, preferred_element_type=F32)
+
+    lanes = iota((slots, width), 1)
+    rank = spread(one_hot(lanes < block)) + place
+    rank = jnp.where(place < spread(one_hot(lanes == block)), rank, -1.0)
+    put = [one_hot(rank - k == lanes.astype(F32)) for k in range(0, count, width)]
+    rows = dot(jnp.concatenate(put, axis=1), rows_ref[...]).astype(BF)
     out_ref[...] = rows.reshape(blocks, most, width)
 
 
-def combine_kernel(place_ref, mix_ref, rows_ref, keep_ref, send_ref):
-    here, cores, most, width = rows_ref.shape
-    both = [rows_ref[:, c].reshape(here * most, width) for c in range(cores)]
-    both = jnp.concatenate(both, axis=1)
-    total = dot(mix_ref[0], both) + dot(mix_ref[1], both)
-    mine = whereabouts(place_ref)[0] == 0
-    keep_ref[...] = jnp.where(mine, total[:, :width], total[:, width:])
-    send_ref[...] = jnp.where(mine, total[:, width:], total[:, :width]).astype(BF)
+def combine_kernel(mix_ref, rows_ref, out_ref):
+    rows = rows_ref[...]
+    out_ref[...] = (dot(mix_ref[0], rows) + dot(mix_ref[1], rows)).astype(BF)
 
 
 def local_call(kernel, outs, *args, place=None, params=(), hbm=(), scratch=()):
@@ -194,7 +194,9 @@
     return pl.pallas_call(
         kernel,
         in_specs=specs,
-        out_specs=jax.tree.map(lambda o: pl.BlockSpec(memory_space=o.memory_space), outs),
+        out_specs=jax.tree.map(
+            lambda o: pl.BlockSpec(memory_space=getattr(o, "memory_space", None)), outs
+        ),
         out_shape=outs,
         scratch_shapes=scratch,
         compiler_params=pltpu.CompilerParams(vmem_limit_bytes=24 * 2**20),
@@ -238,30 +240,30 @@
     arrived = lax.all_to_all(rows.reshape(ep, most, span), EP, 0, 0, tiled=True)
     mix = local_call(
         mix_kernel,
-        array((2, tok, layers * most)),
-        place=place,
+        array((2, tok, experts * most)),
         params=(selected, affinity),
     )
     other = lax.ppermute(mine, "c", CORES)
-    copies = local_call(compact_kernel, array((2, lines, peers, part, span)), arrived)
+    copies, counts = local_call(
+        compact_kernel, [array((2, lines, peers, part, span)), array((tok, span))], arrived
+    )
     chosen = lax.all_to_all(copies.reshape(team, part, span), TEAM, 0, 0, tiled=True)
+    counts = lax.ppermute(counts, ("c", "g", "yy"), TRADE)
+    chosen, counts = lax.optimization_barrier((chosen, counts))
     partial = local_call(ffn_kernel, array((team, part, span)), chosen, mine, other, place=place)
     summands = lax.all_to_all(partial, TEAM, 0, 0, tiled=True)
     result = local_call(
-        expand_kernel,
-        array((ep, most, span)),
-        summands.reshape(2, lines, peers, part, span),
-        arrived,
-    )
+        sum_kernel, array((2 * part, span)), summands.reshape(2, lines, peers, part, span)
+    )
+    result = lax.ppermute(result, ("c", "g", "yy"), TRADE)
+    result = local_call(expand_kernel, array((ep, most, span)), result, counts)
     returned = lax.all_to_all(result, EP, 0, 0, tiled=True)
-    keep, send = local_call(
+    return local_call(
         combine_kernel,
-        [array((tok, span), F32), array((tok, span))],
+        jax.ShapeDtypeStruct((tok, span), BF),
         mix,
-        returned.reshape(layers, 2, most, span),
-        place=place,
-    )
-    return (keep + lax.ppermute(send, ("g", "yy"), PAIR).astype(F32)).astype(BF)
+        returned.reshape(experts * most, span),
+    )
 
 
 def solution(mesh):

time: 124 us -> 127 us (1.024)
  blocking collectives: 40.2 us -> 19.2 us
  waiting for transfers between devices: 45.1 us -> 58.7 us
  starting transfers between devices: 29.4 us -> 37.7 us
  Pallas kernels: 7.63 us -> 9.64 us
    all_to_all x1 -> x0, blocking collectives: 21 us -> none  [per_device(): lax.all_to_all(copies.reshape(team, part, span), TEAM, 0, 0, tiled=True)]
    all_to_all x0 -> x1, waiting for transfers between devices: none -> 9.46 us  [per_device(): lax.all_to_all(copies.reshape(team, part, span), TEAM, 0, 0, tiled=True)]
    ppermute x1 -> x2, waiting for transfers between devices: 3.37 us -> 8.46 us  [the longest x1 5 us: per_device(): result = lax.ppermute(result, ('c', 'g', 'yy'), TRADE)]
    all_to_all x0 -> x1, starting transfers between devices: none -> 4.97 us  [per_device(): lax.all_to_all(copies.reshape(team, part, span), TEAM, 0, 0, tiled=True)]
    ppermute x1 -> x2, starting transfers between devices: 2.49 us -> 5.74 us  [the longest x1 3.25 us: per_device(): counts = lax.ppermute(counts, ('c', 'g', 'yy'), TRADE)]
    pallas_call x7 -> x8, Pallas kernels: 7.63 us -> 9.64 us  [local_call(): pl.pallas_call(kernel, in_specs=specs, out_specs=jax.tree.map(lambda o: p...]
  transfers between devices with their start and end apart: 5 -> 7, of which waited for: 4 -> 6; matrix products, arithmetic and copies ran while one was open for 0% -> 0% of each run, Pallas kernels for 3% -> 3%
where the time goes in v9:
time: 127 us; the launch traced here: 126 us
  waiting for transfers between devices  58.7 us (46%)
  starting transfers between devices  37.7 us (30%)
  blocking collectives  19.2 us (15%)
  Pallas kernels  9.64 us (8%)
    all_to_all x1, waiting for transfers between devices, per_device(): returned = lax.all_to_all(result, EP, 0, 0, tiled=True)  20.5 us
    all_to_all x1, waiting for transfers between devices, per_device(): arrived = lax.all_to_all(rows.reshape(ep, most, span), EP, 0, 0, tiled=True)  19.8 us
    all_to_all x1, blocking collectives, per_device(): summands = lax.all_to_all(partial, TEAM, 0, 0, tiled=True)  19.2 us
    all_to_all x1, starting transfers between devices, per_device(): arrived = lax.all_to_all(rows.reshape(ep, most, span), EP, 0, 0, tiled=True)  15.4 us
    pallas_call x8, Pallas kernels, local_call(): pl.pallas_call(kernel, in_specs=specs, out_specs=jax.tree.map(lambda o: p...  9.64 us
    all_to_all x1, waiting for transfers between devices, per_device(): lax.all_to_all(copies.reshape(team, part, span), TEAM, 0, 0, tiled=True)  9.46 us
    ppermute x1, starting transfers between devices, per_device(): mine = lax.ppermute(packed, ('c', 'g', 'yy'), TRADE)  6.02 us
    ppermute x1, waiting for transfers between devices, per_device(): result = lax.ppermute(result, ('c', 'g', 'yy'), TRADE)  5 us
  transfers between devices with their start and end apart: 7, of which 6 were waited for; matrix products, arithmetic and copies ran while one was open for 0% of the time, Pallas kernels for 3%

profile of v9, /device:TPU:1, one launch (start us, length us, event | category | flops | bytes accessed | tf_op | source)
XLA Modules:
  0.0 126.3 jit_solution(6611619342436941668)
XLA Ops:
  0.0 1.4 %shard_map.67 = bf16[6144,128]{1,0:T(8,128)(2,1)S(1)} custom-call(bf16[1,2048,128]{2,1,0:T(8,128)(2,1)} %gate_ref.1, bf16[1,2048,128]{2,1,0:T(8,128)(2,1)} %up_ref.1, bf16[1,128,2048]{2,1,0:T(8,128)(2,1)} %down_ref.1), custom_call_target="tpu_custom_call" | custom-call | tf_op jit(solution)/shard_map/pallas_call | solution.py:194
  1.4 6.0 %collective-permute-start.1 = (bf16[6144,128]{1,0:T(8,128)(2,1)S(1)}, bf16[6144,128]{1,0:T(8,128)(2,1)S(1)}, u32[]{:S(2)}, u32[]{:S(2)}) collective-permute-start(bf16[6144,128]{1,0:T(8,128)(2,1)S(1)} %shard_map.67), channel_id=1, source_target_pairs={{0,0},{4,4},{24,24},{28,28},{16,12},{12,16},{20,8},{8,20},{1,1},{5... | collective-permute-start | bytes 4718600 | tf_op jit(solution)/shard_map/ppermute | solution.py:227
  7.5 2.1 %shard_map.65 = bf16[16,2,32,128]{3,2,1,0:T(8,128)(2,1)} custom-call(s32[1]{0:T(128)} %bitcast.place_ref, s32[32,32]{1,0:T(8,128)} %selected_ref.3, bf16[128,2048]{1,0:T(8,128)(2,1)} %tokens_ref.1), custom_call_target="tpu_custom_call" | custom-call | tf_op jit(solution)/shard_map/pallas_call | solution.py:194
  9.6 15.4 %all-to-all-start = ((bf16[32,32,128]{2,1,0:T(8,128)(2,1)}), bf16[32,32,128]{2,1,0:T(8,128)(2,1)S(1)}, u32[]{:S(2)}, u32[]{:S(2)}) async-start(bf16[32,32,128]{2,1,0:T(8,128)(2,1)} %bitcast.8), calls=%async_computation | async-start | bytes 524288 | tf_op jit(solution)/shard_map/all_to_all | solution.py:240
  25.0 0.5 collective-permute-done.1.refs_0_
  25.5 1.9 %collective-permute-start.2 = (bf16[6144,128]{1,0:T(8,128)(2,1)S(1)}, bf16[6144,128]{1,0:T(8,128)(2,1)}, u32[]{:S(2)}, u32[]{:S(2)}) collective-permute-start(bf16[6144,128]{1,0:T(8,128)(2,1)S(1)} %collective-permute-done.1.refs_0_), channel_id=1, source_target_pairs={{0,16},{16,0},{1,17},{17,1},{2,18},{18,2},{3,19},{19,3},{4,20},{20... | collective-permute-start | bytes 4718600 | tf_op jit(solution)/shard_map/ppermute | solution.py:246
  27.5 19.8 %all-to-all-done.slots_ref = bf16[32,32,128]{2,1,0:T(8,128)(2,1)S(1)} async-done(((bf16[32,32,128]{2,1,0:T(8,128)(2,1)}), bf16[32,32,128]{2,1,0:T(8,128)(2,1)S(1)}, u32[]{:S(2)}, u32[]{:S(2)}) %all-to-all-start) | async-done | bytes 262176 | tf_op jit(solution)/shard_map/all_to_all | solution.py:240
  47.3 0.8 shard_map.66
  48.1 0.0 copy-start
  48.1 1.0 copy-done
  49.1 5.0 %all-to-all-start.1 = ((bf16[16,256,128]{2,1,0:T(8,128)(2,1)}), bf16[16,256,128]{2,1,0:T(8,128)(2,1)S(1)}, u32[]{:S(2)}, u32[]{:S(2)}) async-start(bf16[16,256,128]{2,1,0:T(8,128)(2,1)} %bitcast.7), calls=%async_computation.1 | async-start | bytes 2097152 | tf_op jit(solution)/shard_map/all_to_all | solution.py:250
  54.0 3.3 %collective-permute-start = (bf16[128,128]{1,0:T(8,128)(2,1)S(1)}, bf16[128,128]{1,0:T(8,128)(2,1)S(1)}, u32[]{:S(2)}, u32[]{:S(2)}) collective-permute-start(bf16[128,128]{1,0:T(8,128)(2,1)S(1)} %get-tuple-element.10), channel_id=1, source_target_pairs={{0,0},{4,4},{24,24},{28,28},{16,12},{12,16},{20,8},{8,20},{1,1},{5... | collective-permute-start | bytes 98312 | tf_op jit(solution)/shard_map/ppermute | solution.py:251
  57.3 3.5 %collective-permute-done.counts_ref = bf16[128,128]{1,0:T(8,128)(2,1)S(1)} collective-permute-done((bf16[128,128]{1,0:T(8,128)(2,1)S(1)}, bf16[128,128]{1,0:T(8,128)(2,1)S(1)}, u32[]{:S(2)}, u32[]{:S(2)}) %collective-permute-start) | collective-permute-done | bytes 32800 | tf_op jit(solution)/shard_map/ppermute | solution.py:251
  60.8 9.5 %all-to-all-done.1.x_ref = bf16[16,256,128]{2,1,0:T(8,128)(2,1)S(1)} async-done(((bf16[16,256,128]{2,1,0:T(8,128)(2,1)}), bf16[16,256,128]{2,1,0:T(8,128)(2,1)S(1)}, u32[]{:S(2)}, u32[]{:S(2)}) %all-to-all-start.1) | async-done | bytes 1048608 | tf_op jit(solution)/shard_map/all_to_all | solution.py:250
  70.2 0.0 collective-permute-done.2.refs_1_
  70.2 2.5 %shard_map.68 = bf16[16,256,128]{2,1,0:T(8,128)(2,1)S(1)} custom-call(s32[1]{0:T(128)} %bitcast.place_ref, bf16[16,256,128]{2,1,0:T(8,128)(2,1)S(1)} %all-to-all-done.1.x_ref, bf16[6144,128]{1,0:T(8,128)(2,1)S(1)} %collective-permute-done.1.refs_0_, bf16[6144,128]{1,0:T(8,128)(2,1)} %collective-permute-done.2.refs_1_), custom_call_target="tpu_custom_call" | custom-call | tf_op jit(solution)/shard_map/pallas_call | solution.py:194
  72.7 19.2 %all_to_all.20 = bf16[16,256,128]{2,1,0:T(8,128)(2,1)S(1)} all-to-all(bf16[16,256,128]{2,1,0:T(8,128)(2,1)S(1)} %shard_map.68), channel_id=1, replica_groups=mesh['z'=16,'c'=2,'g'=2,'yy'=2,'x'=4] {'c','yy','x'}, dimensions={0} | all-to-all | bytes 2097152 | tf_op jit(solution)/shard_map/all_to_all | solution.py:254
  91.9 0.0 copy-start.1
  91.9 0.0 copy-start.2
  91.9 0.1 shard_map.69
  92.0 2.5 %collective-permute-start.3 = (bf16[512,128]{1,0:T(8,128)(2,1)S(1)}, bf16[512,128]{1,0:T(8,128)(2,1)S(1)}, u32[]{:S(2)}, u32[]{:S(2)}) collective-permute-start(bf16[512,128]{1,0:T(8,128)(2,1)S(1)} %shard_map.69), channel_id=1, source_target_pairs={{0,0},{4,4},{24,24},{28,28},{16,12},{12,16},{20,8},{8,20},{1,1},{5... | collective-permute-start | bytes 393224 | tf_op jit(solution)/shard_map/ppermute | solution.py:258
  94.5 5.0 %collective-permute-done.3.rows_ref = bf16[512,128]{1,0:T(8,128)(2,1)S(1)} collective-permute-done((bf16[512,128]{1,0:T(8,128)(2,1)S(1)}, bf16[512,128]{1,0:T(8,128)(2,1)S(1)}, u32[]{:S(2)}, u32[]{:S(2)}) %collective-permute-start.3) | collective-permute-done | bytes 131104 | tf_op jit(solution)/shard_map/ppermute | solution.py:258
  99.5 1.4 %shard_map.70 = bf16[32,32,128]{2,1,0:T(8,128)(2,1)} custom-call(bf16[512,128]{1,0:T(8,128)(2,1)S(1)} %collective-permute-done.3.rows_ref, bf16[128,128]{1,0:T(8,128)(2,1)S(1)} %collective-permute-done.counts_ref), custom_call_target="tpu_custom_call" | custom-call | tf_op jit(solution)/shard_map/pallas_call | solution.py:194
  101.0 3.7 %all-to-all-start.3 = ((bf16[32,32,128]{2,1,0:T(8,128)(2,1)}), bf16[32,32,128]{2,1,0:T(8,128)(2,1)S(1)}, u32[]{:S(2)}, u32[]{:S(2)}) async-start(bf16[32,32,128]{2,1,0:T(8,128)(2,1)} %shard_map.70), calls=%async_computation.3 | async-start | bytes 524288 | tf_op jit(solution)/shard_map/all_to_all | solution.py:260
  104.6 0.0 copy-done.1
  104.6 0.0 copy-done.2
  104.7 0.3 shard_map.64.mix_ref
  105.0 20.5 %all-to-all-done.3 = bf16[32,32,128]{2,1,0:T(8,128)(2,1)S(1)} async-done(((bf16[32,32,128]{2,1,0:T(8,128)(2,1)}), bf16[32,32,128]{2,1,0:T(8,128)(2,1)S(1)}, u32[]{:S(2)}, u32[]{:S(2)}) %all-to-all-start.3) | async-done | bytes 262176 | tf_op jit(solution)/shard_map/all_to_all | solution.py:260
  125.4 0.9 shard_map.71
Async XLA Ops:
  1.4 24.1 %collective-permute-start.1 = (bf16[6144,128]{1,0:T(8,128)(2,1)S(1)}, bf16[6144,128]{1,0:T(8,128)(2,1)S(1)}, u32[]{:S(2)}, u32[]{:S(2)}) collective-permute-start(bf16[6144,128]{1,0:T(8,128)(2,1)S(1)} %shard_map.67), channel_id=1, source_target_pairs={{0,0},{4,4},{24,24},{28,28},{16,12},{12,16},{20,8},{8,20},{1,1},{5... | collective-permute-start | bytes 4718600 | tf_op jit(solution)/shard_map/ppermute | solution.py:227
  9.6 37.6 %all-to-all-start = ((bf16[32,32,128]{2,1,0:T(8,128)(2,1)}), bf16[32,32,128]{2,1,0:T(8,128)(2,1)S(1)}, u32[]{:S(2)}, u32[]{:S(2)}) async-start(bf16[32,32,128]{2,1,0:T(8,128)(2,1)} %bitcast.8), calls=%async_computation | async-start | bytes 524288 | tf_op jit(solution)/shard_map/all_to_all | solution.py:240
  25.5 44.7 %collective-permute-start.2 = (bf16[6144,128]{1,0:T(8,128)(2,1)S(1)}, bf16[6144,128]{1,0:T(8,128)(2,1)}, u32[]{:S(2)}, u32[]{:S(2)}) collective-permute-start(bf16[6144,128]{1,0:T(8,128)(2,1)S(1)} %collective-permute-done.1.refs_0_), channel_id=1, source_target_pairs={{0,16},{16,0},{1,17},{17,1},{2,18},{18,2},{3,19},{19,3},{4,20},{20... | collective-permute-start | bytes 4718600 | tf_op jit(solution)/shard_map/ppermute | solution.py:246
  48.1 1.0 copy-start
  49.1 21.2 %all-to-all-start.1 = ((bf16[16,256,128]{2,1,0:T(8,128)(2,1)}), bf16[16,256,128]{2,1,0:T(8,128)(2,1)S(1)}, u32[]{:S(2)}, u32[]{:S(2)}) async-start(bf16[16,256,128]{2,1,0:T(8,128)(2,1)} %bitcast.7), calls=%async_computation.1 | async-start | bytes 2097152 | tf_op jit(solution)/shard_map/all_to_all | solution.py:250
  54.0 6.7 %collective-permute-start = (bf16[128,128]{1,0:T(8,128)(2,1)S(1)}, bf16[128,128]{1,0:T(8,128)(2,1)S(1)}, u32[]{:S(2)}, u32[]{:S(2)}) collective-permute-start(bf16[128,128]{1,0:T(8,128)(2,1)S(1)} %get-tuple-element.10), channel_id=1, source_target_pairs={{0,0},{4,4},{24,24},{28,28},{16,12},{12,16},{20,8},{8,20},{1,1},{5... | collective-permute-start | bytes 98312 | tf_op jit(solution)/shard_map/ppermute | solution.py:251
  91.9 12.7 %copy-start.1 = (s32[32,32]{1,0:T(8,128)S(1)}, s32[32,32]{1,0:T(8,128)}, u32[]{:S(2)}) copy-start(s32[32,32]{1,0:T(8,128)} %selected_ref.3) | copy-start | bytes 12292
  91.9 12.7 %copy-start.2 = (f32[32,32]{1,0:T(8,128)S(1)}, f32[32,32]{1,0:T(8,128)}, u32[]{:S(2)}) copy-start(f32[32,32]{1,0:T(8,128)} %affinity_ref.1) | copy-start | bytes 12292
  92.0 7.5 %collective-permute-start.3 = (bf16[512,128]{1,0:T(8,128)(2,1)S(1)}, bf16[512,128]{1,0:T(8,128)(2,1)S(1)}, u32[]{:S(2)}, u32[]{:S(2)}) collective-permute-start(bf16[512,128]{1,0:T(8,128)(2,1)S(1)} %shard_map.69), channel_id=1, source_target_pairs={{0,0},{4,4},{24,24},{28,28},{16,12},{12,16},{20,8},{8,20},{1,1},{5... | collective-permute-start | bytes 393224 | tf_op jit(solution)/shard_map/ppermute | solution.py:258
  101.0 24.5 %all-to-all-start.3 = ((bf16[32,32,128]{2,1,0:T(8,128)(2,1)}), bf16[32,32,128]{2,1,0:T(8,128)(2,1)S(1)}, u32[]{:S(2)}, u32[]{:S(2)}) async-start(bf16[32,32,128]{2,1,0:T(8,128)(2,1)} %shard_map.70), calls=%async_computation.3 | async-start | bytes 524288 | tf_op jit(solution)/shard_map/all_to_all | solution.py:260

commit v10 on v6

--- a/solution.py
+++ b/solution.py
@@ -14,7 +14,6 @@
 EMPTY = 64.0
 LIMIT = 32.0
 TRADE = [(0, 0), (1, 1), (6, 6), (7, 7), (4, 3), (3, 4), (5, 2), (2, 5)]
-PAIR = [(0, 3), (3, 0), (1, 2), (2, 1)]
 CORES = [(0, 1), (1, 0)]
 
 
@@ -28,11 +27,6 @@
 
 def one_hot(mask):
     return jnp.where(mask, 1.0, 0.0).astype(BF)
-
-
-def whereabouts(place_ref):
-    place = place_ref[0]
-    return place // 8, place // 4, place % 4
 
 
 def pack_kernel(gate_ref, up_ref, down_ref, out_ref, sems):
@@ -49,15 +43,14 @@
 
 
 def pick_kernel(place_ref, selected_ref, tokens_ref, rows_ref, sel_ref, tile_ref, out_ref, sems):
-    g, y, x = whereabouts(place_ref)
+    g = place_ref[0] // 8
     experts, most = selected_ref.shape
     _, tok, width = tile_ref.shape
     first = pltpu.make_async_copy(selected_ref, sel_ref, sems.at[4])
     first.start()
     loads = []
     for c in range(2):
-        block = 4 * ((jnp.minimum, jnp.maximum)[c](y, 3 - y)) + x
-        at = pl.multiple_of(block * width, width)
+        at = pl.multiple_of((8 * c + place_ref[0] % 8) * width, width)
         loads.append(
             pltpu.make_async_copy(tokens_ref.at[:, pl.ds(at, width)], tile_ref.at[c], sems.at[c])
         )
@@ -82,23 +75,25 @@
         store.wait()
 
 
-def mix_kernel(place_ref, selected_ref, affinity_ref, mix_ref):
-    g, _, _ = whereabouts(place_ref)
+def mix_kernel(selected_ref, affinity_ref, mix_ref):
     experts, most = selected_ref.shape
-    _, tok, slots = mix_ref.shape
+    _, _, tok, slots = mix_ref.shape
+    part = most // 2
+    mine = iota((experts, slots), 0) == iota((experts, slots), 1) // part
     sel = selected_ref[...].astype(F32).astype(BF)
-    tile = one_hot(iota((most, slots), 0) == iota((most, slots), 1) % most)
-    mine = iota((experts, slots), 0) == 2 * (iota((experts, slots), 1) // most) + g
-
-    def as_row(values):
-        return jnp.sum(jnp.where(mine, dot(values, tile), 0.0), axis=0, keepdims=True)
-
     aff = affinity_ref[...]
     high = aff.astype(BF)
     low = (aff - high.astype(F32)).astype(BF)
-    hit = as_row(sel) == iota((tok, slots), 0).astype(F32)
-    mix_ref[0] = jnp.where(hit, as_row(high), 0.0).astype(BF)
-    mix_ref[1] = jnp.where(hit, as_row(low), 0.0).astype(BF)
+    for half in range(2):
+        wanted = iota((most, slots), 1) % part + half * part
+        tile = one_hot(iota((most, slots), 0) == wanted)
+
+        def as_row(values):
+            return jnp.sum(jnp.where(mine, dot(values, tile), 0.0), axis=0, keepdims=True)
+
+        hit = as_row(sel) == iota((tok, slots), 0).astype(F32)
+        mix_ref[half, 0] = jnp.where(hit, as_row(high), 0.0).astype(BF)
+        mix_ref[half, 1] = jnp.where(hit, as_row(low), 0.0).astype(BF)
 
 
 def compact_kernel(slots_ref, rows_ref):
@@ -123,30 +118,33 @@
                 rows_ref[c, k, x] = rows[c * part : (c + 1) * part]
 
 
-def seat(block, g):
-    y = block // 4
-    yy = (0, 1, 1, 0)[y]
-    return (y // 2) * 8 + 4 * (yy + g - 2 * yy * g) + block % 4
-
-
-def ffn_kernel(place_ref, x_ref, *refs):
+def turned(x):
+    half = x.shape[1] // 2
+    return jnp.concatenate([x[:, half:], x[:, :half]], axis=1)
+
+
+def joined(left, right):
+    return jnp.where(iota(left.shape, 1) < left.shape[1] // 2, left, right)
+
+
+def ffn_kernel(x_ref, *refs):
     *weights, out_ref = refs
-    g, _, _ = whereabouts(place_ref)
     peers, _, span = x_ref.shape
     width = peers * span
-    x = jnp.concatenate([x_ref[seat(k, g)] for k in range(peers)], axis=1)
+    x = jnp.concatenate([x_ref[k] for k in range(peers)], axis=1)
     gate = dot(x, jnp.concatenate([w[:width] for w in weights], axis=1))
     up = dot(x, jnp.concatenate([w[width : 2 * width] for w in weights], axis=1))
     hidden = (gate / (1.0 + jnp.exp(-gate)) * up).astype(BF)
-    for k in range(0, peers, 2):
-        at = 2 * width + k * span
-        tiles = [
-            jnp.concatenate([w[at + j * span : at + (j + 1) * span] for w in weights], axis=0)
-            for j in range(2)
-        ]
-        partial = dot(hidden, jnp.concatenate(tiles, axis=1)).astype(BF)
-        for j in range(2):
-            out_ref[seat(k + j, g)] = partial[:, j * span : (j + 1) * span]
+    half = peers // 2
+    for k in range(half):
+        tiles = []
+        for block in (k, k + half):
+            at = 2 * width + block * span
+            tiles.append(jnp.concatenate([w[at : at + span] for w in weights], axis=0))
+        both = dot(hidden, jnp.concatenate(tiles, axis=1))
+        low, high = both[:, :span], both[:, span:]
+        out_ref[k] = joined(low, turned(high)).astype(BF)
+        out_ref[k + half] = joined(turned(low), high).astype(BF)
 
 
 def expand_kernel(parts_ref, slots_ref, out_ref):
@@ -159,27 +157,43 @@
         for k in range(lines):
             for x in range(peers):
                 total = total + parts_ref[c, k, x].astype(F32)
-        halves.append(total.astype(BF))
+        halves.append(total)
+    rows = jnp.concatenate(halves, axis=0)
+    rows = jnp.concatenate([rows, turned(rows)], axis=1).astype(BF)
     live = one_hot(slots_ref[...].reshape(slots, width).astype(F32) < LIMIT)
     in_block = one_hot(iota((blocks, slots), 0) == iota((blocks, slots), 1) // most)
-    before = one_hot(iota((slots, blocks), 1) < iota((slots, blocks), 0) // most)
     counts = dot(in_block, live).astype(BF)
-    rank = dot(before, counts) + (iota((slots, width), 0) % most).astype(F32)
-    rank = jnp.where(live > 0.5, rank, -1.0)
-    lanes = iota((slots, width), 1).astype(F32)
-    put = [one_hot(rank - k == lanes) for k in range(0, cores * part, width)]
-    rows = dot(jnp.concatenate(put, axis=1), jnp.concatenate(halves, axis=0)).astype(BF)
-    out_ref[...] = rows.reshape(blocks, most, width)
-
-
-def combine_kernel(place_ref, mix_ref, rows_ref, keep_ref, send_ref):
-    here, cores, most, width = rows_ref.shape
-    both = [rows_ref[:, c].reshape(here * most, width) for c in range(cores)]
+    few = slots // 2
+    step = most // 2
+    block = iota((few, blocks), 0) // step
+    before = dot(one_hot(iota((few, blocks), 1) < block), counts)
+    count = dot(one_hot(iota((few, blocks), 1) == block), counts)
+    lanes = iota((few, width), 1).astype(F32)
+    found = []
+    for half in range(2):
+        place = (iota((few, width), 0) % step + half * step).astype(F32)
+        rank = jnp.where(place < count, before + place, -1.0)
+        put = [one_hot(rank - k == lanes) for k in range(0, cores * part, width)]
+        found.append(dot(jnp.concatenate(put, axis=1), rows))
+    first, second = found
+    for g in range(2):
+        straight, swapped = (slice(0, width), slice(width, 2 * width))
+        if g == 0:
+            out = joined(first[:, straight], second[:, swapped])
+        else:
+            out = joined(first[:, swapped], second[:, straight])
+        out_ref[:, g] = out.astype(BF).reshape(blocks, step, width)
+
+
+def combine_kernel(mix_ref, rows_ref, out_ref):
+    layers, cores, teams, step, width = rows_ref.shape
+    both = [rows_ref[:, c].reshape(layers * teams * step, width) for c in range(cores)]
     both = jnp.concatenate(both, axis=1)
-    total = dot(mix_ref[0], both) + dot(mix_ref[1], both)
-    mine = whereabouts(place_ref)[0] == 0
-    keep_ref[...] = jnp.where(mine, total[:, :width], total[:, width:])
-    send_ref[...] = jnp.where(mine, total[:, width:], total[:, :width]).astype(BF)
+    first = dot(mix_ref[0, 0], both) + dot(mix_ref[0, 1], both)
+    second = dot(mix_ref[1, 0], both) + dot(mix_ref[1, 1], both)
+    low = first[:, :width] + turned(second[:, :width])
+    high = turned(first[:, width:]) + second[:, width:]
+    out_ref[...] = joined(low, high).astype(BF)
 
 
 def local_call(kernel, outs, *args, place=None, params=(), hbm=(), scratch=()):
@@ -194,7 +208,9 @@
     return pl.pallas_call(
         kernel,
         in_specs=specs,
-        out_specs=jax.tree.map(lambda o: pl.BlockSpec(memory_space=o.memory_space), outs),
+        out_specs=jax.tree.map(
+            lambda o: pl.BlockSpec(memory_space=getattr(o, "memory_space", None)), outs
+        ),
         out_shape=outs,
         scratch_shapes=scratch,
         compiler_params=pltpu.CompilerParams(vmem_limit_bytes=24 * 2**20),
@@ -238,30 +254,35 @@
     arrived = lax.all_to_all(rows.reshape(ep, most, span), EP, 0, 0, tiled=True)
     mix = local_call(
         mix_kernel,
-        array((2, tok, layers * most)),
-        place=place,
+        array((2, 2, tok, experts * most // 2)),
         params=(selected, affinity),
     )
     other = lax.ppermute(mine, "c", CORES)
     copies = local_call(compact_kernel, array((2, lines, peers, part, span)), arrived)
     chosen = lax.all_to_all(copies.reshape(team, part, span), TEAM, 0, 0, tiled=True)
-    partial = local_call(ffn_kernel, array((team, part, span)), chosen, mine, other, place=place)
+    partial = local_call(
+        ffn_kernel,
+        array((team, part, span)),
+        chosen,
+        mine,
+        other,
+    )
     summands = lax.all_to_all(partial, TEAM, 0, 0, tiled=True)
     result = local_call(
         expand_kernel,
-        array((ep, most, span)),
+        array((ep, 2, most // 2, span)),
         summands.reshape(2, lines, peers, part, span),
         arrived,
     )
-    returned = lax.all_to_all(result, EP, 0, 0, tiled=True)
-    keep, send = local_call(
+    returned = lax.all_to_all(
+        result.reshape(2 * ep, most // 2, span), ("z", "c", "g"), 0, 0, tiled=True
+    )
+    return local_call(
         combine_kernel,
-        [array((tok, span), F32), array((tok, span))],
+        jax.ShapeDtypeStruct((tok, span), BF),
         mix,
-        returned.reshape(layers, 2, most, span),
-        place=place,
-    )
-    return (keep + lax.ppermute(send, ("g", "yy"), PAIR).astype(F32)).astype(BF)
+        returned.reshape(layers, 2, 2, most // 2, span),
+    )
 
 
 def solution(mesh):

time: 124 us -> 119 us (0.960)
  waiting for transfers between devices: 45.1 us -> 42.7 us
  starting transfers between devices: 29.4 us -> 27.5 us
    ppermute x1 -> x0, waiting for transfers between devices: 3.37 us -> none  [per_device(): return (keep + lax.ppermute(send, ('g', 'yy'), PAIR).astype(F32)).astype(BF)]
    ppermute x1 -> x0, starting transfers between devices: 2.49 us -> none  [per_device(): return (keep + lax.ppermute(send, ('g', 'yy'), PAIR).astype(F32)).astype(BF)]
  transfers between devices with their start and end apart: 5 -> 4, of which waited for: 4 -> 3; matrix products, arithmetic and copies ran while one was open for 0% -> 0% of each run, Pallas kernels for 3% -> 3%
where the time goes in v10:
time: 119 us
  waiting for transfers between devices  42.7 us (36%)
  blocking collectives  40.2 us (34%)
  starting transfers between devices  27.5 us (23%)
  Pallas kernels  8.26 us (7%)
    all_to_all x1, waiting for transfers between devices, per_device(): lax.all_to_all(result.reshape(2 * ep, most // 2, span), ('z', 'c', 'g'),...  22.3 us
    all_to_all x1, blocking collectives, per_device(): lax.all_to_all(copies.reshape(team, part, span), TEAM, 0, 0, tiled=True)  21 us
    all_to_all x1, waiting for transfers between devices, per_device(): arrived = lax.all_to_all(rows.reshape(ep, most, span), EP, 0, 0, tiled=True)  19.8 us
    all_to_all x1, blocking collectives, per_device(): summands = lax.all_to_all(partial, TEAM, 0, 0, tiled=True)  19.2 us
    all_to_all x1, starting transfers between devices, per_device(): arrived = lax.all_to_all(rows.reshape(ep, most, span), EP, 0, 0, tiled=True)  15.4 us
    pallas_call x7, Pallas kernels, local_call(): pl.pallas_call(kernel, in_specs=specs, out_specs=jax.tree.map(lambda o: p...  8.26 us
    ppermute x1, starting transfers between devices, per_device(): mine = lax.ppermute(packed, ('c', 'g', 'yy'), TRADE)  6.02 us
    all_to_all x1, starting transfers between devices, per_device(): lax.all_to_all(result.reshape(2 * ep, most // 2, span), ('z', 'c', 'g'),...  4.18 us
  transfers between devices with their start and end apart: 4, of which 3 were waited for; matrix products, arithmetic and copies ran while one was open for 0% of the time, Pallas kernels for 3%

profile of v10, /device:TPU:1, one launch (start us, length us, event | category | flops | bytes accessed | tf_op | source)
XLA Modules:
  0.0 118.7 jit_solution(16144159669829744419)
XLA Ops:
  0.0 1.4 %shard_map.67 = bf16[6144,128]{1,0:T(8,128)(2,1)S(1)} custom-call(bf16[1,2048,128]{2,1,0:T(8,128)(2,1)} %gate_ref.1, bf16[1,2048,128]{2,1,0:T(8,128)(2,1)} %up_ref.1, bf16[1,128,2048]{2,1,0:T(8,128)(2,1)} %down_ref.1), custom_call_target="tpu_custom_call" | custom-call | tf_op jit(solution)/shard_map/pallas_call | solution.py:208
  1.4 6.0 %collective-permute-start = (bf16[6144,128]{1,0:T(8,128)(2,1)S(1)}, bf16[6144,128]{1,0:T(8,128)(2,1)S(1)}, u32[]{:S(2)}, u32[]{:S(2)}) collective-permute-start(bf16[6144,128]{1,0:T(8,128)(2,1)S(1)} %shard_map.67), channel_id=1, source_target_pairs={{0,0},{4,4},{24,24},{28,28},{16,12},{12,16},{20,8},{8,20},{1,1},{5... | collective-permute-start | bytes 4718600 | tf_op jit(solution)/shard_map/ppermute | solution.py:241
  7.5 2.1 %shard_map.65 = bf16[16,2,32,128]{3,2,1,0:T(8,128)(2,1)} custom-call(s32[1]{0:T(128)} %bitcast.place_ref, s32[32,32]{1,0:T(8,128)} %selected_ref.3, bf16[128,2048]{1,0:T(8,128)(2,1)} %tokens_ref.1), custom_call_target="tpu_custom_call" | custom-call | tf_op jit(solution)/shard_map/pallas_call | solution.py:208
  9.6 15.4 %all-to-all-start = ((bf16[32,32,128]{2,1,0:T(8,128)(2,1)}), bf16[32,32,128]{2,1,0:T(8,128)(2,1)S(1)}, u32[]{:S(2)}, u32[]{:S(2)}) async-start(bf16[32,32,128]{2,1,0:T(8,128)(2,1)} %bitcast.9), calls=%async_computation | async-start | bytes 524288 | tf_op jit(solution)/shard_map/all_to_all | solution.py:254
  25.0 0.5 collective-permute-done.refs_0_
  25.5 1.9 %collective-permute-start.1 = (bf16[6144,128]{1,0:T(8,128)(2,1)S(1)}, bf16[6144,128]{1,0:T(8,128)(2,1)S(1)}, u32[]{:S(2)}, u32[]{:S(2)}) collective-permute-start(bf16[6144,128]{1,0:T(8,128)(2,1)S(1)} %collective-permute-done.refs_0_), channel_id=1, source_target_pairs={{0,16},{16,0},{1,17},{17,1},{2,18},{18,2},{3,19},{19,3},{4,20},{20... | collective-permute-start | bytes 4718600 | tf_op jit(solution)/shard_map/ppermute | solution.py:260
  27.5 19.8 %all-to-all-done.slots_ref = bf16[32,32,128]{2,1,0:T(8,128)(2,1)S(1)} async-done(((bf16[32,32,128]{2,1,0:T(8,128)(2,1)}), bf16[32,32,128]{2,1,0:T(8,128)(2,1)S(1)}, u32[]{:S(2)}, u32[]{:S(2)}) %all-to-all-start) | async-done | bytes 262176 | tf_op jit(solution)/shard_map/all_to_all | solution.py:254
  47.3 0.8 shard_map.66
  48.1 21.0 %all_to_all.20.x_ref = bf16[16,256,128]{2,1,0:T(8,128)(2,1)S(1)} all-to-all(bf16[16,256,128]{2,1,0:T(8,128)(2,1)S(1)} %bitcast.6), channel_id=1, replica_groups=mesh['z'=16,'c'=2,'g'=2,'yy'=2,'x'=4] {'c','yy','x'}, dimensions={0} | all-to-all | bytes 2097152 | tf_op jit(solution)/shard_map/all_to_all | solution.py:262
  69.1 0.0 collective-permute-done.1.refs_1_
  69.1 1.2 shard_map.68
  70.3 19.2 %all_to_all.21 = bf16[16,256,128]{2,1,0:T(8,128)(2,1)S(1)} all-to-all(bf16[16,256,128]{2,1,0:T(8,128)(2,1)S(1)} %shard_map.68), channel_id=1, replica_groups=mesh['z'=16,'c'=2,'g'=2,'yy'=2,'x'=4] {'c','yy','x'}, dimensions={0} | all-to-all | bytes 2097152 | tf_op jit(solution)/shard_map/all_to_all | solution.py:270
  89.4 0.0 copy-start
  89.4 0.0 copy-start.1
  89.4 1.5 %shard_map.69 = bf16[32,2,16,128]{3,2,1,0:T(8,128)(2,1)} custom-call(bf16[2,2,4,256,128]{4,3,2,1,0:T(8,128)(2,1)S(1)} %bitcast.7, bf16[32,32,128]{2,1,0:T(8,128)(2,1)S(1)} %all-to-all-done.slots_ref), custom_call_target="tpu_custom_call" | custom-call | tf_op jit(solution)/shard_map/pallas_call | solution.py:208
  90.9 4.2 %all-to-all-start.3 = ((bf16[64,16,128]{2,1,0:T(8,128)(2,1)}), bf16[64,16,128]{2,1,0:T(8,128)(2,1)S(1)}, u32[]{:S(2)}, u32[]{:S(2)}) async-start(bf16[64,16,128]{2,1,0:T(8,128)(2,1)} %bitcast.4), calls=%async_computation.3 | async-start | bytes 524288 | tf_op jit(solution)/shard_map/all_to_all | solution.py:277
  95.1 0.0 copy-done
  95.1 0.0 copy-done.1
  95.1 0.3 shard_map.64.mix_ref
  95.4 22.3 %all-to-all-done.3 = bf16[64,16,128]{2,1,0:T(8,128)(2,1)S(1)} async-done(((bf16[64,16,128]{2,1,0:T(8,128)(2,1)}), bf16[64,16,128]{2,1,0:T(8,128)(2,1)S(1)}, u32[]{:S(2)}, u32[]{:S(2)}) %all-to-all-start.3) | async-done | bytes 262176 | tf_op jit(solution)/shard_map/all_to_all | solution.py:277
  117.7 1.0 shard_map.70
Async XLA Ops:
  1.4 24.1 %collective-permute-start = (bf16[6144,128]{1,0:T(8,128)(2,1)S(1)}, bf16[6144,128]{1,0:T(8,128)(2,1)S(1)}, u32[]{:S(2)}, u32[]{:S(2)}) collective-permute-start(bf16[6144,128]{1,0:T(8,128)(2,1)S(1)} %shard_map.67), channel_id=1, source_target_pairs={{0,0},{4,4},{24,24},{28,28},{16,12},{12,16},{20,8},{8,20},{1,1},{5... | collective-permute-start | bytes 4718600 | tf_op jit(solution)/shard_map/ppermute | solution.py:241
  9.6 37.6 %all-to-all-start = ((bf16[32,32,128]{2,1,0:T(8,128)(2,1)}), bf16[32,32,128]{2,1,0:T(8,128)(2,1)S(1)}, u32[]{:S(2)}, u32[]{:S(2)}) async-start(bf16[32,32,128]{2,1,0:T(8,128)(2,1)} %bitcast.9), calls=%async_computation | async-start | bytes 524288 | tf_op jit(solution)/shard_map/all_to_all | solution.py:254
  25.5 43.6 %collective-permute-start.1 = (bf16[6144,128]{1,0:T(8,128)(2,1)S(1)}, bf16[6144,128]{1,0:T(8,128)(2,1)S(1)}, u32[]{:S(2)}, u32[]{:S(2)}) collective-permute-start(bf16[6144,128]{1,0:T(8,128)(2,1)S(1)} %collective-permute-done.refs_0_), channel_id=1, source_target_pairs={{0,16},{16,0},{1,17},{17,1},{2,18},{18,2},{3,19},{19,3},{4,20},{20... | collective-permute-start | bytes 4718600 | tf_op jit(solution)/shard_map/ppermute | solution.py:260
  89.4 5.6 %copy-start = (s32[32,32]{1,0:T(8,128)S(1)}, s32[32,32]{1,0:T(8,128)}, u32[]{:S(2)}) copy-start(s32[32,32]{1,0:T(8,128)} %selected_ref.3) | copy-start | bytes 12292
  89.4 5.7 %copy-start.1 = (f32[32,32]{1,0:T(8,128)S(1)}, f32[32,32]{1,0:T(8,128)}, u32[]{:S(2)}) copy-start(f32[32,32]{1,0:T(8,128)} %affinity_ref.1) | copy-start | bytes 12292
  90.9 26.8 %all-to-all-start.3 = ((bf16[64,16,128]{2,1,0:T(8,128)(2,1)}), bf16[64,16,128]{2,1,0:T(8,128)(2,1)S(1)}, u32[]{:S(2)}, u32[]{:S(2)}) async-start(bf16[64,16,128]{2,1,0:T(8,128)(2,1)} %bitcast.4), calls=%async_computation.3 | async-start | bytes 524288 | tf_op jit(solution)/shard_map/all_to_all | solution.py:277

commit v11 on v10

--- a/solution.py
+++ b/solution.py
@@ -29,17 +29,19 @@
     return jnp.where(mask, 1.0, 0.0).astype(BF)
 
 
-def pack_kernel(gate_ref, up_ref, down_ref, out_ref, sems):
+def pack_kernel(gate_ref, up_ref, down_ref, out_ref, rest_ref, down_out_ref, sems):
     _, width, span = gate_ref.shape
-    copies = [(gate_ref.at[0], out_ref.at[:width]), (up_ref.at[0], out_ref.at[width : 2 * width])]
-    for k in range(width // span):
-        at = 2 * width + k * span
-        copies.append((down_ref.at[0, :, k * span : (k + 1) * span], out_ref.at[at : at + span]))
+    copies = [(gate_ref.at[0], out_ref.at[:width]), (up_ref.at[0], out_ref.at[width:])]
+    for at in range(0, width, span):
+        copies.append((down_ref.at[0, :, at : at + span], down_out_ref.at[at : at + span]))
     copies = [pltpu.make_async_copy(*c, sems.at[k]) for k, c in enumerate(copies)]
     for copy in copies:
         copy.start()
     for copy in copies:
         copy.wait()
+    store = pltpu.make_async_copy(down_out_ref, rest_ref, sems.at[0])
+    store.start()
+    store.wait()
 
 
 def pick_kernel(place_ref, selected_ref, tokens_ref, rows_ref, sel_ref, tile_ref, out_ref, sems):
@@ -75,7 +77,7 @@
         store.wait()
 
 
-def mix_kernel(selected_ref, affinity_ref, mix_ref):
+def mix_kernel(selected_ref, affinity_ref, out_ref, mix_ref, sem):
     experts, most = selected_ref.shape
     _, _, tok, slots = mix_ref.shape
     part = most // 2
@@ -94,6 +96,9 @@
         hit = as_row(sel) == iota((tok, slots), 0).astype(F32)
         mix_ref[half, 0] = jnp.where(hit, as_row(high), 0.0).astype(BF)
         mix_ref[half, 1] = jnp.where(hit, as_row(low), 0.0).astype(BF)
+    store = pltpu.make_async_copy(mix_ref, out_ref, sem)
+    store.start()
+    store.wait()
 
 
 def compact_kernel(slots_ref, rows_ref):
@@ -127,20 +132,25 @@
     return jnp.where(iota(left.shape, 1) < left.shape[1] // 2, left, right)
 
 
-def ffn_kernel(x_ref, *refs):
-    *weights, out_ref = refs
+def ffn_kernel(x_ref, mine_ref, other_ref, mine_down_ref, other_down_ref, out_ref, down_ref, sems):
     peers, _, span = x_ref.shape
     width = peers * span
+    loads = []
+    for k, ref in enumerate((mine_down_ref, other_down_ref)):
+        loads.append(pltpu.make_async_copy(ref, down_ref.at[k], sems.at[k]))
+        loads[k].start()
     x = jnp.concatenate([x_ref[k] for k in range(peers)], axis=1)
-    gate = dot(x, jnp.concatenate([w[:width] for w in weights], axis=1))
-    up = dot(x, jnp.concatenate([w[width : 2 * width] for w in weights], axis=1))
+    pair = (mine_ref, other_ref)
+    gate = dot(x, jnp.concatenate([w[:width] for w in pair], axis=1))
+    up = dot(x, jnp.concatenate([w[width:] for w in pair], axis=1))
     hidden = (gate / (1.0 + jnp.exp(-gate)) * up).astype(BF)
+    for load in loads:
+        load.wait()
     half = peers // 2
     for k in range(half):
         tiles = []
-        for block in (k, k + half):
-            at = 2 * width + block * span
-            tiles.append(jnp.concatenate([w[at : at + span] for w in weights], axis=0))
+        for at in (k * span, (k + half) * span):
+            tiles.append(jnp.concatenate([down_ref[j, at : at + span] for j in range(2)], axis=0))
         both = dot(hidden, jnp.concatenate(tiles, axis=1))
         low, high = both[:, :span], both[:, span:]
         out_ref[k] = joined(low, turned(high)).astype(BF)
@@ -232,13 +242,14 @@
     lines = lax.axis_size("yy")
     peers = lax.axis_size("x")
     place = lax.axis_index(TP).astype(jnp.int32).reshape(1)
-    packed = local_call(
+    packed, rest = local_call(
         pack_kernel,
-        array((3 * width, span)),
+        [array((2 * width, span)), pltpu.HBM((width, span), BF)],
         hbm=(w_gate, w_up, w_down),
-        scratch=[pltpu.SemaphoreType.DMA((2 + team,))],
+        scratch=[pltpu.VMEM((width, span), BF), pltpu.SemaphoreType.DMA((2 + team,))],
     )
     mine = lax.ppermute(packed, ("c", "g", "yy"), TRADE)
+    mine_down = lax.ppermute(rest, ("c", "g", "yy"), TRADE)
     rows = local_call(
         pick_kernel,
         pltpu.HBM((layers, 2, most, span), BF),
@@ -254,10 +265,15 @@
     arrived = lax.all_to_all(rows.reshape(ep, most, span), EP, 0, 0, tiled=True)
     mix = local_call(
         mix_kernel,
-        array((2, 2, tok, experts * most // 2)),
+        pltpu.HBM((2, 2, tok, experts * most // 2), BF),
         params=(selected, affinity),
+        scratch=[
+            pltpu.VMEM((2, 2, tok, experts * most // 2), BF),
+            pltpu.SemaphoreType.DMA(()),
+        ],
     )
     other = lax.ppermute(mine, "c", CORES)
+    other_down = lax.ppermute(mine_down, "c", CORES)
     copies = local_call(compact_kernel, array((2, lines, peers, part, span)), arrived)
     chosen = lax.all_to_all(copies.reshape(team, part, span), TEAM, 0, 0, tiled=True)
     partial = local_call(
@@ -266,6 +282,8 @@
         chosen,
         mine,
         other,
+        hbm=(mine_down, other_down),
+        scratch=[pltpu.VMEM((2, width, span), BF), pltpu.SemaphoreType.DMA((2,))],
     )
     summands = lax.all_to_all(partial, TEAM, 0, 0, tiled=True)
     result = local_call(

time: 119 us -> 124 us (1.042)
  blocking collectives: 40.2 us -> 19.2 us
  starting transfers between devices: 27.5 us -> 40.2 us
  waiting for transfers between devices: 42.7 us -> 50.4 us
  Pallas kernels: 8.26 us -> 11.9 us
    all_to_all x1 -> x0, blocking collectives: 21 us -> none  [per_device(): lax.all_to_all(copies.reshape(team, part, span), TEAM, 0, 0, tiled=True)]
    all_to_all x0 -> x1, waiting for transfers between devices: none -> 12 us  [per_device(): lax.all_to_all(copies.reshape(team, part, span), TEAM, 0, 0, tiled=True)]
    all_to_all x1, waiting for transfers between devices: 19.8 us -> 14.7 us  [per_device(): arrived = lax.all_to_all(rows.reshape(ep, most, span), EP, 0, 0, tiled=True)]
    all_to_all x0 -> x1, starting transfers between devices: none -> 4.97 us  [per_device(): lax.all_to_all(copies.reshape(team, part, span), TEAM, 0, 0, tiled=True)]
    ppermute x0 -> x2, starting transfers between devices: none -> 4.05 us  [the longest x1 2.04 us: per_device(): mine_down = lax.ppermute(rest, ('c', 'g', 'yy'), TRADE)]
    pallas_call x7, Pallas kernels: 8.26 us -> 11.9 us  [local_call(): pl.pallas_call(kernel, in_specs=specs, out_specs=jax.tree.map(lambda o: p...]
    ppermute x1, starting transfers between devices: 1.91 us -> 5.44 us  [per_device(): other = lax.ppermute(mine, 'c', CORES)]
    ppermute x0 -> x2, waiting for transfers between devices: none -> 2.13 us  [the longest x1 2.13 us: per_device(): other_down = lax.ppermute(mine_down, 'c', CORES)]
  transfers between devices with their start and end apart: 4 -> 7, of which waited for: 3 -> 4; matrix products, arithmetic and copies ran while one was open for 0% -> 0% of each run, Pallas kernels for 3% -> 4%
where the time goes in v11:
time: 124 us; the launch traced here: 123 us
  waiting for transfers between devices  50.4 us (41%)
  starting transfers between devices  40.2 us (32%)
  blocking collectives  19.2 us (15%)
  Pallas kernels  11.9 us (10%)
    all_to_all x1, waiting for transfers between devices, per_device(): lax.all_to_all(result.reshape(2 * ep, most // 2, span), ('z', 'c', 'g'),...  21.5 us
    all_to_all x1, blocking collectives, per_device(): summands = lax.all_to_all(partial, TEAM, 0, 0, tiled=True)  19.2 us
    all_to_all x1, starting transfers between devices, per_device(): arrived = lax.all_to_all(rows.reshape(ep, most, span), EP, 0, 0, tiled=True)  15.4 us
    all_to_all x1, waiting for transfers between devices, per_device(): arrived = lax.all_to_all(rows.reshape(ep, most, span), EP, 0, 0, tiled=True)  14.7 us
    all_to_all x1, waiting for transfers between devices, per_device(): lax.all_to_all(copies.reshape(team, part, span), TEAM, 0, 0, tiled=True)  12 us
    pallas_call x7, Pallas kernels, local_call(): pl.pallas_call(kernel, in_specs=specs, out_specs=jax.tree.map(lambda o: p...  11.9 us
    ppermute x1, starting transfers between devices, per_device(): mine = lax.ppermute(packed, ('c', 'g', 'yy'), TRADE)  6.02 us
    ppermute x1, starting transfers between devices, per_device(): other = lax.ppermute(mine, 'c', CORES)  5.44 us
  transfers between devices with their start and end apart: 7, of which 4 were waited for; matrix products, arithmetic and copies ran while one was open for 0% of the time, Pallas kernels for 4%

profile of v11, /device:TPU:1, one launch (start us, length us, event | category | flops | bytes accessed | tf_op | source)
XLA Modules:
  0.0 122.9 jit_solution(17941814698580267470)
XLA Ops:
  0.0 2.2 %shard_map.67 = (bf16[4096,128]{1,0:T(8,128)(2,1)S(1)}, bf16[2048,128]{1,0:T(8,128)(2,1)}) custom-call(bf16[1,2048,128]{2,1,0:T(8,128)(2,1)} %gate_ref.1, bf16[1,2048,128]{2,1,0:T(8,128)(2,1)} %up_ref.1, bf16[1,128,2048]{2,1,0:T(8,128)(2,1)} %down_ref.1), custom_call_target="tpu_custom_call" | custom-call | tf_op jit(solution)/shard_map/pallas_call | solution.py:218
  2.2 6.0 %collective-permute-start = (bf16[4096,128]{1,0:T(8,128)(2,1)S(1)}, bf16[4096,128]{1,0:T(8,128)(2,1)S(1)}, u32[]{:S(2)}, u32[]{:S(2)}) collective-permute-start(bf16[4096,128]{1,0:T(8,128)(2,1)S(1)} %get-tuple-element.7), channel_id=1, source_target_pairs={{0,0},{4,4},{24,24},{28,28},{16,12},{12,16},{20,8},{8,20},{1,1},{5... | collective-permute-start | bytes 3145736 | tf_op jit(solution)/shard_map/ppermute | solution.py:251
  8.3 2.1 %shard_map.65 = bf16[16,2,32,128]{3,2,1,0:T(8,128)(2,1)} custom-call(s32[1]{0:T(128)} %bitcast.place_ref, s32[32,32]{1,0:T(8,128)} %selected_ref.3, bf16[128,2048]{1,0:T(8,128)(2,1)} %tokens_ref.1), custom_call_target="tpu_custom_call" | custom-call | tf_op jit(solution)/shard_map/pallas_call | solution.py:218
  10.4 15.4 %all-to-all-start = ((bf16[32,32,128]{2,1,0:T(8,128)(2,1)}), bf16[32,32,128]{2,1,0:T(8,128)(2,1)S(1)}, u32[]{:S(2)}, u32[]{:S(2)}) async-start(bf16[32,32,128]{2,1,0:T(8,128)(2,1)} %bitcast.8), calls=%async_computation | async-start | bytes 524288 | tf_op jit(solution)/shard_map/all_to_all | solution.py:265
  25.8 2.0 %collective-permute-start.2 = (bf16[2048,128]{1,0:T(8,128)(2,1)}, bf16[2048,128]{1,0:T(8,128)(2,1)}, u32[]{:S(2)}, u32[]{:S(2)}) collective-permute-start(bf16[2048,128]{1,0:T(8,128)(2,1)} %get-tuple-element.8), channel_id=1, source_target_pairs={{0,0},{4,4},{24,24},{28,28},{16,12},{12,16},{20,8},{8,20},{1,1},{5... | collective-permute-start | bytes 1572872 | tf_op jit(solution)/shard_map/ppermute | solution.py:252
  27.9 0.0 collective-permute-done.mine_ref
  27.9 5.4 %collective-permute-start.1 = (bf16[4096,128]{1,0:T(8,128)(2,1)S(1)}, bf16[4096,128]{1,0:T(8,128)(2,1)S(1)}, u32[]{:S(2)}, u32[]{:S(2)}) collective-permute-start(bf16[4096,128]{1,0:T(8,128)(2,1)S(1)} %collective-permute-done.mine_ref), channel_id=1, source_target_pairs={{0,16},{16,0},{1,17},{17,1},{2,18},{18,2},{3,19},{19,3},{4,20},{20... | collective-permute-start | bytes 3145736 | tf_op jit(solution)/shard_map/ppermute | solution.py:275
  33.3 14.7 %all-to-all-done.slots_ref = bf16[32,32,128]{2,1,0:T(8,128)(2,1)S(1)} async-done(((bf16[32,32,128]{2,1,0:T(8,128)(2,1)}), bf16[32,32,128]{2,1,0:T(8,128)(2,1)S(1)}, u32[]{:S(2)}, u32[]{:S(2)}) %all-to-all-start) | async-done | bytes 262176 | tf_op jit(solution)/shard_map/all_to_all | solution.py:265
  48.1 1.8 %shard_map.66 = bf16[2,2,4,256,128]{4,3,2,1,0:T(8,128)(2,1)} custom-call(bf16[32,32,128]{2,1,0:T(8,128)(2,1)S(1)} %all-to-all-done.slots_ref), custom_call_target="tpu_custom_call" | custom-call | tf_op jit(solution)/shard_map/pallas_call | solution.py:218
  49.9 5.0 %all-to-all-start.1 = ((bf16[16,256,128]{2,1,0:T(8,128)(2,1)}), bf16[16,256,128]{2,1,0:T(8,128)(2,1)S(1)}, u32[]{:S(2)}, u32[]{:S(2)}) async-start(bf16[16,256,128]{2,1,0:T(8,128)(2,1)} %bitcast.2), calls=%async_computation.1 | async-start | bytes 2097152 | tf_op jit(solution)/shard_map/all_to_all | solution.py:278
  54.8 0.0 collective-permute-done.2.mine_down_ref
  54.8 2.0 %collective-permute-start.3 = (bf16[2048,128]{1,0:T(8,128)(2,1)}, bf16[2048,128]{1,0:T(8,128)(2,1)}, u32[]{:S(2)}, u32[]{:S(2)}) collective-permute-start(bf16[2048,128]{1,0:T(8,128)(2,1)} %collective-permute-done.2.mine_down_ref), channel_id=1, source_target_pairs={{0,16},{16,0},{1,17},{17,1},{2,18},{18,2},{3,19},{19,3},{4,20},{20... | collective-permute-start | bytes 1572872 | tf_op jit(solution)/shard_map/ppermute | solution.py:276
  56.9 2.1 %collective-permute-done.3.other_down_ref = bf16[2048,128]{1,0:T(8,128)(2,1)} collective-permute-done((bf16[2048,128]{1,0:T(8,128)(2,1)}, bf16[2048,128]{1,0:T(8,128)(2,1)}, u32[]{:S(2)}, u32[]{:S(2)}) %collective-permute-start.3) | collective-permute-done | bytes 524320 | tf_op jit(solution)/shard_map/ppermute | solution.py:276
  59.0 12.0 %all-to-all-done.1.x_ref = bf16[16,256,128]{2,1,0:T(8,128)(2,1)S(1)} async-done(((bf16[16,256,128]{2,1,0:T(8,128)(2,1)}), bf16[16,256,128]{2,1,0:T(8,128)(2,1)S(1)}, u32[]{:S(2)}, u32[]{:S(2)}) %all-to-all-start.1) | async-done | bytes 1048608 | tf_op jit(solution)/shard_map/all_to_all | solution.py:278
  71.0 0.0 collective-permute-done.1.other_ref
  71.0 2.2 %shard_map.68 = bf16[16,256,128]{2,1,0:T(8,128)(2,1)S(1)} custom-call(bf16[16,256,128]{2,1,0:T(8,128)(2,1)S(1)} %all-to-all-done.1.x_ref, bf16[4096,128]{1,0:T(8,128)(2,1)S(1)} %collective-permute-done.mine_ref, bf16[4096,128]{1,0:T(8,128)(2,1)S(1)} %collective-permute-done.1.other_ref, bf16[2048,128]{1,0:T(8,128)(2,1)} %collective-permute-done.2.mine_down_ref, ...), custom_call_target="tpu_custom_call" | custom-call | tf_op jit(solution)/shard_map/pallas_call | solution.py:218
  73.3 19.2 %all_to_all.20 = bf16[16,256,128]{2,1,0:T(8,128)(2,1)S(1)} all-to-all(bf16[16,256,128]{2,1,0:T(8,128)(2,1)S(1)} %shard_map.68), channel_id=1, replica_groups=mesh['z'=16,'c'=2,'g'=2,'yy'=2,'x'=4] {'c','yy','x'}, dimensions={0} | all-to-all | bytes 2097152 | tf_op jit(solution)/shard_map/all_to_all | solution.py:288
  92.4 1.5 %shard_map.69 = bf16[32,2,16,128]{3,2,1,0:T(8,128)(2,1)} custom-call(bf16[2,2,4,256,128]{4,3,2,1,0:T(8,128)(2,1)S(1)} %bitcast.6, bf16[32,32,128]{2,1,0:T(8,128)(2,1)S(1)} %all-to-all-done.slots_ref), custom_call_target="tpu_custom_call" | custom-call | tf_op jit(solution)/shard_map/pallas_call | solution.py:218
  93.9 0.0 copy-start.1
  93.9 0.0 copy-start.2
  93.9 4.3 %all-to-all-start.3 = ((bf16[64,16,128]{2,1,0:T(8,128)(2,1)}), bf16[64,16,128]{2,1,0:T(8,128)(2,1)S(1)}, u32[]{:S(2)}, u32[]{:S(2)}) async-start(bf16[64,16,128]{2,1,0:T(8,128)(2,1)} %bitcast.4), calls=%async_computation.3 | async-start | bytes 524288 | tf_op jit(solution)/shard_map/all_to_all | solution.py:295
  98.2 0.0 copy-done.1
  98.2 0.0 copy-done.2
  98.2 1.1 shard_map.64.mix_ref
  99.3 21.5 %all-to-all-done.3 = bf16[64,16,128]{2,1,0:T(8,128)(2,1)S(1)} async-done(((bf16[64,16,128]{2,1,0:T(8,128)(2,1)}), bf16[64,16,128]{2,1,0:T(8,128)(2,1)S(1)}, u32[]{:S(2)}, u32[]{:S(2)}) %all-to-all-start.3) | async-done | bytes 262176 | tf_op jit(solution)/shard_map/all_to_all | solution.py:295
  120.8 0.0 copy-start
  120.8 1.0 copy-done
  121.9 1.0 shard_map.70
Async XLA Ops:
  2.2 25.6 %collective-permute-start = (bf16[4096,128]{1,0:T(8,128)(2,1)S(1)}, bf16[4096,128]{1,0:T(8,128)(2,1)S(1)}, u32[]{:S(2)}, u32[]{:S(2)}) collective-permute-start(bf16[4096,128]{1,0:T(8,128)(2,1)S(1)} %get-tuple-element.7), channel_id=1, source_target_pairs={{0,0},{4,4},{24,24},{28,28},{16,12},{12,16},{20,8},{8,20},{1,1},{5... | collective-permute-start | bytes 3145736 | tf_op jit(solution)/shard_map/ppermute | solution.py:251
  10.4 37.6 %all-to-all-start = ((bf16[32,32,128]{2,1,0:T(8,128)(2,1)}), bf16[32,32,128]{2,1,0:T(8,128)(2,1)S(1)}, u32[]{:S(2)}, u32[]{:S(2)}) async-start(bf16[32,32,128]{2,1,0:T(8,128)(2,1)} %bitcast.8), calls=%async_computation | async-start | bytes 524288 | tf_op jit(solution)/shard_map/all_to_all | solution.py:265
  25.8 29.0 %collective-permute-start.2 = (bf16[2048,128]{1,0:T(8,128)(2,1)}, bf16[2048,128]{1,0:T(8,128)(2,1)}, u32[]{:S(2)}, u32[]{:S(2)}) collective-permute-start(bf16[2048,128]{1,0:T(8,128)(2,1)} %get-tuple-element.8), channel_id=1, source_target_pairs={{0,0},{4,4},{24,24},{28,28},{16,12},{12,16},{20,8},{8,20},{1,1},{5... | collective-permute-start | bytes 1572872 | tf_op jit(solution)/shard_map/ppermute | solution.py:252
  27.9 43.2 %collective-permute-start.1 = (bf16[4096,128]{1,0:T(8,128)(2,1)S(1)}, bf16[4096,128]{1,0:T(8,128)(2,1)S(1)}, u32[]{:S(2)}, u32[]{:S(2)}) collective-permute-start(bf16[4096,128]{1,0:T(8,128)(2,1)S(1)} %collective-permute-done.mine_ref), channel_id=1, source_target_pairs={{0,16},{16,0},{1,17},{17,1},{2,18},{18,2},{3,19},{19,3},{4,20},{20... | collective-permute-start | bytes 3145736 | tf_op jit(solution)/shard_map/ppermute | solution.py:275
  49.9 21.2 %all-to-all-start.1 = ((bf16[16,256,128]{2,1,0:T(8,128)(2,1)}), bf16[16,256,128]{2,1,0:T(8,128)(2,1)S(1)}, u32[]{:S(2)}, u32[]{:S(2)}) async-start(bf16[16,256,128]{2,1,0:T(8,128)(2,1)} %bitcast.2), calls=%async_computation.1 | async-start | bytes 2097152 | tf_op jit(solution)/shard_map/all_to_all | solution.py:278
  54.8 4.1 %collective-permute-start.3 = (bf16[2048,128]{1,0:T(8,128)(2,1)}, bf16[2048,128]{1,0:T(8,128)(2,1)}, u32[]{:S(2)}, u32[]{:S(2)}) collective-permute-start(bf16[2048,128]{1,0:T(8,128)(2,1)} %collective-permute-done.2.mine_down_ref), channel_id=1, source_target_pairs={{0,16},{16,0},{1,17},{17,1},{2,18},{18,2},{3,19},{19,3},{4,20},{20... | collective-permute-start | bytes 1572872 | tf_op jit(solution)/shard_map/ppermute | solution.py:276
  93.9 4.3 %copy-start.1 = (s32[32,32]{1,0:T(8,128)S(1)}, s32[32,32]{1,0:T(8,128)}, u32[]{:S(2)}) copy-start(s32[32,32]{1,0:T(8,128)} %selected_ref.3) | copy-start | bytes 12292
  93.9 4.3 %copy-start.2 = (f32[32,32]{1,0:T(8,128)S(1)}, f32[32,32]{1,0:T(8,128)}, u32[]{:S(2)}) copy-start(f32[32,32]{1,0:T(8,128)} %affinity_ref.1) | copy-start | bytes 12292
  93.9 26.9 %all-to-all-start.3 = ((bf16[64,16,128]{2,1,0:T(8,128)(2,1)}), bf16[64,16,128]{2,1,0:T(8,128)(2,1)S(1)}, u32[]{:S(2)}, u32[]{:S(2)}) async-start(bf16[64,16,128]{2,1,0:T(8,128)(2,1)} %bitcast.4), calls=%async_computation.3 | async-start | bytes 524288 | tf_op jit(solution)/shard_map/all_to_all | solution.py:295
  120.8 1.0 copy-start

commit v12 on v10

--- a/solution.py
+++ b/solution.py
@@ -15,6 +15,11 @@
 LIMIT = 32.0
 TRADE = [(0, 0), (1, 1), (6, 6), (7, 7), (4, 3), (3, 4), (5, 2), (2, 5)]
 CORES = [(0, 1), (1, 0)]
+
+
+def turned_groups(layers, members):
+    ranks = layers * members
+    return [[(k + ranks // 2) % ranks for k in range(ranks)]]
 
 
 def iota(shape, dim):
@@ -59,7 +64,8 @@
     slots = here * most
     first.wait()
     sel = sel_ref[...].astype(F32).astype(BF)
-    repeat = one_hot(2 * (iota((slots, experts), 0) // most) + g == iota((slots, experts), 1))
+    layer = (iota((slots, experts), 0) // most + here // 2) % here
+    repeat = one_hot(2 * layer + g == iota((slots, experts), 1))
     own = iota((slots, most), 0) % most == iota((slots, most), 1)
     spread = jnp.where(own, dot(repeat, sel), 0.0).astype(BF)
     position = dot(spread, jnp.ones((most, tok), BF))
@@ -79,7 +85,8 @@
     experts, most = selected_ref.shape
     _, _, tok, slots = mix_ref.shape
     part = most // 2
-    mine = iota((experts, slots), 0) == iota((experts, slots), 1) // part
+    expert = (iota((experts, slots), 1) // part + experts // 2) % experts
+    mine = iota((experts, slots), 0) == expert
     sel = selected_ref[...].astype(F32).astype(BF)
     aff = affinity_ref[...]
     high = aff.astype(BF)
@@ -251,7 +258,14 @@
             pltpu.SemaphoreType.DMA((5,)),
         ],
     )
-    arrived = lax.all_to_all(rows.reshape(ep, most, span), EP, 0, 0, tiled=True)
+    arrived = lax.all_to_all(
+        rows.reshape(ep, most, span),
+        EP,
+        0,
+        0,
+        axis_index_groups=turned_groups(layers, 2),
+        tiled=True,
+    )
     mix = local_call(
         mix_kernel,
         array((2, 2, tok, experts * most // 2)),
@@ -275,7 +289,12 @@
         arrived,
     )
     returned = lax.all_to_all(
-        result.reshape(2 * ep, most // 2, span), ("z", "c", "g"), 0, 0, tiled=True
+        result.reshape(2 * ep, most // 2, span),
+        ("z", "c", "g"),
+        0,
+        0,
+        axis_index_groups=turned_groups(layers, 4),
+        tiled=True,
     )
     return local_call(
         combine_kernel,

time: 119 us -> 115 us (0.966)
  waiting for transfers between devices: 42.7 us -> 24.5 us
  starting transfers between devices: 27.5 us -> 41.4 us
    all_to_all x1, starting transfers between devices: 4.18 us -> 14.4 us  [per_device(): lax.all_to_all(result.reshape(2 * ep, most // 2, span), ('z', 'c', 'g'),...]
    all_to_all x1, waiting for transfers between devices: 19.8 us -> 10.2 us  [per_device(): lax.all_to_all(rows.reshape(ep, most, span), EP, 0, 0, axis_index_groups=...]
    all_to_all x1, waiting for transfers between devices: 22.3 us -> 14.3 us  [per_device(): lax.all_to_all(result.reshape(2 * ep, most // 2, span), ('z', 'c', 'g'),...]
    all_to_all x1, starting transfers between devices: 15.4 us -> 18.7 us  [per_device(): lax.all_to_all(rows.reshape(ep, most, span), EP, 0, 0, axis_index_groups=...]
  transfers between devices with their start and end apart: 4 -> 4, of which waited for: 3 -> 2; matrix products, arithmetic and copies ran while one was open for 0% -> 0% of each run, Pallas kernels for 3% -> 3%
where the time goes in v12:
time: 115 us; the launch traced here: 114 us
  starting transfers between devices  41.4 us (36%)
  blocking collectives  39.9 us (35%)
  waiting for transfers between devices  24.5 us (21%)
  Pallas kernels  8.33 us (7%)
    all_to_all x1, blocking collectives, per_device(): lax.all_to_all(copies.reshape(team, part, span), TEAM, 0, 0, tiled=True)  20.7 us
    all_to_all x1, blocking collectives, per_device(): summands = lax.all_to_all(partial, TEAM, 0, 0, tiled=True)  19.2 us
    all_to_all x1, starting transfers between devices, per_device(): lax.all_to_all(rows.reshape(ep, most, span), EP, 0, 0, axis_index_groups=...  18.7 us
    all_to_all x1, starting transfers between devices, per_device(): lax.all_to_all(result.reshape(2 * ep, most // 2, span), ('z', 'c', 'g'),...  14.4 us
    all_to_all x1, waiting for transfers between devices, per_device(): lax.all_to_all(result.reshape(2 * ep, most // 2, span), ('z', 'c', 'g'),...  14.3 us
    all_to_all x1, waiting for transfers between devices, per_device(): lax.all_to_all(rows.reshape(ep, most, span), EP, 0, 0, axis_index_groups=...  10.2 us
    pallas_call x7, Pallas kernels, local_call(): pl.pallas_call(kernel, in_specs=specs, out_specs=jax.tree.map(lambda o: p...  8.33 us
    ppermute x1, starting transfers between devices, per_device(): mine = lax.ppermute(packed, ('c', 'g', 'yy'), TRADE)  6.02 us
  transfers between devices with their start and end apart: 4, of which 2 were waited for; matrix products, arithmetic and copies ran while one was open for 0% of the time, Pallas kernels for 3%

profile of v12, /device:TPU:1, one launch (start us, length us, event | category | flops | bytes accessed | tf_op | source)
XLA Modules:
  0.0 114.3 jit_solution(15252634267941210350)
XLA Ops:
  0.0 1.4 %shard_map.67 = bf16[6144,128]{1,0:T(8,128)(2,1)S(1)} custom-call(bf16[1,2048,128]{2,1,0:T(8,128)(2,1)} %gate_ref.1, bf16[1,2048,128]{2,1,0:T(8,128)(2,1)} %up_ref.1, bf16[1,128,2048]{2,1,0:T(8,128)(2,1)} %down_ref.1), custom_call_target="tpu_custom_call" | custom-call | tf_op jit(solution)/shard_map/pallas_call | solution.py:215
  1.4 6.0 %collective-permute-start = (bf16[6144,128]{1,0:T(8,128)(2,1)S(1)}, bf16[6144,128]{1,0:T(8,128)(2,1)S(1)}, u32[]{:S(2)}, u32[]{:S(2)}) collective-permute-start(bf16[6144,128]{1,0:T(8,128)(2,1)S(1)} %shard_map.67), channel_id=1, source_target_pairs={{0,0},{4,4},{24,24},{28,28},{16,12},{12,16},{20,8},{8,20},{1,1},{5... | collective-permute-start | bytes 4718600 | tf_op jit(solution)/shard_map/ppermute | solution.py:248
  7.5 2.2 %shard_map.65 = bf16[16,2,32,128]{3,2,1,0:T(8,128)(2,1)} custom-call(s32[1]{0:T(128)} %bitcast.place_ref, s32[32,32]{1,0:T(8,128)} %selected_ref.3, bf16[128,2048]{1,0:T(8,128)(2,1)} %tokens_ref.1), custom_call_target="tpu_custom_call" | custom-call | tf_op jit(solution)/shard_map/pallas_call | solution.py:215
  9.7 18.7 %all-to-all-start = ((bf16[32,32,128]{2,1,0:T(8,128)(2,1)}), bf16[32,32,128]{2,1,0:T(8,128)(2,1)S(1)}, u32[]{:S(2)}, u32[]{:S(2)}) async-start(bf16[32,32,128]{2,1,0:T(8,128)(2,1)} %bitcast.9), calls=%async_computation | async-start | bytes 524288 | tf_op jit(solution)/shard_map/all_to_all | solution.py:261
  28.4 0.0 collective-permute-done.refs_0_
  28.4 2.3 %collective-permute-start.1 = (bf16[6144,128]{1,0:T(8,128)(2,1)S(1)}, bf16[6144,128]{1,0:T(8,128)(2,1)S(1)}, u32[]{:S(2)}, u32[]{:S(2)}) collective-permute-start(bf16[6144,128]{1,0:T(8,128)(2,1)S(1)} %collective-permute-done.refs_0_), channel_id=1, source_target_pairs={{0,16},{16,0},{1,17},{17,1},{2,18},{18,2},{3,19},{19,3},{4,20},{20... | collective-permute-start | bytes 4718600 | tf_op jit(solution)/shard_map/ppermute | solution.py:274
  30.7 10.2 %all-to-all-done.slots_ref = bf16[32,32,128]{2,1,0:T(8,128)(2,1)S(1)} async-done(((bf16[32,32,128]{2,1,0:T(8,128)(2,1)}), bf16[32,32,128]{2,1,0:T(8,128)(2,1)S(1)}, u32[]{:S(2)}, u32[]{:S(2)}) %all-to-all-start) | async-done | bytes 262176 | tf_op jit(solution)/shard_map/all_to_all | solution.py:261
  40.9 0.8 shard_map.66
  41.7 20.7 %all_to_all.20.x_ref = bf16[16,256,128]{2,1,0:T(8,128)(2,1)S(1)} all-to-all(bf16[16,256,128]{2,1,0:T(8,128)(2,1)S(1)} %bitcast.6), channel_id=1, replica_groups=mesh['z'=16,'c'=2,'g'=2,'yy'=2,'x'=4] {'c','yy','x'}, dimensions={0} | all-to-all | bytes 2097152 | tf_op jit(solution)/shard_map/all_to_all | solution.py:276
  62.5 0.0 collective-permute-done.1.refs_1_
  62.5 1.2 %shard_map.68 = bf16[16,256,128]{2,1,0:T(8,128)(2,1)S(1)} custom-call(bf16[16,256,128]{2,1,0:T(8,128)(2,1)S(1)} %all_to_all.20.x_ref, bf16[6144,128]{1,0:T(8,128)(2,1)S(1)} %collective-permute-done.refs_0_, bf16[6144,128]{1,0:T(8,128)(2,1)S(1)} %collective-permute-done.1.refs_1_), custom_call_target="tpu_custom_call" | custom-call | tf_op jit(solution)/shard_map/pallas_call | solution.py:215
  63.6 19.2 %all_to_all.21 = bf16[16,256,128]{2,1,0:T(8,128)(2,1)S(1)} all-to-all(bf16[16,256,128]{2,1,0:T(8,128)(2,1)S(1)} %shard_map.68), channel_id=1, replica_groups=mesh['z'=16,'c'=2,'g'=2,'yy'=2,'x'=4] {'c','yy','x'}, dimensions={0} | all-to-all | bytes 2097152 | tf_op jit(solution)/shard_map/all_to_all | solution.py:284
  82.8 0.0 copy-start
  82.8 0.0 copy-start.1
  82.8 1.5 %shard_map.69 = bf16[32,2,16,128]{3,2,1,0:T(8,128)(2,1)} custom-call(bf16[2,2,4,256,128]{4,3,2,1,0:T(8,128)(2,1)S(1)} %bitcast.7, bf16[32,32,128]{2,1,0:T(8,128)(2,1)S(1)} %all-to-all-done.slots_ref), custom_call_target="tpu_custom_call" | custom-call | tf_op jit(solution)/shard_map/pallas_call | solution.py:215
  84.3 14.4 %all-to-all-start.3 = ((bf16[64,16,128]{2,1,0:T(8,128)(2,1)}), bf16[64,16,128]{2,1,0:T(8,128)(2,1)S(1)}, u32[]{:S(2)}, u32[]{:S(2)}) async-start(bf16[64,16,128]{2,1,0:T(8,128)(2,1)} %bitcast.4), calls=%async_computation.3 | async-start | bytes 524288 | tf_op jit(solution)/shard_map/all_to_all | solution.py:291
  98.7 0.0 copy-done
  98.7 0.0 copy-done.1
  98.7 0.3 shard_map.64.mix_ref
  99.0 14.3 %all-to-all-done.3 = bf16[64,16,128]{2,1,0:T(8,128)(2,1)S(1)} async-done(((bf16[64,16,128]{2,1,0:T(8,128)(2,1)}), bf16[64,16,128]{2,1,0:T(8,128)(2,1)S(1)}, u32[]{:S(2)}, u32[]{:S(2)}) %all-to-all-start.3) | async-done | bytes 262176 | tf_op jit(solution)/shard_map/all_to_all | solution.py:291
  113.3 1.0 shard_map.70
Async XLA Ops:
  1.4 27.0 %collective-permute-start = (bf16[6144,128]{1,0:T(8,128)(2,1)S(1)}, bf16[6144,128]{1,0:T(8,128)(2,1)S(1)}, u32[]{:S(2)}, u32[]{:S(2)}) collective-permute-start(bf16[6144,128]{1,0:T(8,128)(2,1)S(1)} %shard_map.67), channel_id=1, source_target_pairs={{0,0},{4,4},{24,24},{28,28},{16,12},{12,16},{20,8},{8,20},{1,1},{5... | collective-permute-start | bytes 4718600 | tf_op jit(solution)/shard_map/ppermute | solution.py:248
  9.7 31.2 %all-to-all-start = ((bf16[32,32,128]{2,1,0:T(8,128)(2,1)}), bf16[32,32,128]{2,1,0:T(8,128)(2,1)S(1)}, u32[]{:S(2)}, u32[]{:S(2)}) async-start(bf16[32,32,128]{2,1,0:T(8,128)(2,1)} %bitcast.9), calls=%async_computation | async-start | bytes 524288 | tf_op jit(solution)/shard_map/all_to_all | solution.py:261
  28.4 34.1 %collective-permute-start.1 = (bf16[6144,128]{1,0:T(8,128)(2,1)S(1)}, bf16[6144,128]{1,0:T(8,128)(2,1)S(1)}, u32[]{:S(2)}, u32[]{:S(2)}) collective-permute-start(bf16[6144,128]{1,0:T(8,128)(2,1)S(1)} %collective-permute-done.refs_0_), channel_id=1, source_target_pairs={{0,16},{16,0},{1,17},{17,1},{2,18},{18,2},{3,19},{19,3},{4,20},{20... | collective-permute-start | bytes 4718600 | tf_op jit(solution)/shard_map/ppermute | solution.py:274
  82.8 15.9 %copy-start = (s32[32,32]{1,0:T(8,128)S(1)}, s32[32,32]{1,0:T(8,128)}, u32[]{:S(2)}) copy-start(s32[32,32]{1,0:T(8,128)} %selected_ref.3) | copy-start | bytes 12292
  82.8 15.9 %copy-start.1 = (f32[32,32]{1,0:T(8,128)S(1)}, f32[32,32]{1,0:T(8,128)}, u32[]{:S(2)}) copy-start(f32[32,32]{1,0:T(8,128)} %affinity_ref.1) | copy-start | bytes 12292
  84.3 29.0 %all-to-all-start.3 = ((bf16[64,16,128]{2,1,0:T(8,128)(2,1)}), bf16[64,16,128]{2,1,0:T(8,128)(2,1)S(1)}, u32[]{:S(2)}, u32[]{:S(2)}) async-start(bf16[64,16,128]{2,1,0:T(8,128)(2,1)} %bitcast.4), calls=%async_computation.3 | async-start | bytes 524288 | tf_op jit(solution)/shard_map/all_to_all | solution.py:291

commit v13 on v12

--- a/solution.py
+++ b/solution.py
@@ -17,9 +17,13 @@
 CORES = [(0, 1), (1, 0)]
 
 
-def turned_groups(layers, members):
-    ranks = layers * members
-    return [[(k + ranks // 2) % ranks for k in range(ranks)]]
+def turned_groups(layers, teams):
+    order = [(p + layers // 2) % layers for p in range(layers)]
+    return [[(z * 2 + c) * teams + g for z in order for c in (1, 0) for g in range(teams)]]
+
+
+def team_groups(members):
+    return [[(k + members // 2) % members for k in range(members)]]
 
 
 def iota(shape, dim):
@@ -55,7 +59,7 @@
     first.start()
     loads = []
     for c in range(2):
-        at = pl.multiple_of((8 * c + place_ref[0] % 8) * width, width)
+        at = pl.multiple_of((8 * (1 - c) + place_ref[0] % 8) * width, width)
         loads.append(
             pltpu.make_async_copy(tokens_ref.at[:, pl.ds(at, width)], tile_ref.at[c], sems.at[c])
         )
@@ -138,11 +142,11 @@
     *weights, out_ref = refs
     peers, _, span = x_ref.shape
     width = peers * span
-    x = jnp.concatenate([x_ref[k] for k in range(peers)], axis=1)
+    half = peers // 2
+    x = jnp.concatenate([x_ref[(k + half) % peers] for k in range(peers)], axis=1)
     gate = dot(x, jnp.concatenate([w[:width] for w in weights], axis=1))
     up = dot(x, jnp.concatenate([w[width : 2 * width] for w in weights], axis=1))
     hidden = (gate / (1.0 + jnp.exp(-gate)) * up).astype(BF)
-    half = peers // 2
     for k in range(half):
         tiles = []
         for block in (k, k + half):
@@ -150,8 +154,8 @@
             tiles.append(jnp.concatenate([w[at : at + span] for w in weights], axis=0))
         both = dot(hidden, jnp.concatenate(tiles, axis=1))
         low, high = both[:, :span], both[:, span:]
-        out_ref[k] = joined(low, turned(high)).astype(BF)
-        out_ref[k + half] = joined(turned(low), high).astype(BF)
+        out_ref[k + half] = joined(low, turned(high)).astype(BF)
+        out_ref[k] = joined(turned(low), high).astype(BF)
 
 
 def expand_kernel(parts_ref, slots_ref, out_ref):
@@ -193,8 +197,8 @@
 
 
 def combine_kernel(mix_ref, rows_ref, out_ref):
-    layers, cores, teams, step, width = rows_ref.shape
-    both = [rows_ref[:, c].reshape(layers * teams * step, width) for c in range(cores)]
+    layers, _, teams, step, width = rows_ref.shape
+    both = [rows_ref[:, c].reshape(layers * teams * step, width) for c in (1, 0)]
     both = jnp.concatenate(both, axis=1)
     first = dot(mix_ref[0, 0], both) + dot(mix_ref[0, 1], both)
     second = dot(mix_ref[1, 0], both) + dot(mix_ref[1, 1], both)
@@ -263,7 +267,7 @@
         EP,
         0,
         0,
-        axis_index_groups=turned_groups(layers, 2),
+        axis_index_groups=turned_groups(layers, 1),
         tiled=True,
     )
     mix = local_call(
@@ -273,7 +277,14 @@
     )
     other = lax.ppermute(mine, "c", CORES)
     copies = local_call(compact_kernel, array((2, lines, peers, part, span)), arrived)
-    chosen = lax.all_to_all(copies.reshape(team, part, span), TEAM, 0, 0, tiled=True)
+    chosen = lax.all_to_all(
+        copies.reshape(team, part, span),
+        TEAM,
+        0,
+        0,
+        axis_index_groups=team_groups(team),
+        tiled=True,
+    )
     partial = local_call(
         ffn_kernel,
         array((team, part, span)),
@@ -281,7 +292,7 @@
         mine,
         other,
     )
-    summands = lax.all_to_all(partial, TEAM, 0, 0, tiled=True)
+    summands = lax.all_to_all(partial, TEAM, 0, 0, axis_index_groups=team_groups(team), tiled=True)
     result = local_call(
         expand_kernel,
         array((ep, 2, most // 2, span)),
@@ -293,7 +304,7 @@
         ("z", "c", "g"),
         0,
         0,
-        axis_index_groups=turned_groups(layers, 4),
+        axis_index_groups=turned_groups(layers, 2),
         tiled=True,
     )
     return local_call(

time: 115 us -> 114 us (level)
  no operation moved by 1% of the time
where the time goes in v13:
time: 114 us; the launch traced here: 113 us
  starting transfers between devices  41.4 us (36%)
  blocking collectives  39.3 us (34%)
  waiting for transfers between devices  24.3 us (21%)
  Pallas kernels  8.32 us (7%)
    all_to_all x1, blocking collectives, per_device(): lax.all_to_all(copies.reshape(team, part, span), TEAM, 0, 0, axis_index_g...  20.4 us
    all_to_all x1, blocking collectives, per_device(): lax.all_to_all(partial, TEAM, 0, 0, axis_index_groups=team_groups(team),...  18.9 us
    all_to_all x1, starting transfers between devices, per_device(): lax.all_to_all(rows.reshape(ep, most, span), EP, 0, 0, axis_index_groups=...  18.5 us
    all_to_all x1, starting transfers between devices, per_device(): lax.all_to_all(result.reshape(2 * ep, most // 2, span), ('z', 'c', 'g'),...  14.6 us
    all_to_all x1, waiting for transfers between devices, per_device(): lax.all_to_all(result.reshape(2 * ep, most // 2, span), ('z', 'c', 'g'),...  14.2 us
    all_to_all x1, waiting for transfers between devices, per_device(): lax.all_to_all(rows.reshape(ep, most, span), EP, 0, 0, axis_index_groups=...  10.1 us
    pallas_call x7, Pallas kernels, local_call(): pl.pallas_call(kernel, in_specs=specs, out_specs=jax.tree.map(lambda o: p...  8.32 us
    ppermute x1, starting transfers between devices, per_device(): mine = lax.ppermute(packed, ('c', 'g', 'yy'), TRADE)  6.02 us
  transfers between devices with their start and end apart: 4, of which 2 were waited for; matrix products, arithmetic and copies ran while one was open for 0% of the time, Pallas kernels for 3%

profile of v13, /device:TPU:1, one launch (start us, length us, event | category | flops | bytes accessed | tf_op | source)
XLA Modules:
  0.0 113.4 jit_solution(1470421512177523114)
XLA Ops:
  0.0 1.4 %shard_map.67 = bf16[6144,128]{1,0:T(8,128)(2,1)S(1)} custom-call(bf16[1,2048,128]{2,1,0:T(8,128)(2,1)} %gate_ref.1, bf16[1,2048,128]{2,1,0:T(8,128)(2,1)} %up_ref.1, bf16[1,128,2048]{2,1,0:T(8,128)(2,1)} %down_ref.1), custom_call_target="tpu_custom_call" | custom-call | tf_op jit(solution)/shard_map/pallas_call | solution.py:219
  1.4 6.0 %collective-permute-start = (bf16[6144,128]{1,0:T(8,128)(2,1)S(1)}, bf16[6144,128]{1,0:T(8,128)(2,1)S(1)}, u32[]{:S(2)}, u32[]{:S(2)}) collective-permute-start(bf16[6144,128]{1,0:T(8,128)(2,1)S(1)} %shard_map.67), channel_id=1, source_target_pairs={{0,0},{4,4},{24,24},{28,28},{16,12},{12,16},{20,8},{8,20},{1,1},{5... | collective-permute-start | bytes 4718600 | tf_op jit(solution)/shard_map/ppermute | solution.py:252
  7.5 2.2 %shard_map.65 = bf16[16,2,32,128]{3,2,1,0:T(8,128)(2,1)} custom-call(s32[1]{0:T(128)} %bitcast.place_ref, s32[32,32]{1,0:T(8,128)} %selected_ref.3, bf16[128,2048]{1,0:T(8,128)(2,1)} %tokens_ref.1), custom_call_target="tpu_custom_call" | custom-call | tf_op jit(solution)/shard_map/pallas_call | solution.py:219
  9.7 18.5 %all-to-all-start = ((bf16[32,32,128]{2,1,0:T(8,128)(2,1)}), bf16[32,32,128]{2,1,0:T(8,128)(2,1)S(1)}, u32[]{:S(2)}, u32[]{:S(2)}) async-start(bf16[32,32,128]{2,1,0:T(8,128)(2,1)} %bitcast.9), calls=%async_computation | async-start | bytes 524288 | tf_op jit(solution)/shard_map/all_to_all | solution.py:265
  28.1 0.0 collective-permute-done.refs_0_
  28.1 2.3 %collective-permute-start.1 = (bf16[6144,128]{1,0:T(8,128)(2,1)S(1)}, bf16[6144,128]{1,0:T(8,128)(2,1)S(1)}, u32[]{:S(2)}, u32[]{:S(2)}) collective-permute-start(bf16[6144,128]{1,0:T(8,128)(2,1)S(1)} %collective-permute-done.refs_0_), channel_id=1, source_target_pairs={{0,16},{16,0},{1,17},{17,1},{2,18},{18,2},{3,19},{19,3},{4,20},{20... | collective-permute-start | bytes 4718600 | tf_op jit(solution)/shard_map/ppermute | solution.py:278
  30.4 10.1 %all-to-all-done.slots_ref = bf16[32,32,128]{2,1,0:T(8,128)(2,1)S(1)} async-done(((bf16[32,32,128]{2,1,0:T(8,128)(2,1)}), bf16[32,32,128]{2,1,0:T(8,128)(2,1)S(1)}, u32[]{:S(2)}, u32[]{:S(2)}) %all-to-all-start) | async-done | bytes 262176 | tf_op jit(solution)/shard_map/all_to_all | solution.py:265
  40.5 0.8 shard_map.66
  41.4 20.4 %all_to_all.20.x_ref = bf16[16,256,128]{2,1,0:T(8,128)(2,1)S(1)} all-to-all(bf16[16,256,128]{2,1,0:T(8,128)(2,1)S(1)} %bitcast.6), channel_id=1, replica_groups={{16,17,18,19,20,21,22,23,0,1,2,3,4,5,6,7},{24,25,26,27,28,29,30,31,8,9,..., dimensions={0} | all-to-all | bytes 2097152 | tf_op jit(solution)/shard_map/all_to_all | solution.py:280
  61.8 0.0 collective-permute-done.1.refs_1_
  61.8 1.2 %shard_map.68 = bf16[16,256,128]{2,1,0:T(8,128)(2,1)S(1)} custom-call(bf16[16,256,128]{2,1,0:T(8,128)(2,1)S(1)} %all_to_all.20.x_ref, bf16[6144,128]{1,0:T(8,128)(2,1)S(1)} %collective-permute-done.refs_0_, bf16[6144,128]{1,0:T(8,128)(2,1)S(1)} %collective-permute-done.1.refs_1_), custom_call_target="tpu_custom_call" | custom-call | tf_op jit(solution)/shard_map/pallas_call | solution.py:219
  62.9 18.9 %all_to_all.21 = bf16[16,256,128]{2,1,0:T(8,128)(2,1)S(1)} all-to-all(bf16[16,256,128]{2,1,0:T(8,128)(2,1)S(1)} %shard_map.68), channel_id=1, replica_groups={{16,17,18,19,20,21,22,23,0,1,2,3,4,5,6,7},{24,25,26,27,28,29,30,31,8,9,..., dimensions={0} | all-to-all | bytes 2097152 | tf_op jit(solution)/shard_map/all_to_all | solution.py:295
  81.8 0.0 copy-start
  81.8 0.0 copy-start.1
  81.8 1.5 %shard_map.69 = bf16[32,2,16,128]{3,2,1,0:T(8,128)(2,1)} custom-call(bf16[2,2,4,256,128]{4,3,2,1,0:T(8,128)(2,1)S(1)} %bitcast.7, bf16[32,32,128]{2,1,0:T(8,128)(2,1)S(1)} %all-to-all-done.slots_ref), custom_call_target="tpu_custom_call" | custom-call | tf_op jit(solution)/shard_map/pallas_call | solution.py:219
  83.3 14.6 %all-to-all-start.3 = ((bf16[64,16,128]{2,1,0:T(8,128)(2,1)}), bf16[64,16,128]{2,1,0:T(8,128)(2,1)S(1)}, u32[]{:S(2)}, u32[]{:S(2)}) async-start(bf16[64,16,128]{2,1,0:T(8,128)(2,1)} %bitcast.4), calls=%async_computation.3 | async-start | bytes 524288 | tf_op jit(solution)/shard_map/all_to_all | solution.py:302
  97.9 0.0 copy-done
  98.0 0.0 copy-done.1
  98.0 0.3 shard_map.64.mix_ref
  98.3 14.2 %all-to-all-done.3 = bf16[64,16,128]{2,1,0:T(8,128)(2,1)S(1)} async-done(((bf16[64,16,128]{2,1,0:T(8,128)(2,1)}), bf16[64,16,128]{2,1,0:T(8,128)(2,1)S(1)}, u32[]{:S(2)}, u32[]{:S(2)}) %all-to-all-start.3) | async-done | bytes 262176 | tf_op jit(solution)/shard_map/all_to_all | solution.py:302
  112.4 1.0 shard_map.70
Async XLA Ops:
  1.4 26.7 %collective-permute-start = (bf16[6144,128]{1,0:T(8,128)(2,1)S(1)}, bf16[6144,128]{1,0:T(8,128)(2,1)S(1)}, u32[]{:S(2)}, u32[]{:S(2)}) collective-permute-start(bf16[6144,128]{1,0:T(8,128)(2,1)S(1)} %shard_map.67), channel_id=1, source_target_pairs={{0,0},{4,4},{24,24},{28,28},{16,12},{12,16},{20,8},{8,20},{1,1},{5... | collective-permute-start | bytes 4718600 | tf_op jit(solution)/shard_map/ppermute | solution.py:252
  9.7 30.9 %all-to-all-start = ((bf16[32,32,128]{2,1,0:T(8,128)(2,1)}), bf16[32,32,128]{2,1,0:T(8,128)(2,1)S(1)}, u32[]{:S(2)}, u32[]{:S(2)}) async-start(bf16[32,32,128]{2,1,0:T(8,128)(2,1)} %bitcast.9), calls=%async_computation | async-start | bytes 524288 | tf_op jit(solution)/shard_map/all_to_all | solution.py:265
  28.1 33.6 %collective-permute-start.1 = (bf16[6144,128]{1,0:T(8,128)(2,1)S(1)}, bf16[6144,128]{1,0:T(8,128)(2,1)S(1)}, u32[]{:S(2)}, u32[]{:S(2)}) collective-permute-start(bf16[6144,128]{1,0:T(8,128)(2,1)S(1)} %collective-permute-done.refs_0_), channel_id=1, source_target_pairs={{0,16},{16,0},{1,17},{17,1},{2,18},{18,2},{3,19},{19,3},{4,20},{20... | collective-permute-start | bytes 4718600 | tf_op jit(solution)/shard_map/ppermute | solution.py:278
  81.8 16.1 %copy-start = (s32[32,32]{1,0:T(8,128)S(1)}, s32[32,32]{1,0:T(8,128)}, u32[]{:S(2)}) copy-start(s32[32,32]{1,0:T(8,128)} %selected_ref.3) | copy-start | bytes 12292
  81.8 16.1 %copy-start.1 = (f32[32,32]{1,0:T(8,128)S(1)}, f32[32,32]{1,0:T(8,128)}, u32[]{:S(2)}) copy-start(f32[32,32]{1,0:T(8,128)} %affinity_ref.1) | copy-start | bytes 12292
  83.3 29.1 %all-to-all-start.3 = ((bf16[64,16,128]{2,1,0:T(8,128)(2,1)}), bf16[64,16,128]{2,1,0:T(8,128)(2,1)S(1)}, u32[]{:S(2)}, u32[]{:S(2)}) async-start(bf16[64,16,128]{2,1,0:T(8,128)(2,1)} %bitcast.4), calls=%async_computation.3 | async-start | bytes 524288 | tf_op jit(solution)/shard_map/all_to_all | solution.py:302

commit v14 on v11

--- a/solution.py
+++ b/solution.py
@@ -13,8 +13,18 @@
 F32 = jnp.float32
 EMPTY = 64.0
 LIMIT = 32.0
+FIRST = 10
 TRADE = [(0, 0), (1, 1), (6, 6), (7, 7), (4, 3), (3, 4), (5, 2), (2, 5)]
 CORES = [(0, 1), (1, 0)]
+
+
+def turned_groups(layers, teams):
+    order = [(p + FIRST) % layers for p in range(layers)]
+    return [[(z * 2 + c) * teams + g for z in order for c in (1, 0) for g in range(teams)]]
+
+
+def team_groups(members):
+    return [[(k + members // 2) % members for k in range(members)]]
 
 
 def iota(shape, dim):
@@ -52,7 +62,7 @@
     first.start()
     loads = []
     for c in range(2):
-        at = pl.multiple_of((8 * c + place_ref[0] % 8) * width, width)
+        at = pl.multiple_of((8 * (1 - c) + place_ref[0] % 8) * width, width)
         loads.append(
             pltpu.make_async_copy(tokens_ref.at[:, pl.ds(at, width)], tile_ref.at[c], sems.at[c])
         )
@@ -61,7 +71,8 @@
     slots = here * most
     first.wait()
     sel = sel_ref[...].astype(F32).astype(BF)
-    repeat = one_hot(2 * (iota((slots, experts), 0) // most) + g == iota((slots, experts), 1))
+    layer = (iota((slots, experts), 0) // most + FIRST) % here
+    repeat = one_hot(2 * layer + g == iota((slots, experts), 1))
     own = iota((slots, most), 0) % most == iota((slots, most), 1)
     spread = jnp.where(own, dot(repeat, sel), 0.0).astype(BF)
     position = dot(spread, jnp.ones((most, tok), BF))
@@ -81,7 +92,8 @@
     experts, most = selected_ref.shape
     _, _, tok, slots = mix_ref.shape
     part = most // 2
-    mine = iota((experts, slots), 0) == iota((experts, slots), 1) // part
+    expert = (iota((experts, slots), 1) // part + 2 * FIRST) % experts
+    mine = iota((experts, slots), 0) == expert
     sel = selected_ref[...].astype(F32).astype(BF)
     aff = affinity_ref[...]
     high = aff.astype(BF)
@@ -139,22 +151,22 @@
     for k, ref in enumerate((mine_down_ref, other_down_ref)):
         loads.append(pltpu.make_async_copy(ref, down_ref.at[k], sems.at[k]))
         loads[k].start()
-    x = jnp.concatenate([x_ref[k] for k in range(peers)], axis=1)
+    half = peers // 2
+    x = jnp.concatenate([x_ref[(k + half) % peers] for k in range(peers)], axis=1)
     pair = (mine_ref, other_ref)
     gate = dot(x, jnp.concatenate([w[:width] for w in pair], axis=1))
     up = dot(x, jnp.concatenate([w[width:] for w in pair], axis=1))
     hidden = (gate / (1.0 + jnp.exp(-gate)) * up).astype(BF)
     for load in loads:
         load.wait()
-    half = peers // 2
     for k in range(half):
         tiles = []
         for at in (k * span, (k + half) * span):
             tiles.append(jnp.concatenate([down_ref[j, at : at + span] for j in range(2)], axis=0))
         both = dot(hidden, jnp.concatenate(tiles, axis=1))
         low, high = both[:, :span], both[:, span:]
-        out_ref[k] = joined(low, turned(high)).astype(BF)
-        out_ref[k + half] = joined(turned(low), high).astype(BF)
+        out_ref[k + half] = joined(low, turned(high)).astype(BF)
+        out_ref[k] = joined(turned(low), high).astype(BF)
 
 
 def expand_kernel(parts_ref, slots_ref, out_ref):
@@ -196,8 +208,8 @@
 
 
 def combine_kernel(mix_ref, rows_ref, out_ref):
-    layers, cores, teams, step, width = rows_ref.shape
-    both = [rows_ref[:, c].reshape(layers * teams * step, width) for c in range(cores)]
+    layers, _, teams, step, width = rows_ref.shape
+    both = [rows_ref[:, c].reshape(layers * teams * step, width) for c in (1, 0)]
     both = jnp.concatenate(both, axis=1)
     first = dot(mix_ref[0, 0], both) + dot(mix_ref[0, 1], both)
     second = dot(mix_ref[1, 0], both) + dot(mix_ref[1, 1], both)
@@ -262,7 +274,14 @@
             pltpu.SemaphoreType.DMA((5,)),
         ],
     )
-    arrived = lax.all_to_all(rows.reshape(ep, most, span), EP, 0, 0, tiled=True)
+    arrived = lax.all_to_all(
+        rows.reshape(ep, most, span),
+        EP,
+        0,
+        0,
+        axis_index_groups=turned_groups(layers, 1),
+        tiled=True,
+    )
     mix = local_call(
         mix_kernel,
         pltpu.HBM((2, 2, tok, experts * most // 2), BF),
@@ -275,7 +294,14 @@
     other = lax.ppermute(mine, "c", CORES)
     other_down = lax.ppermute(mine_down, "c", CORES)
     copies = local_call(compact_kernel, array((2, lines, peers, part, span)), arrived)
-    chosen = lax.all_to_all(copies.reshape(team, part, span), TEAM, 0, 0, tiled=True)
+    chosen = lax.all_to_all(
+        copies.reshape(team, part, span),
+        TEAM,
+        0,
+        0,
+        axis_index_groups=team_groups(team),
+        tiled=True,
+    )
     partial = local_call(
         ffn_kernel,
         array((team, part, span)),
@@ -285,7 +311,7 @@
         hbm=(mine_down, other_down),
         scratch=[pltpu.VMEM((2, width, span), BF), pltpu.SemaphoreType.DMA((2,))],
     )
-    summands = lax.all_to_all(partial, TEAM, 0, 0, tiled=True)
+    summands = lax.all_to_all(partial, TEAM, 0, 0, axis_index_groups=team_groups(team), tiled=True)
     result = local_call(
         expand_kernel,
         array((ep, 2, most // 2, span)),
@@ -293,7 +319,12 @@
         arrived,
     )
     returned = lax.all_to_all(
-        result.reshape(2 * ep, most // 2, span), ("z", "c", "g"), 0, 0, tiled=True
+        result.reshape(2 * ep, most // 2, span),
+        ("z", "c", "g"),
+        0,
+        0,
+        axis_index_groups=turned_groups(layers, 2),
+        tiled=True,
     )
     return local_call(
         combine_kernel,

time: 124 us -> 117 us (0.944)
  waiting for transfers between devices: 50.4 us -> 34 us
  starting transfers between devices: 40.2 us -> 49.8 us
    all_to_all x1, starting transfers between devices: 4.32 us -> 12.8 us  [per_device(): lax.all_to_all(result.reshape(2 * ep, most // 2, span), ('z', 'c', 'g'),...]
    all_to_all x2, waiting for transfers between devices: 26.8 us -> 18.6 us  [the longest x1 12 us: per_device(): lax.all_to_all(copies.reshape(team, part, span), TEAM, 0, 0, axis_index_g...]
    all_to_all x1, waiting for transfers between devices: 21.5 us -> 13.6 us  [per_device(): lax.all_to_all(result.reshape(2 * ep, most // 2, span), ('z', 'c', 'g'),...]
where the time goes in v14:
time: 117 us; the launch traced here: 116 us
  starting transfers between devices  49.8 us (43%)
  waiting for transfers between devices  34 us (29%)
  blocking collectives  18.9 us (16%)
  Pallas kernels  12 us (10%)
    all_to_all x1, blocking collectives, per_device(): lax.all_to_all(partial, TEAM, 0, 0, axis_index_groups=team_groups(team),...  18.9 us
    all_to_all x1, starting transfers between devices, per_device(): lax.all_to_all(rows.reshape(ep, most, span), EP, 0, 0, axis_index_groups=...  16.6 us
    all_to_all x1, waiting for transfers between devices, per_device(): lax.all_to_all(result.reshape(2 * ep, most // 2, span), ('z', 'c', 'g'),...  13.6 us
    all_to_all x1, starting transfers between devices, per_device(): lax.all_to_all(result.reshape(2 * ep, most // 2, span), ('z', 'c', 'g'),...  12.8 us
    all_to_all x1, waiting for transfers between devices, per_device(): lax.all_to_all(copies.reshape(team, part, span), TEAM, 0, 0, axis_index_g...  12 us
    pallas_call x7, Pallas kernels, local_call(): pl.pallas_call(kernel, in_specs=specs, out_specs=jax.tree.map(lambda o: p...  12 us
    all_to_all x1, waiting for transfers between devices, per_device(): lax.all_to_all(rows.reshape(ep, most, span), EP, 0, 0, axis_index_groups=...  6.6 us
    ppermute x1, starting transfers between devices, per_device(): mine = lax.ppermute(packed, ('c', 'g', 'yy'), TRADE)  6.02 us
  transfers between devices with their start and end apart: 7, of which 4 were waited for; matrix products, arithmetic and copies ran while one was open for 0% of the time, Pallas kernels for 4%

profile of v14, /device:TPU:1, one launch (start us, length us, event | category | flops | bytes accessed | tf_op | source)
XLA Modules:
  0.0 115.9 jit_solution(15373278791860619760)
XLA Ops:
  0.0 2.2 %shard_map.67 = (bf16[4096,128]{1,0:T(8,128)(2,1)S(1)}, bf16[2048,128]{1,0:T(8,128)(2,1)}) custom-call(bf16[1,2048,128]{2,1,0:T(8,128)(2,1)} %gate_ref.1, bf16[1,2048,128]{2,1,0:T(8,128)(2,1)} %up_ref.1, bf16[1,128,2048]{2,1,0:T(8,128)(2,1)} %down_ref.1), custom_call_target="tpu_custom_call" | custom-call | tf_op jit(solution)/shard_map/pallas_call | solution.py:230
  2.2 6.0 %collective-permute-start = (bf16[4096,128]{1,0:T(8,128)(2,1)S(1)}, bf16[4096,128]{1,0:T(8,128)(2,1)S(1)}, u32[]{:S(2)}, u32[]{:S(2)}) collective-permute-start(bf16[4096,128]{1,0:T(8,128)(2,1)S(1)} %get-tuple-element.7), channel_id=1, source_target_pairs={{0,0},{4,4},{24,24},{28,28},{16,12},{12,16},{20,8},{8,20},{1,1},{5... | collective-permute-start | bytes 3145736 | tf_op jit(solution)/shard_map/ppermute | solution.py:263
  8.3 2.2 %shard_map.65 = bf16[16,2,32,128]{3,2,1,0:T(8,128)(2,1)} custom-call(s32[1]{0:T(128)} %bitcast.place_ref, s32[32,32]{1,0:T(8,128)} %selected_ref.3, bf16[128,2048]{1,0:T(8,128)(2,1)} %tokens_ref.1), custom_call_target="tpu_custom_call" | custom-call | tf_op jit(solution)/shard_map/pallas_call | solution.py:230
  10.5 16.6 %all-to-all-start = ((bf16[32,32,128]{2,1,0:T(8,128)(2,1)}), bf16[32,32,128]{2,1,0:T(8,128)(2,1)S(1)}, u32[]{:S(2)}, u32[]{:S(2)}) async-start(bf16[32,32,128]{2,1,0:T(8,128)(2,1)} %bitcast.8), calls=%async_computation | async-start | bytes 524288 | tf_op jit(solution)/shard_map/all_to_all | solution.py:277
  27.1 2.2 %collective-permute-start.2 = (bf16[2048,128]{1,0:T(8,128)(2,1)}, bf16[2048,128]{1,0:T(8,128)(2,1)}, u32[]{:S(2)}, u32[]{:S(2)}) collective-permute-start(bf16[2048,128]{1,0:T(8,128)(2,1)} %get-tuple-element.8), channel_id=1, source_target_pairs={{0,0},{4,4},{24,24},{28,28},{16,12},{12,16},{20,8},{8,20},{1,1},{5... | collective-permute-start | bytes 1572872 | tf_op jit(solution)/shard_map/ppermute | solution.py:264
  29.3 0.0 collective-permute-done.mine_ref
  29.3 5.4 %collective-permute-start.1 = (bf16[4096,128]{1,0:T(8,128)(2,1)S(1)}, bf16[4096,128]{1,0:T(8,128)(2,1)S(1)}, u32[]{:S(2)}, u32[]{:S(2)}) collective-permute-start(bf16[4096,128]{1,0:T(8,128)(2,1)S(1)} %collective-permute-done.mine_ref), channel_id=1, source_target_pairs={{0,16},{16,0},{1,17},{17,1},{2,18},{18,2},{3,19},{19,3},{4,20},{20... | collective-permute-start | bytes 3145736 | tf_op jit(solution)/shard_map/ppermute | solution.py:294
  34.8 6.6 %all-to-all-done.slots_ref = bf16[32,32,128]{2,1,0:T(8,128)(2,1)S(1)} async-done(((bf16[32,32,128]{2,1,0:T(8,128)(2,1)}), bf16[32,32,128]{2,1,0:T(8,128)(2,1)S(1)}, u32[]{:S(2)}, u32[]{:S(2)}) %all-to-all-start) | async-done | bytes 262176 | tf_op jit(solution)/shard_map/all_to_all | solution.py:277
  41.4 1.8 %shard_map.66 = bf16[2,2,4,256,128]{4,3,2,1,0:T(8,128)(2,1)} custom-call(bf16[32,32,128]{2,1,0:T(8,128)(2,1)S(1)} %all-to-all-done.slots_ref), custom_call_target="tpu_custom_call" | custom-call | tf_op jit(solution)/shard_map/pallas_call | solution.py:230
  43.2 4.4 %all-to-all-start.1 = ((bf16[16,256,128]{2,1,0:T(8,128)(2,1)}), bf16[16,256,128]{2,1,0:T(8,128)(2,1)S(1)}, u32[]{:S(2)}, u32[]{:S(2)}) async-start(bf16[16,256,128]{2,1,0:T(8,128)(2,1)} %bitcast.2), calls=%async_computation.1 | async-start | bytes 2097152 | tf_op jit(solution)/shard_map/all_to_all | solution.py:297
  47.6 0.0 collective-permute-done.2.mine_down_ref
  47.6 2.3 %collective-permute-start.3 = (bf16[2048,128]{1,0:T(8,128)(2,1)}, bf16[2048,128]{1,0:T(8,128)(2,1)}, u32[]{:S(2)}, u32[]{:S(2)}) collective-permute-start(bf16[2048,128]{1,0:T(8,128)(2,1)} %collective-permute-done.2.mine_down_ref), channel_id=1, source_target_pairs={{0,16},{16,0},{1,17},{17,1},{2,18},{18,2},{3,19},{19,3},{4,20},{20... | collective-permute-start | bytes 1572872 | tf_op jit(solution)/shard_map/ppermute | solution.py:295
  49.9 1.9 %collective-permute-done.3.other_down_ref = bf16[2048,128]{1,0:T(8,128)(2,1)} collective-permute-done((bf16[2048,128]{1,0:T(8,128)(2,1)}, bf16[2048,128]{1,0:T(8,128)(2,1)}, u32[]{:S(2)}, u32[]{:S(2)}) %collective-permute-start.3) | collective-permute-done | bytes 524320 | tf_op jit(solution)/shard_map/ppermute | solution.py:295
  51.8 12.0 %all-to-all-done.1.x_ref = bf16[16,256,128]{2,1,0:T(8,128)(2,1)S(1)} async-done(((bf16[16,256,128]{2,1,0:T(8,128)(2,1)}), bf16[16,256,128]{2,1,0:T(8,128)(2,1)S(1)}, u32[]{:S(2)}, u32[]{:S(2)}) %all-to-all-start.1) | async-done | bytes 1048608 | tf_op jit(solution)/shard_map/all_to_all | solution.py:297
  63.8 0.0 collective-permute-done.1.other_ref
  63.8 2.2 %shard_map.68 = bf16[16,256,128]{2,1,0:T(8,128)(2,1)S(1)} custom-call(bf16[16,256,128]{2,1,0:T(8,128)(2,1)S(1)} %all-to-all-done.1.x_ref, bf16[4096,128]{1,0:T(8,128)(2,1)S(1)} %collective-permute-done.mine_ref, bf16[4096,128]{1,0:T(8,128)(2,1)S(1)} %collective-permute-done.1.other_ref, bf16[2048,128]{1,0:T(8,128)(2,1)} %collective-permute-done.2.mine_down_ref, ...), custom_call_target="tpu_custom_call" | custom-call | tf_op jit(solution)/shard_map/pallas_call | solution.py:230
  66.0 18.9 %all_to_all.20 = bf16[16,256,128]{2,1,0:T(8,128)(2,1)S(1)} all-to-all(bf16[16,256,128]{2,1,0:T(8,128)(2,1)S(1)} %shard_map.68), channel_id=1, replica_groups={{16,17,18,19,20,21,22,23,0,1,2,3,4,5,6,7},{24,25,26,27,28,29,30,31,8,9,..., dimensions={0} | all-to-all | bytes 2097152 | tf_op jit(solution)/shard_map/all_to_all | solution.py:314
  84.9 1.5 %shard_map.69 = bf16[32,2,16,128]{3,2,1,0:T(8,128)(2,1)} custom-call(bf16[2,2,4,256,128]{4,3,2,1,0:T(8,128)(2,1)S(1)} %bitcast.6, bf16[32,32,128]{2,1,0:T(8,128)(2,1)S(1)} %all-to-all-done.slots_ref), custom_call_target="tpu_custom_call" | custom-call | tf_op jit(solution)/shard_map/pallas_call | solution.py:230
  86.4 0.0 copy-start.1
  86.4 0.0 copy-start.2
  86.4 12.8 %all-to-all-start.3 = ((bf16[64,16,128]{2,1,0:T(8,128)(2,1)}), bf16[64,16,128]{2,1,0:T(8,128)(2,1)S(1)}, u32[]{:S(2)}, u32[]{:S(2)}) async-start(bf16[64,16,128]{2,1,0:T(8,128)(2,1)} %bitcast.4), calls=%async_computation.3 | async-start | bytes 524288 | tf_op jit(solution)/shard_map/all_to_all | solution.py:321
  99.2 0.0 copy-done.1
  99.2 0.0 copy-done.2
  99.2 1.1 shard_map.64.mix_ref
  100.3 13.6 %all-to-all-done.3 = bf16[64,16,128]{2,1,0:T(8,128)(2,1)S(1)} async-done(((bf16[64,16,128]{2,1,0:T(8,128)(2,1)}), bf16[64,16,128]{2,1,0:T(8,128)(2,1)S(1)}, u32[]{:S(2)}, u32[]{:S(2)}) %all-to-all-start.3) | async-done | bytes 262176 | tf_op jit(solution)/shard_map/all_to_all | solution.py:321
  113.9 0.0 copy-start
  113.9 1.0 copy-done
  114.9 1.0 shard_map.70
Async XLA Ops:
  2.2 27.1 %collective-permute-start = (bf16[4096,128]{1,0:T(8,128)(2,1)S(1)}, bf16[4096,128]{1,0:T(8,128)(2,1)S(1)}, u32[]{:S(2)}, u32[]{:S(2)}) collective-permute-start(bf16[4096,128]{1,0:T(8,128)(2,1)S(1)} %get-tuple-element.7), channel_id=1, source_target_pairs={{0,0},{4,4},{24,24},{28,28},{16,12},{12,16},{20,8},{8,20},{1,1},{5... | collective-permute-start | bytes 3145736 | tf_op jit(solution)/shard_map/ppermute | solution.py:263
  10.5 30.9 %all-to-all-start = ((bf16[32,32,128]{2,1,0:T(8,128)(2,1)}), bf16[32,32,128]{2,1,0:T(8,128)(2,1)S(1)}, u32[]{:S(2)}, u32[]{:S(2)}) async-start(bf16[32,32,128]{2,1,0:T(8,128)(2,1)} %bitcast.8), calls=%async_computation | async-start | bytes 524288 | tf_op jit(solution)/shard_map/all_to_all | solution.py:277
  27.1 20.5 %collective-permute-start.2 = (bf16[2048,128]{1,0:T(8,128)(2,1)}, bf16[2048,128]{1,0:T(8,128)(2,1)}, u32[]{:S(2)}, u32[]{:S(2)}) collective-permute-start(bf16[2048,128]{1,0:T(8,128)(2,1)} %get-tuple-element.8), channel_id=1, source_target_pairs={{0,0},{4,4},{24,24},{28,28},{16,12},{12,16},{20,8},{8,20},{1,1},{5... | collective-permute-start | bytes 1572872 | tf_op jit(solution)/shard_map/ppermute | solution.py:264
  29.3 34.5 %collective-permute-start.1 = (bf16[4096,128]{1,0:T(8,128)(2,1)S(1)}, bf16[4096,128]{1,0:T(8,128)(2,1)S(1)}, u32[]{:S(2)}, u32[]{:S(2)}) collective-permute-start(bf16[4096,128]{1,0:T(8,128)(2,1)S(1)} %collective-permute-done.mine_ref), channel_id=1, source_target_pairs={{0,16},{16,0},{1,17},{17,1},{2,18},{18,2},{3,19},{19,3},{4,20},{20... | collective-permute-start | bytes 3145736 | tf_op jit(solution)/shard_map/ppermute | solution.py:294
  43.2 20.6 %all-to-all-start.1 = ((bf16[16,256,128]{2,1,0:T(8,128)(2,1)}), bf16[16,256,128]{2,1,0:T(8,128)(2,1)S(1)}, u32[]{:S(2)}, u32[]{:S(2)}) async-start(bf16[16,256,128]{2,1,0:T(8,128)(2,1)} %bitcast.2), calls=%async_computation.1 | async-start | bytes 2097152 | tf_op jit(solution)/shard_map/all_to_all | solution.py:297
  47.6 4.2 %collective-permute-start.3 = (bf16[2048,128]{1,0:T(8,128)(2,1)}, bf16[2048,128]{1,0:T(8,128)(2,1)}, u32[]{:S(2)}, u32[]{:S(2)}) collective-permute-start(bf16[2048,128]{1,0:T(8,128)(2,1)} %collective-permute-done.2.mine_down_ref), channel_id=1, source_target_pairs={{0,16},{16,0},{1,17},{17,1},{2,18},{18,2},{3,19},{19,3},{4,20},{20... | collective-permute-start | bytes 1572872 | tf_op jit(solution)/shard_map/ppermute | solution.py:295
  86.4 12.8 %copy-start.1 = (s32[32,32]{1,0:T(8,128)S(1)}, s32[32,32]{1,0:T(8,128)}, u32[]{:S(2)}) copy-start(s32[32,32]{1,0:T(8,128)} %selected_ref.3) | copy-start | bytes 12292
  86.4 12.9 %copy-start.2 = (f32[32,32]{1,0:T(8,128)S(1)}, f32[32,32]{1,0:T(8,128)}, u32[]{:S(2)}) copy-start(f32[32,32]{1,0:T(8,128)} %affinity_ref.1) | copy-start | bytes 12292
  86.4 27.5 %all-to-all-start.3 = ((bf16[64,16,128]{2,1,0:T(8,128)(2,1)}), bf16[64,16,128]{2,1,0:T(8,128)(2,1)S(1)}, u32[]{:S(2)}, u32[]{:S(2)}) async-start(bf16[64,16,128]{2,1,0:T(8,128)(2,1)} %bitcast.4), calls=%async_computation.3 | async-start | bytes 524288 | tf_op jit(solution)/shard_map/all_to_all | solution.py:321
  113.9 1.0 copy-start

commit v15 on v13

--- a/solution.py
+++ b/solution.py
@@ -13,12 +13,13 @@
 F32 = jnp.float32
 EMPTY = 64.0
 LIMIT = 32.0
+FIRST = 11
 TRADE = [(0, 0), (1, 1), (6, 6), (7, 7), (4, 3), (3, 4), (5, 2), (2, 5)]
 CORES = [(0, 1), (1, 0)]
 
 
 def turned_groups(layers, teams):
-    order = [(p + layers // 2) % layers for p in range(layers)]
+    order = [(p + FIRST) % layers for p in range(layers)]
     return [[(z * 2 + c) * teams + g for z in order for c in (1, 0) for g in range(teams)]]
 
 
@@ -68,7 +69,7 @@
     slots = here * most
     first.wait()
     sel = sel_ref[...].astype(F32).astype(BF)
-    layer = (iota((slots, experts), 0) // most + here // 2) % here
+    layer = (iota((slots, experts), 0) // most + FIRST) % here
     repeat = one_hot(2 * layer + g == iota((slots, experts), 1))
     own = iota((slots, most), 0) % most == iota((slots, most), 1)
     spread = jnp.where(own, dot(repeat, sel), 0.0).astype(BF)
@@ -89,7 +90,7 @@
     experts, most = selected_ref.shape
     _, _, tok, slots = mix_ref.shape
     part = most // 2
-    expert = (iota((experts, slots), 1) // part + experts // 2) % experts
+    expert = (iota((experts, slots), 1) // part + 2 * FIRST) % experts
     mine = iota((experts, slots), 0) == expert
     sel = selected_ref[...].astype(F32).astype(BF)
     aff = affinity_ref[...]

time: 114 us -> 112 us (0.982)
  starting transfers between devices: 41.4 us -> 35.4 us
  waiting for transfers between devices: 24.3 us -> 28.3 us
    all_to_all x1, starting transfers between devices: 14.6 us -> 11.6 us  [per_device(): lax.all_to_all(result.reshape(2 * ep, most // 2, span), ('z', 'c', 'g'),...]
    all_to_all x1, waiting for transfers between devices: 10.1 us -> 12.9 us  [per_device(): lax.all_to_all(rows.reshape(ep, most, span), EP, 0, 0, axis_index_groups=...]
    all_to_all x1, starting transfers between devices: 18.5 us -> 15.8 us  [per_device(): lax.all_to_all(rows.reshape(ep, most, span), EP, 0, 0, axis_index_groups=...]
  transfers between devices with their start and end apart: 4 -> 4, of which waited for: 2 -> 3; matrix products, arithmetic and copies ran while one was open for 0% -> 0% of each run, Pallas kernels for 3% -> 3%
where the time goes in v15:
time: 112 us; the launch traced here: 111 us
  blocking collectives  39.1 us (35%)
  starting transfers between devices  35.4 us (32%)
  waiting for transfers between devices  28.3 us (25%)
  Pallas kernels  8.32 us (7%)
    all_to_all x1, blocking collectives, per_device(): lax.all_to_all(copies.reshape(team, part, span), TEAM, 0, 0, axis_index_g...  20.2 us
    all_to_all x1, blocking collectives, per_device(): lax.all_to_all(partial, TEAM, 0, 0, axis_index_groups=team_groups(team),...  18.9 us
    all_to_all x1, starting transfers between devices, per_device(): lax.all_to_all(rows.reshape(ep, most, span), EP, 0, 0, axis_index_groups=...  15.8 us
    all_to_all x1, waiting for transfers between devices, per_device(): lax.all_to_all(result.reshape(2 * ep, most // 2, span), ('z', 'c', 'g'),...  15 us
    all_to_all x1, waiting for transfers between devices, per_device(): lax.all_to_all(rows.reshape(ep, most, span), EP, 0, 0, axis_index_groups=...  12.9 us
    all_to_all x1, starting transfers between devices, per_device(): lax.all_to_all(result.reshape(2 * ep, most // 2, span), ('z', 'c', 'g'),...  11.6 us
    pallas_call x7, Pallas kernels, local_call(): pl.pallas_call(kernel, in_specs=specs, out_specs=jax.tree.map(lambda o: p...  8.32 us
    ppermute x1, starting transfers between devices, per_device(): mine = lax.ppermute(packed, ('c', 'g', 'yy'), TRADE)  6.02 us
  transfers between devices with their start and end apart: 4, of which 3 were waited for; matrix products, arithmetic and copies ran while one was open for 0% of the time, Pallas kernels for 3%

profile of v15, /device:TPU:1, one launch (start us, length us, event | category | flops | bytes accessed | tf_op | source)
XLA Modules:
  0.0 111.2 jit_solution(16848447694021724550)
XLA Ops:
  0.0 1.4 %shard_map.67 = bf16[6144,128]{1,0:T(8,128)(2,1)S(1)} custom-call(bf16[1,2048,128]{2,1,0:T(8,128)(2,1)} %gate_ref.1, bf16[1,2048,128]{2,1,0:T(8,128)(2,1)} %up_ref.1, bf16[1,128,2048]{2,1,0:T(8,128)(2,1)} %down_ref.1), custom_call_target="tpu_custom_call" | custom-call | tf_op jit(solution)/shard_map/pallas_call | solution.py:220
  1.4 6.0 %collective-permute-start = (bf16[6144,128]{1,0:T(8,128)(2,1)S(1)}, bf16[6144,128]{1,0:T(8,128)(2,1)S(1)}, u32[]{:S(2)}, u32[]{:S(2)}) collective-permute-start(bf16[6144,128]{1,0:T(8,128)(2,1)S(1)} %shard_map.67), channel_id=1, source_target_pairs={{0,0},{4,4},{24,24},{28,28},{16,12},{12,16},{20,8},{8,20},{1,1},{5... | collective-permute-start | bytes 4718600 | tf_op jit(solution)/shard_map/ppermute | solution.py:253
  7.5 2.2 %shard_map.65 = bf16[16,2,32,128]{3,2,1,0:T(8,128)(2,1)} custom-call(s32[1]{0:T(128)} %bitcast.place_ref, s32[32,32]{1,0:T(8,128)} %selected_ref.3, bf16[128,2048]{1,0:T(8,128)(2,1)} %tokens_ref.1), custom_call_target="tpu_custom_call" | custom-call | tf_op jit(solution)/shard_map/pallas_call | solution.py:220
  9.7 15.8 %all-to-all-start = ((bf16[32,32,128]{2,1,0:T(8,128)(2,1)}), bf16[32,32,128]{2,1,0:T(8,128)(2,1)S(1)}, u32[]{:S(2)}, u32[]{:S(2)}) async-start(bf16[32,32,128]{2,1,0:T(8,128)(2,1)} %bitcast.9), calls=%async_computation | async-start | bytes 524288 | tf_op jit(solution)/shard_map/all_to_all | solution.py:266
  25.5 0.4 collective-permute-done.refs_0_
  25.8 1.9 %collective-permute-start.1 = (bf16[6144,128]{1,0:T(8,128)(2,1)S(1)}, bf16[6144,128]{1,0:T(8,128)(2,1)S(1)}, u32[]{:S(2)}, u32[]{:S(2)}) collective-permute-start(bf16[6144,128]{1,0:T(8,128)(2,1)S(1)} %collective-permute-done.refs_0_), channel_id=1, source_target_pairs={{0,16},{16,0},{1,17},{17,1},{2,18},{18,2},{3,19},{19,3},{4,20},{20... | collective-permute-start | bytes 4718600 | tf_op jit(solution)/shard_map/ppermute | solution.py:279
  27.8 12.9 %all-to-all-done.slots_ref = bf16[32,32,128]{2,1,0:T(8,128)(2,1)S(1)} async-done(((bf16[32,32,128]{2,1,0:T(8,128)(2,1)}), bf16[32,32,128]{2,1,0:T(8,128)(2,1)S(1)}, u32[]{:S(2)}, u32[]{:S(2)}) %all-to-all-start) | async-done | bytes 262176 | tf_op jit(solution)/shard_map/all_to_all | solution.py:266
  40.7 0.8 shard_map.66
  41.5 20.2 %all_to_all.20.x_ref = bf16[16,256,128]{2,1,0:T(8,128)(2,1)S(1)} all-to-all(bf16[16,256,128]{2,1,0:T(8,128)(2,1)S(1)} %bitcast.6), channel_id=1, replica_groups={{16,17,18,19,20,21,22,23,0,1,2,3,4,5,6,7},{24,25,26,27,28,29,30,31,8,9,..., dimensions={0} | all-to-all | bytes 2097152 | tf_op jit(solution)/shard_map/all_to_all | solution.py:281
  61.7 0.0 collective-permute-done.1.refs_1_
  61.7 1.2 %shard_map.68 = bf16[16,256,128]{2,1,0:T(8,128)(2,1)S(1)} custom-call(bf16[16,256,128]{2,1,0:T(8,128)(2,1)S(1)} %all_to_all.20.x_ref, bf16[6144,128]{1,0:T(8,128)(2,1)S(1)} %collective-permute-done.refs_0_, bf16[6144,128]{1,0:T(8,128)(2,1)S(1)} %collective-permute-done.1.refs_1_), custom_call_target="tpu_custom_call" | custom-call | tf_op jit(solution)/shard_map/pallas_call | solution.py:220
  62.8 18.9 %all_to_all.21 = bf16[16,256,128]{2,1,0:T(8,128)(2,1)S(1)} all-to-all(bf16[16,256,128]{2,1,0:T(8,128)(2,1)S(1)} %shard_map.68), channel_id=1, replica_groups={{16,17,18,19,20,21,22,23,0,1,2,3,4,5,6,7},{24,25,26,27,28,29,30,31,8,9,..., dimensions={0} | all-to-all | bytes 2097152 | tf_op jit(solution)/shard_map/all_to_all | solution.py:296
  81.7 0.0 copy-start
  81.7 0.0 copy-start.1
  81.7 1.5 %shard_map.69 = bf16[32,2,16,128]{3,2,1,0:T(8,128)(2,1)} custom-call(bf16[2,2,4,256,128]{4,3,2,1,0:T(8,128)(2,1)S(1)} %bitcast.7, bf16[32,32,128]{2,1,0:T(8,128)(2,1)S(1)} %all-to-all-done.slots_ref), custom_call_target="tpu_custom_call" | custom-call | tf_op jit(solution)/shard_map/pallas_call | solution.py:220
  83.2 11.6 %all-to-all-start.3 = ((bf16[64,16,128]{2,1,0:T(8,128)(2,1)}), bf16[64,16,128]{2,1,0:T(8,128)(2,1)S(1)}, u32[]{:S(2)}, u32[]{:S(2)}) async-start(bf16[64,16,128]{2,1,0:T(8,128)(2,1)} %bitcast.4), calls=%async_computation.3 | async-start | bytes 524288 | tf_op jit(solution)/shard_map/all_to_all | solution.py:303
  94.8 0.0 copy-done
  94.8 0.0 copy-done.1
  94.8 0.3 shard_map.64.mix_ref
  95.1 15.0 %all-to-all-done.3 = bf16[64,16,128]{2,1,0:T(8,128)(2,1)S(1)} async-done(((bf16[64,16,128]{2,1,0:T(8,128)(2,1)}), bf16[64,16,128]{2,1,0:T(8,128)(2,1)S(1)}, u32[]{:S(2)}, u32[]{:S(2)}) %all-to-all-start.3) | async-done | bytes 262176 | tf_op jit(solution)/shard_map/all_to_all | solution.py:303
  110.2 1.0 shard_map.70
Async XLA Ops:
  1.4 24.4 %collective-permute-start = (bf16[6144,128]{1,0:T(8,128)(2,1)S(1)}, bf16[6144,128]{1,0:T(8,128)(2,1)S(1)}, u32[]{:S(2)}, u32[]{:S(2)}) collective-permute-start(bf16[6144,128]{1,0:T(8,128)(2,1)S(1)} %shard_map.67), channel_id=1, source_target_pairs={{0,0},{4,4},{24,24},{28,28},{16,12},{12,16},{20,8},{8,20},{1,1},{5... | collective-permute-start | bytes 4718600 | tf_op jit(solution)/shard_map/ppermute | solution.py:253
  9.7 31.0 %all-to-all-start = ((bf16[32,32,128]{2,1,0:T(8,128)(2,1)}), bf16[32,32,128]{2,1,0:T(8,128)(2,1)S(1)}, u32[]{:S(2)}, u32[]{:S(2)}) async-start(bf16[32,32,128]{2,1,0:T(8,128)(2,1)} %bitcast.9), calls=%async_computation | async-start | bytes 524288 | tf_op jit(solution)/shard_map/all_to_all | solution.py:266
  25.8 35.8 %collective-permute-start.1 = (bf16[6144,128]{1,0:T(8,128)(2,1)S(1)}, bf16[6144,128]{1,0:T(8,128)(2,1)S(1)}, u32[]{:S(2)}, u32[]{:S(2)}) collective-permute-start(bf16[6144,128]{1,0:T(8,128)(2,1)S(1)} %collective-permute-done.refs_0_), channel_id=1, source_target_pairs={{0,16},{16,0},{1,17},{17,1},{2,18},{18,2},{3,19},{19,3},{4,20},{20... | collective-permute-start | bytes 4718600 | tf_op jit(solution)/shard_map/ppermute | solution.py:279
  81.7 13.1 %copy-start = (s32[32,32]{1,0:T(8,128)S(1)}, s32[32,32]{1,0:T(8,128)}, u32[]{:S(2)}) copy-start(s32[32,32]{1,0:T(8,128)} %selected_ref.3) | copy-start | bytes 12292
  81.7 13.1 %copy-start.1 = (f32[32,32]{1,0:T(8,128)S(1)}, f32[32,32]{1,0:T(8,128)}, u32[]{:S(2)}) copy-start(f32[32,32]{1,0:T(8,128)} %affinity_ref.1) | copy-start | bytes 12292
  83.2 27.0 %all-to-all-start.3 = ((bf16[64,16,128]{2,1,0:T(8,128)(2,1)}), bf16[64,16,128]{2,1,0:T(8,128)(2,1)S(1)}, u32[]{:S(2)}, u32[]{:S(2)}) async-start(bf16[64,16,128]{2,1,0:T(8,128)(2,1)} %bitcast.4), calls=%async_computation.3 | async-start | bytes 524288 | tf_op jit(solution)/shard_map/all_to_all | solution.py:303
